TPU v7x, 32 devices: a whole 2x2x4 slice. The times are simulated.
32 devices in a mesh: ep: 16 (over z, y, x), tp: 2 (over core).
Axes of the slice: x: 2, y: 2, z: 4, core: 2. Of those that a mesh axis runs over, the one named last changes fastest.
Arguments:
- tokens: bfloat16 [64, 4096], P('ep'), may hold values from -6 to 6
- memory: float32 [64, 8, 256, 512], P('ep', 'tp'), may hold values from -6 to 6
- normalizer: float32 [64, 8, 256], P('ep', 'tp'), may hold values from -6 to 6
- stabilizer: float32 [64, 8], P('ep', 'tp'), may hold values from -4 to 4
- norm_gain: float32 [4096], replicated, may hold values from 0.1 to 1.9
- w_query: bfloat16 [4096, 8, 256], P(None, 'tp', 'ep'), may hold values from -0.09375 to 0.09375
- w_key: bfloat16 [4096, 8, 256], P(None, 'tp', 'ep'), may hold values from -0.09375 to 0.09375
- w_value: bfloat16 [4096, 8, 512], P(None, 'tp', 'ep'), may hold values from -0.09375 to 0.09375
- w_outgate: bfloat16 [4096, 8, 512], P(None, 'tp', 'ep'), may hold values from -0.09375 to 0.09375
- w_input: bfloat16 [4096, 8], P(None, 'tp'), may hold values from -0.09375 to 0.09375
- w_forget: bfloat16 [4096, 8], P(None, 'tp'), may hold values from -0.09375 to 0.09375
- forget_bias: float32 [8], P('tp'), may hold values from 0 to 4
- w_out: bfloat16 [4096, 4096], P('tp', 'ep'), may hold values from -0.09375 to 0.09375
- ffn_gain: float32 [4096], replicated, may hold values from 0.1 to 1.9
- w_gate: bfloat16 [16, 4096, 512], P('ep', None, 'tp'), may hold values from -0.09375 to 0.09375
- w_up: bfloat16 [16, 4096, 512], P('ep', None, 'tp'), may hold values from -0.09375 to 0.09375
- w_down: bfloat16 [16, 512, 4096], P('ep', 'tp'), may hold values from -0.25 to 0.25
- expert_ids: int32 [64, 2], P('ep'), may hold values from 0 to 15, as said below
- route_weights: float32 [64, 2], P('ep'), may hold values from 0.1 to 1
Outputs:
- out: bfloat16 [64, 4096], P('ep')
- memory_next: float32 [64, 8, 256, 512], P('ep', 'tp')
- normalizer_next: float32 [64, 8, 256], P('ep', 'tp')
- stabilizer_next: float32 [64, 8], P('ep', 'tp')
Inputs may be any that keep to these rules, and one draw needn't show every extreme that they name: `expert_ids`: the 2 experts of a token differ and lie in one group of 8 consecutive experts. Beyond that, any choice is allowed: for instance, all 4 tokens of one index of ep may name the same expert.
All inputs are finite; a program needn't handle non-finite values.
Results may differ from a plain program's by a relative error of at most 0.013.
Values may be sent and summed in bfloat16 or wider, within the bound.
No kernel may reach another device: no remote copies, remote signals or barrier semaphores. Data moves between devices by JAX's collectives and lax.ppermute only.
A program may use at most 128 MiB of HBM per device.

v0:
```python
import jax
import jax.numpy as jnp
from jax import lax
from jax.sharding import PartitionSpec as P


def rms_scale(values, gain):
    return values * lax.rsqrt(jnp.mean(values * values, axis=-1, keepdims=True) + 1e-06) * gain


def product(left, right):
    return jnp.dot(left, right, preferred_element_type=jnp.float32)


def rounded_term(values):
    return lax.optimization_barrier(values.astype(jnp.bfloat16)).astype(jnp.float32)


def body(
    tokens,
    memory,
    normalizer,
    stabilizer,
    norm_gain,
    w_query,
    w_key,
    w_value,
    w_outgate,
    w_input,
    w_forget,
    forget_bias,
    w_out,
    ffn_gain,
    w_gate,
    w_up,
    w_down,
    expert_ids,
    route_weights,
):
    seqs, width = tokens.shape
    heads, key_size, value_size = (memory.shape[1], memory.shape[2], memory.shape[3])
    value_width = heads * value_size
    key_piece = w_query.shape[2]
    value_piece = w_value.shape[2]
    query_cols = w_query.reshape(width, heads * key_piece)
    key_cols = w_key.reshape(width, heads * key_piece)
    value_cols = w_value.reshape(width, heads * value_piece)
    outgate_cols = w_outgate.reshape(width, heads * value_piece)
    normed = rms_scale(tokens.astype(jnp.float32), norm_gain).astype(jnp.bfloat16)
    piece = lax.all_gather(normed, "ep", axis=0, tiled=True)
    projected = jnp.concatenate(
        [
            product(piece, query_cols),
            product(piece, key_cols),
            product(piece, value_cols),
            product(piece, outgate_cols),
        ],
        axis=1,
    ).astype(jnp.bfloat16)
    all_rows = projected.shape[0]
    narrow = heads * key_piece
    broad = heads * value_piece
    query_part = projected[:, :narrow].reshape(all_rows, heads, key_piece)
    key_part = projected[:, narrow : 2 * narrow].reshape(all_rows, heads, key_piece)
    value_part = projected[:, 2 * narrow : 2 * narrow + broad].reshape(all_rows, heads, value_piece)
    outgate_part = projected[:, 2 * narrow + broad :].reshape(all_rows, heads, value_piece)
    query, key, value, outgate = (
        lax.all_to_all(query_part, "ep", split_axis=0, concat_axis=2, tiled=True),
        lax.all_to_all(key_part, "ep", split_axis=0, concat_axis=2, tiled=True),
        lax.all_to_all(value_part, "ep", split_axis=0, concat_axis=2, tiled=True),
        lax.all_to_all(outgate_part, "ep", split_axis=0, concat_axis=2, tiled=True),
    )
    in_pre = product(normed, w_input)
    log_forget = jax.nn.log_sigmoid(product(normed, w_forget) + forget_bias)
    scaled = query.astype(jnp.float32) * key_size ** (-0.5)
    key_heads = key.astype(jnp.float32)
    value_heads = value.astype(jnp.float32)
    stab_next = jnp.maximum(log_forget + stabilizer, in_pre)
    decay = jnp.exp(log_forget + stabilizer - stab_next)
    inweight = jnp.exp(in_pre - stab_next)
    memory_next = decay[:, :, None, None] * memory + inweight[:, :, None, None] * (
        key_heads[:, :, :, None] * value_heads[:, :, None, :]
    )
    normalizer_next = decay[:, :, None] * normalizer + inweight[:, :, None] * key_heads
    numerator = jnp.einsum("shd,shde->she", scaled, memory_next, precision=lax.Precision.HIGHEST)
    denominator = jnp.sum(scaled * normalizer_next, axis=-1)
    hidden = numerator / jnp.maximum(jnp.abs(denominator), jnp.exp(-stab_next))[:, :, None]
    hidden = (
        hidden.reshape(seqs, value_width)
        * jax.nn.sigmoid(outgate.reshape(seqs, value_width).astype(jnp.float32))
    ).astype(jnp.bfloat16)
    partial_value = product(lax.all_gather(hidden, "ep", axis=0, tiled=True), w_out)
    summed = lax.psum(rounded_term(partial_value).astype(jnp.bfloat16), "tp")
    mixed = lax.all_to_all(summed, "ep", split_axis=0, concat_axis=1, tiled=True)
    resid = tokens.astype(jnp.float32) + mixed.astype(jnp.float32)
    ffn_in = rms_scale(resid, ffn_gain).astype(jnp.bfloat16)
    gate_local, up_local, down_local = (w_gate[0], w_up[0], w_down[0])
    n_experts = lax.axis_size("ep") * w_gate.shape[0]
    piece = lax.all_gather(ffn_in, "ep", axis=0, tiled=True)
    gate_part = product(piece, gate_local)
    up_part = product(piece, up_local)
    act = (jax.nn.silu(gate_part) * up_part).astype(jnp.bfloat16)
    expert_terms = rounded_term(product(act, down_local))
    labels = jnp.arange(n_experts, dtype=jnp.int32)
    route_dense = jnp.sum(
        jnp.where(expert_ids[:, :, None] == labels[None, None, :], route_weights[:, :, None], 0.0),
        axis=1,
    )
    my_weight = lax.all_to_all(route_dense, "ep", split_axis=1, concat_axis=0, tiled=True)
    contrib = expert_terms * my_weight
    n_ep = lax.axis_size("ep")
    n_tp = lax.axis_size("tp")
    arranged = jnp.swapaxes(contrib.reshape(n_ep, seqs, n_tp, width // n_tp), 1, 2)
    arranged = arranged.reshape(n_ep * n_tp * seqs, width // n_tp)
    mine = lax.psum_scatter(arranged, ("ep", "tp"), scatter_dimension=0, tiled=True)
    ffn_out = lax.all_gather(mine.astype(jnp.bfloat16), "tp", axis=1, tiled=True).astype(mine.dtype)
    out = (resid + ffn_out).astype(jnp.bfloat16)
    return (out, memory_next, normalizer_next, stab_next)


def solution(mesh):
    return jax.shard_map(
        body,
        mesh=mesh,
        in_specs=(
            P("ep", None),
            P("ep", "tp", None, None),
            P("ep", "tp", None),
            P("ep", "tp"),
            P(),
            P(None, "tp", "ep"),
            P(None, "tp", "ep"),
            P(None, "tp", "ep"),
            P(None, "tp", "ep"),
            P(None, "tp"),
            P(None, "tp"),
            P("tp"),
            P("tp", "ep"),
            P(),
            P("ep", None, "tp"),
            P("ep", None, "tp"),
            P("ep", "tp", None),
            P("ep", None),
            P("ep", None),
        ),
        out_specs=(P("ep", None), P("ep", "tp", None, None), P("ep", "tp", None), P("ep", "tp")),
        check_vma=False,
    )
```

profile of v0, /device:TPU:0, one launch (start us, length us, event | category | flops | bytes accessed | tf_op | source)
XLA Modules:
  0.0 274.0 jit_solution(16929384175384432204)
XLA Ops:
  0.7 1.1 fusion.14
  1.7 0.9 fusion.49
  2.6 45.3 %all-gather = bf16[16,4,4096]{2,1,0:T(4,128)(2,1)S(1)} all-gather(bf16[1,4,4096]{2,1,0:T(4,128)(2,1)S(1)} %fusion.49), channel_id=1, replica_groups=mesh['ep'=16,'tp'=2] {'ep'}, dimensions={0}, use_global_device_ids=true | all-gather | bytes 557056 | tf_op jit(solution)/shard_map/all_gather | solution.py:50
  48.0 1.3 convolution_convert_fusion.4
  49.5 0.1 copy.119
  49.6 0.7 reshape.153
  50.3 3.5 %all-to-all-start.1 = ((bf16[16,2,128]{2,1,0:T(2,128)(2,1)}), bf16[16,2,128]{2,1,0:T(2,128)(2,1)S(1)}, u32[]{:S(2)}, u32[]{:S(2)}) async-start(bf16[16,2,128]{2,1,0:T(2,128)(2,1)} %reshape.153), calls=%async_computation.1 | async-start | bytes 16384 | tf_op jit(solution)/shard_map/all_to_all | solution.py:69
  53.8 0.8 fusion.16
  54.6 0.9 fusion.29
  55.5 0.9 subtract_exponential_fusion.1
  56.5 1.3 convolution_convert_fusion.5
  57.9 1.7 convolution_convert_fusion.3
  59.6 1.7 convolution_convert_fusion.2
  61.3 0.8 select_reduce_fusion
  62.2 0.1 copy.114
  62.3 0.7 reshape.149
  63.1 0.1 copy.123
  63.2 0.7 reshape.151
  64.1 0.1 copy.127
  64.2 0.7 reshape.155
  64.9 0.7 copy.131
  65.6 6.9 %all-to-all-start = ((bf16[16,2,128]{2,1,0:T(2,128)(2,1)}), bf16[16,2,128]{2,1,0:T(2,128)(2,1)S(1)}, u32[]{:S(2)}, u32[]{:S(2)}) async-start(bf16[16,2,128]{2,1,0:T(2,128)(2,1)} %reshape.149), calls=%async_computation | async-start | bytes 16384 | tf_op jit(solution)/shard_map/all_to_all | solution.py:68
  72.7 7.0 %all-to-all-done = bf16[16,2,128]{2,1,0:T(2,128)(2,1)S(1)} async-done(((bf16[16,2,128]{2,1,0:T(2,128)(2,1)}), bf16[16,2,128]{2,1,0:T(2,128)(2,1)S(1)}, u32[]{:S(2)}, u32[]{:S(2)}) %all-to-all-start) | async-done | bytes 8224 | tf_op jit(solution)/shard_map/all_to_all | solution.py:68
  79.7 3.5 %all-to-all-start.2 = ((bf16[16,2,256]{2,1,0:T(2,128)(2,1)}), bf16[16,2,256]{2,1,0:T(2,128)(2,1)S(1)}, u32[]{:S(2)}, u32[]{:S(2)}) async-start(bf16[16,2,256]{2,1,0:T(2,128)(2,1)} %reshape.151), calls=%async_computation.2 | async-start | bytes 32768 | tf_op jit(solution)/shard_map/all_to_all | solution.py:70
  83.6 0.7 multiply_reduce_fusion.1
  84.5 6.1 %all-to-all-done.2 = bf16[16,2,256]{2,1,0:T(2,128)(2,1)S(1)} async-done(((bf16[16,2,256]{2,1,0:T(2,128)(2,1)}), bf16[16,2,256]{2,1,0:T(2,128)(2,1)S(1)}, u32[]{:S(2)}, u32[]{:S(2)}) %all-to-all-start.2) | async-done | bytes 16416 | tf_op jit(solution)/shard_map/all_to_all | solution.py:70
  90.6 3.5 %all-to-all-start.3 = ((bf16[16,2,256]{2,1,0:T(2,128)(2,1)}), bf16[16,2,256]{2,1,0:T(2,128)(2,1)S(1)}, u32[]{:S(2)}, u32[]{:S(2)}) async-start(bf16[16,2,256]{2,1,0:T(2,128)(2,1)} %reshape.155), calls=%async_computation.3 | async-start | bytes 32768 | tf_op jit(solution)/shard_map/all_to_all | solution.py:71
  94.3 4.2 %multiply_add_fusion = f32[4,4,256,512]{3,2,1,0:T(8,128)S(1)} fusion(f32[4,4,256,512]{3,2,1,0:T(8,128)} %param.20, f32[4,4,512]{2,1,0:T(4,128)S(1)} %reshape.121, f32[4,4,256]{2,1,0:T(4,128)S(1)} %reshape.120, f32[4,4]{1,0:T(4,128)S(1)} %subtract_exponential_fusion, f32[4,4]{1,0:T(4,128)S(1)} %get-tuple-element.6), kind=kLoop, calls=%fused_computation | loop fusion | flops 8388608 | bytes 16826496 | tf_op jit(solution)/shard_map/add | solution.py:81
  98.5 3.4 %copy-done.1 = f32[4,4,256,512]{3,2,1,0:T(8,128)} copy-done((f32[4,4,256,512]{3,2,1,0:T(8,128)}, f32[4,4,256,512]{3,2,1,0:T(8,128)S(1)}, u32[]{:S(2)}) %copy-start.1) | copy-done | bytes 8388632
  101.9 4.0 %fusion.30 = f32[4,4,1,512]{3,2,1,0:T(1,128)S(1)} fusion(f32[4,4,256,1]{2,3,1,0:T(1,128)S(1)} %reshape.141, f32[4,4,256,512]{3,2,1,0:T(8,128)S(1)} %multiply_add_fusion), kind=kOutput, calls=%fused_computation.57 | convolution fusion | flops 25165824 | bytes 8437760 | tf_op jit(solution)/shard_map/shd,shde->she/dot_general | solution.py:85
  106.1 6.9 %all-to-all-start.5 = ((f32[4,16,1]{0,2,1:T(1,128)}), f32[4,16,1]{0,2,1:T(1,128)S(1)}, u32[]{:S(2)}, u32[]{:S(2)}) async-start(f32[4,16,1]{0,2,1:T(1,128)} %copy.131), calls=%async_computation.5 | async-start | bytes 16384 | tf_op jit(solution)/shard_map/all_to_all | solution.py:109
  113.5 42.4 %all-gather.1 = bf16[16,4,2048]{2,1,0:T(4,128)(2,1)S(1)} all-gather(bf16[1,4,2048]{2,1,0:T(4,128)(2,1)S(1)} %fusion.25), channel_id=1, replica_groups=mesh['ep'=16,'tp'=2] {'ep'}, dimensions={0}, use_global_device_ids=true | all-gather | bytes 278528 | tf_op jit(solution)/shard_map/all_gather | solution.py:92
  155.8 0.8 reshape.135
  156.6 1.2 convolution_convert_fusion.1
  157.9 4.0 %psum.7 = bf16[16,4,256]{2,1,0:T(4,128)(2,1)} all-reduce(bf16[16,4,256]{2,1,0:T(4,128)(2,1)S(1)} %all_to_all.24), channel_id=1, replica_groups=mesh['ep'=16,'tp'=2] {'tp'}, use_global_device_ids=true, to_apply=%region_2.3 | all-reduce | flops 16384 | bytes 65536 | tf_op jit(solution)/shard_map/psum | solution.py:93
  161.9 3.5 %all-to-all-start.4 = ((bf16[16,4,256]{2,1,0:T(4,128)(2,1)}), bf16[16,4,256]{2,1,0:T(4,128)(2,1)S(1)}, u32[]{:S(2)}, u32[]{:S(2)}) async-start(bf16[16,4,256]{2,1,0:T(4,128)(2,1)} %psum.7), calls=%async_computation.4 | async-start | bytes 65536 | tf_op jit(solution)/shard_map/all_to_all | solution.py:94
  165.5 7.3 %all-to-all-done.4 = bf16[16,4,256]{2,1,0:T(4,128)(2,1)S(1)} async-done(((bf16[16,4,256]{2,1,0:T(4,128)(2,1)}), bf16[16,4,256]{2,1,0:T(4,128)(2,1)S(1)}, u32[]{:S(2)}, u32[]{:S(2)}) %all-to-all-start.4) | async-done | bytes 32800 | tf_op jit(solution)/shard_map/all_to_all | solution.py:94
  172.8 0.1 multiply_reduce_fusion
  173.0 39.4 %all-gather.2 = bf16[16,4,4096]{2,1,0:T(4,128)(2,1)S(1)} all-gather(bf16[1,4,4096]{2,1,0:T(4,128)(2,1)S(1)} %fusion.22), channel_id=1, replica_groups=mesh['ep'=16,'tp'=2] {'ep'}, dimensions={0}, use_global_device_ids=true | all-gather | bytes 557056 | tf_op jit(solution)/shard_map/all_gather | solution.py:99
  212.5 2.0 fusion.3
  214.6 3.8 %convolution_convert_fusion = bf16[64,4096]{1,0:T(8,128)(2,1)} fusion(bf16[1,256,4096]{2,1,0:T(8,128)(2,1)S(1)} %copy-done, bf16[64,4096]{1,0:T(8,128)(2,1)S(1)} %reshape.137, bf16[1,4096,256]{2,1,0:T(8,128)(2,1)} %param.34, f32[64,256]{1,0:T(8,128)S(1)} %fusion.3), kind=kOutput, calls=%fused_computation.1 | convolution fusion | flops 268795904 | bytes 5308416 | tf_op jit(solution)/shard_map/dot_general | solution.py:12
  218.4 1.2 convert_multiply_fusion
  219.6 1.9 reshape.118
  221.4 1.9 copy.132
  223.4 1.3 reshape.119
  224.7 46.8 %all-reduce.2 = bf16[128,2048]{1,0:T(8,128)(2,1)S(1)} all-reduce(f32[128,2048]{1,0:T(8,128)} %reshape.119), channel_id=2, replica_groups=mesh['ep'=16,'tp'=2] {'ep','tp'}, use_global_device_ids=true, to_apply=%region_5.6.clone | all-reduce | flops 262144 | bytes 1572864
  271.5 1.8 all_gather.15
  273.4 0.6 add_convert_fusion
  (58 shorter events, 2.5 us)
Async XLA Ops:
  0.6 214.0 %copy-start = (bf16[1,256,4096]{2,1,0:T(8,128)(2,1)S(1)}, bf16[1,256,4096]{2,1,0:T(8,128)(2,1)}, u32[]{:S(2)}) copy-start(bf16[1,256,4096]{2,1,0:T(8,128)(2,1)} %param.35) | copy-start | bytes 6291460
  0.6 83.0 %copy-start.5 = (f32[4,4,256]{2,1,0:T(4,128)S(1)}, f32[4,4,256]{2,1,0:T(4,128)}, u32[]{:S(2)}) copy-start(f32[4,4,256]{2,1,0:T(4,128)} %param.21) | copy-start | bytes 49156
  50.3 15.3 %all-to-all-start.1 = ((bf16[16,2,128]{2,1,0:T(2,128)(2,1)}), bf16[16,2,128]{2,1,0:T(2,128)(2,1)S(1)}, u32[]{:S(2)}, u32[]{:S(2)}) async-start(bf16[16,2,128]{2,1,0:T(2,128)(2,1)} %reshape.153), calls=%async_computation.1 | async-start | bytes 16384 | tf_op jit(solution)/shard_map/all_to_all | solution.py:69
  56.5 42.0 %copy-start.6 = (f32[4,4]{1,0:T(4,128)}, f32[4,4]{1,0:T(4,128)S(1)}, u32[]{:S(2)}) copy-start(f32[4,4]{1,0:T(4,128)S(1)} %get-tuple-element.7) | copy-start | bytes 196
  65.6 14.1 %all-to-all-start = ((bf16[16,2,128]{2,1,0:T(2,128)(2,1)}), bf16[16,2,128]{2,1,0:T(2,128)(2,1)S(1)}, u32[]{:S(2)}, u32[]{:S(2)}) async-start(bf16[16,2,128]{2,1,0:T(2,128)(2,1)} %reshape.149), calls=%async_computation | async-start | bytes 16384 | tf_op jit(solution)/shard_map/all_to_all | solution.py:68
  79.7 10.9 %all-to-all-start.2 = ((bf16[16,2,256]{2,1,0:T(2,128)(2,1)}), bf16[16,2,256]{2,1,0:T(2,128)(2,1)S(1)}, u32[]{:S(2)}, u32[]{:S(2)}) async-start(bf16[16,2,256]{2,1,0:T(2,128)(2,1)} %reshape.151), calls=%async_computation.2 | async-start | bytes 32768 | tf_op jit(solution)/shard_map/all_to_all | solution.py:70
  90.6 15.5 %all-to-all-start.3 = ((bf16[16,2,256]{2,1,0:T(2,128)(2,1)}), bf16[16,2,256]{2,1,0:T(2,128)(2,1)S(1)}, u32[]{:S(2)}, u32[]{:S(2)}) async-start(bf16[16,2,256]{2,1,0:T(2,128)(2,1)} %reshape.155), calls=%async_computation.3 | async-start | bytes 32768 | tf_op jit(solution)/shard_map/all_to_all | solution.py:71
  98.5 3.4 %copy-start.1 = (f32[4,4,256,512]{3,2,1,0:T(8,128)}, f32[4,4,256,512]{3,2,1,0:T(8,128)S(1)}, u32[]{:S(2)}) copy-start(f32[4,4,256,512]{3,2,1,0:T(8,128)S(1)} %multiply_add_fusion) | copy-start | bytes 25165828
  101.9 54.7 %copy-start.3 = (bf16[2048,256]{1,0:T(8,128)(2,1)S(1)}, bf16[2048,256]{1,0:T(8,128)(2,1)}, u32[]{:S(2)}) copy-start(bf16[2048,256]{1,0:T(8,128)(2,1)} %param.31) | copy-start | bytes 3145732
  101.9 70.8 %copy-start.2 = (bf16[4,4096]{1,0:T(4,128)(2,1)S(1)}, bf16[4,4096]{1,0:T(4,128)(2,1)}, u32[]{:S(2)}) copy-start(bf16[4,4096]{1,0:T(4,128)(2,1)} %param.19) | copy-start | bytes 98308
  101.9 71.0 %copy-start.4 = (f32[4096]{0:T(1024)S(1)}, f32[4096]{0:T(1024)}, u32[]{:S(2)}) copy-start(f32[4096]{0:T(1024)} %param.32) | copy-start | bytes 49156
  106.1 55.8 %all-to-all-start.5 = ((f32[4,16,1]{0,2,1:T(1,128)}), f32[4,16,1]{0,2,1:T(1,128)S(1)}, u32[]{:S(2)}, u32[]{:S(2)}) async-start(f32[4,16,1]{0,2,1:T(1,128)} %copy.131), calls=%async_computation.5 | async-start | bytes 16384 | tf_op jit(solution)/shard_map/all_to_all | solution.py:109
  161.9 10.9 %all-to-all-start.4 = ((bf16[16,4,256]{2,1,0:T(4,128)(2,1)}), bf16[16,4,256]{2,1,0:T(4,128)(2,1)S(1)}, u32[]{:S(2)}, u32[]{:S(2)}) async-start(bf16[16,4,256]{2,1,0:T(4,128)(2,1)} %psum.7), calls=%async_computation.4 | async-start | bytes 65536 | tf_op jit(solution)/shard_map/all_to_all | solution.py:94
where the time goes:
time: 275 us; the launch traced here: 274 us
  blocking collectives  180 us (65%)
  starting transfers between devices  27.7 us (10%)
  waiting for transfers between devices  20.3 us (7%)
  matrix products  19 us (7%)
  local copies, waits for them, and re-layouts  15.6 us (6%)
  other arithmetic  10.7 us (4%)
    unnamed x1, blocking collectives  46.8 us
    all_gather x1, blocking collectives, body(): piece = lax.all_gather(normed, 'ep', axis=0, tiled=True)  45.3 us
    all_gather x1, blocking collectives, body(): lax.all_gather(hidden, 'ep', axis=0, tiled=True)  42.4 us
    all_gather x1, blocking collectives, body(): piece = lax.all_gather(ffn_in, 'ep', axis=0, tiled=True)  39.4 us
    dot_general x9, matrix products, product(): return jnp.dot(left, right, preferred_element_type=jnp.float32)  15 us
    unnamed x26, local copies, waits for them, and re-layouts  7.67 us
    all_to_all x1, waiting for transfers between devices, body(): lax.all_to_all(summed, 'ep', split_axis=0, concat_axis=1, tiled=True)  7.25 us
    all_to_all x1, waiting for transfers between devices, body(): lax.all_to_all(query_part, 'ep', split_axis=0, concat_axis=2, tiled=True)  6.95 us
  transfers between devices with their start and end apart: 6, of which 3 were waited for; matrix products, arithmetic and copies ran while one was open for 9% of the time, Pallas kernels for 0%

commit v1 on v0

v1 whole, which is shorter than its diff:
```python
import jax
import jax.numpy as jnp
from jax import lax
from jax.sharding import PartitionSpec as P


def rms_scale(values, gain):
    return values * lax.rsqrt(jnp.mean(values * values, axis=-1, keepdims=True) + 1e-06) * gain


def product(left, right):
    return jnp.dot(left, right, preferred_element_type=jnp.float32)


def to_all(block, n_ep):
    copies = jnp.broadcast_to(block[None], (n_ep,) + block.shape)
    return lax.all_to_all(copies, "ep", split_axis=0, concat_axis=0, tiled=True)


def body(
    tokens,
    memory,
    normalizer,
    stabilizer,
    norm_gain,
    w_query,
    w_key,
    w_value,
    w_outgate,
    w_input,
    w_forget,
    forget_bias,
    w_out,
    ffn_gain,
    w_gate,
    w_up,
    w_down,
    expert_ids,
    route_weights,
):
    n_ep = lax.axis_size("ep")
    n_tp = lax.axis_size("tp")
    me_ep = lax.axis_index("ep")
    me_tp = lax.axis_index("tp")
    seqs, width = tokens.shape
    share = seqs // n_tp
    heads, key_size, value_size = (memory.shape[1], memory.shape[2], memory.shape[3])
    value_width = heads * value_size
    key_piece = w_query.shape[2]
    value_piece = w_value.shape[2]

    tokens_share = lax.dynamic_slice_in_dim(tokens, me_tp * share, share, 0)
    raw_share = to_all(tokens_share, n_ep).reshape(n_ep * share, width)
    raw_share_f32 = raw_share.astype(jnp.float32)
    normed_share = rms_scale(raw_share_f32, norm_gain).astype(jnp.bfloat16)
    normed_all = lax.all_gather(normed_share, "tp", axis=0, tiled=True)

    columns = [w.reshape(width, -1) for w in (w_query, w_key, w_value, w_outgate)]
    projected = jnp.concatenate([product(normed_all, w) for w in columns], axis=1).astype(jnp.bfloat16)
    total = projected.shape[1]
    projected = jnp.swapaxes(projected.reshape(n_tp, n_ep, share, total), 0, 1)
    projected = projected.reshape(n_ep, seqs, total)
    pieces = lax.all_to_all(projected, "ep", split_axis=0, concat_axis=0, tiled=True)

    def heads_of(start, piece):
        part = pieces[:, :, start : start + heads * piece].reshape(n_ep, seqs, heads, piece)
        return jnp.transpose(part, (1, 2, 0, 3)).reshape(seqs, heads, n_ep * piece).astype(jnp.float32)

    narrow = heads * key_piece
    broad = heads * value_piece
    scaled = heads_of(0, key_piece) * key_size ** (-0.5)
    key_heads = heads_of(narrow, key_piece)
    value_heads = heads_of(2 * narrow, value_piece)
    outgate = heads_of(2 * narrow + broad, value_piece)

    normed = rms_scale(tokens.astype(jnp.float32), norm_gain).astype(jnp.bfloat16)
    in_pre = product(normed, w_input)
    log_forget = jax.nn.log_sigmoid(product(normed, w_forget) + forget_bias)
    stab_next = jnp.maximum(log_forget + stabilizer, in_pre)
    decay = jnp.exp(log_forget + stabilizer - stab_next)
    inweight = jnp.exp(in_pre - stab_next)

    normalizer_next = decay[:, :, None] * normalizer + inweight[:, :, None] * key_heads
    denominator = jnp.sum(scaled * normalizer_next, axis=-1)
    along = jnp.sum(scaled * key_heads, axis=-1)
    recalled = jnp.sum(scaled[:, :, :, None] * memory, axis=2)
    numerator = decay[:, :, None] * recalled + (inweight * along)[:, :, None] * value_heads
    hidden = numerator / jnp.maximum(jnp.abs(denominator), jnp.exp(-stab_next))[:, :, None]
    hidden = (hidden * jax.nn.sigmoid(outgate)).reshape(seqs, value_width).astype(jnp.bfloat16)
    memory_next = decay[:, :, None, None] * memory + inweight[:, :, None, None] * (
        key_heads[:, :, :, None] * value_heads[:, :, None, :]
    )

    hidden_all = to_all(hidden, n_ep).reshape(n_ep * seqs, value_width)
    term = product(hidden_all, w_out).astype(jnp.bfloat16).reshape(n_ep, n_tp, share, -1)
    own_term = lax.dynamic_index_in_dim(term, me_tp, 1, keepdims=False)
    mixed = own_term.astype(jnp.float32)
    for step in range(1, n_tp):
        theirs = lax.dynamic_index_in_dim(term, (me_tp + step) % n_tp, 1, keepdims=False)
        shift = [(i, (i + step) % n_tp) for i in range(n_tp)]
        mixed = mixed + lax.ppermute(theirs, "tp", shift).astype(jnp.float32)
    mixed = mixed.astype(jnp.bfloat16).reshape(n_ep * share, -1)
    mixed_share = jnp.swapaxes(to_all(mixed, n_ep), 0, 1).reshape(n_ep * share, width)

    resid_share = raw_share_f32 + mixed_share.astype(jnp.float32)
    ffn_share = rms_scale(resid_share, ffn_gain).astype(jnp.bfloat16)
    ffn_all = lax.all_gather(ffn_share, "tp", axis=0, tiled=True)

    gate_part = product(ffn_all, w_gate[0])
    up_part = product(ffn_all, w_up[0])
    act = (jax.nn.silu(gate_part) * up_part).astype(jnp.bfloat16)
    down_term = product(act, w_down[0]).astype(jnp.bfloat16).reshape(n_tp, n_ep * share, width)
    summed = lax.dynamic_index_in_dim(down_term, me_tp, 0, keepdims=False).astype(jnp.float32)
    for step in range(1, n_tp):
        theirs = lax.dynamic_index_in_dim(down_term, (me_tp + step) % n_tp, 0, keepdims=False)
        shift = [(i, (i + step) % n_tp) for i in range(n_tp)]
        summed = summed + lax.ppermute(theirs, "tp", shift).astype(jnp.float32)
    summed = summed.astype(jnp.bfloat16).reshape(n_ep, share, width)
    by_expert = lax.all_to_all(summed, "ep", split_axis=0, concat_axis=0, tiled=True)

    n_experts = n_ep * w_gate.shape[0]
    labels = jnp.arange(n_experts, dtype=jnp.int32)
    ids = lax.dynamic_slice_in_dim(expert_ids, me_tp * share, share, 0)
    gains = lax.dynamic_slice_in_dim(route_weights, me_tp * share, share, 0)
    route = jnp.sum(jnp.where(ids[:, :, None] == labels[None, None, :], gains[:, :, None], 0.0), axis=1)
    ffn_out = jnp.sum(by_expert.astype(jnp.float32) * jnp.swapaxes(route, 0, 1)[:, :, None], axis=0)
    resid_own = lax.dynamic_slice_in_dim(resid_share, me_ep * share, share, 0)
    out_share = (resid_own + ffn_out).astype(jnp.bfloat16)
    out = lax.all_gather(out_share, "tp", axis=0, tiled=True)
    return (out, memory_next, normalizer_next, stab_next)


def solution(mesh):
    return jax.shard_map(
        body,
        mesh=mesh,
        in_specs=(
            P("ep", None),
            P("ep", "tp", None, None),
            P("ep", "tp", None),
            P("ep", "tp"),
            P(),
            P(None, "tp", "ep"),
            P(None, "tp", "ep"),
            P(None, "tp", "ep"),
            P(None, "tp", "ep"),
            P(None, "tp"),
            P(None, "tp"),
            P("tp"),
            P("tp", "ep"),
            P(),
            P("ep", None, "tp"),
            P("ep", None, "tp"),
            P("ep", "tp", None),
            P("ep", None),
            P("ep", None),
        ),
        out_specs=(P("ep", None), P("ep", "tp", None, None), P("ep", "tp", None), P("ep", "tp")),
        check_vma=False,
    )
```

time: 275 us -> 119 us (0.43)
  blocking collectives: 180 us -> 19.8 us
  waiting for transfers between devices: 20.3 us -> 37 us
  starting transfers between devices: 27.7 us -> 19.2 us
  matrix products: 19 us -> 13.4 us
  other arithmetic: 10.7 us -> 15.6 us
  local copies, waits for them, and re-layouts: 15.6 us -> 11.7 us
    all_gather x4 -> x3, blocking collectives: 129 us -> 6.31 us  [the longest x1 2.31 us: body(): normed_all = lax.all_gather(normed_share, 'tp', axis=0, tiled=True)]
    unnamed x1 -> x0, blocking collectives: 46.8 us -> none
    all_to_all x6 -> x4, waiting for transfers between devices: 20.3 us -> 34.4 us  [the longest x2 17.3 us: to_all(): return lax.all_to_all(copies, 'ep', split_axis=0, concat_axis=0, tiled=True)]
    all_to_all x0 -> x1, blocking collectives: none -> 13.5 us  [to_all(): return lax.all_to_all(copies, 'ep', split_axis=0, concat_axis=0, tiled=True)]
    all_to_all x6 -> x4, starting transfers between devices: 27.7 us -> 19 us  [the longest x2 11.9 us: to_all(): return lax.all_to_all(copies, 'ep', split_axis=0, concat_axis=0, tiled=True)]
    unnamed x26, local copies, waits for them, and re-layouts: 7.67 us -> 0.88 us
    dot_general x1 -> x0, matrix products: 4.04 us -> none  [body(): jnp.einsum('shd,shde->she', scaled, memory_next, precision=lax.Precision....]
    psum x1 -> x0, blocking collectives: 4 us -> none  [body(): summed = lax.psum(rounded_term(partial_value).astype(jnp.bfloat16), 'tp')]
  transfers between devices with their start and end apart: 6 -> 6, of which waited for: 3 -> 6; matrix products, arithmetic and copies ran while one was open for 9% -> 2% of each run, Pallas kernels for 0% -> 0%
where the time goes in v1:
time: 119 us; the launch traced here: 118 us
  waiting for transfers between devices  37 us (31%)
  blocking collectives  19.8 us (17%)
  starting transfers between devices  19.2 us (16%)
  other arithmetic  15.6 us (13%)
  matrix products  13.4 us (11%)
  local copies, waits for them, and re-layouts  11.7 us (10%)
    all_to_all x2, waiting for transfers between devices, to_all(): return lax.all_to_all(copies, 'ep', split_axis=0, concat_axis=0, tiled=True)  17.3 us
    all_to_all x1, blocking collectives, to_all(): return lax.all_to_all(copies, 'ep', split_axis=0, concat_axis=0, tiled=True)  13.5 us
    dot_general x9, matrix products, product(): return jnp.dot(left, right, preferred_element_type=jnp.float32)  13.4 us
    all_to_all x2, starting transfers between devices, to_all(): return lax.all_to_all(copies, 'ep', split_axis=0, concat_axis=0, tiled=True)  11.9 us
    all_to_all x1, waiting for transfers between devices, body(): lax.all_to_all(summed, 'ep', split_axis=0, concat_axis=0, tiled=True)  9.85 us
    add x1, other arithmetic, body(): decay[:, :, None, None] * memory  7.63 us
    all_to_all x1, waiting for transfers between devices, body(): lax.all_to_all(projected, 'ep', split_axis=0, concat_axis=0, tiled=True)  7.28 us
    all_to_all x1, starting transfers between devices, body(): lax.all_to_all(summed, 'ep', split_axis=0, concat_axis=0, tiled=True)  3.55 us
  transfers between devices with their start and end apart: 6, of which 6 were waited for; matrix products, arithmetic and copies ran while one was open for 2% of the time, Pallas kernels for 0%

profile of v1, /device:TPU:0, one launch (start us, length us, event | category | flops | bytes accessed | tf_op | source)
XLA Modules:
  0.0 117.9 jit_solution(10323628438035030262)
XLA Ops:
  0.7 0.9 constant_dynamic-slice_fusion.2
  1.6 0.9 broadcast_in_dim.16
  2.5 8.3 %all-to-all-start = ((bf16[16,2,4096]{2,1,0:T(2,128)(2,1)}), bf16[16,2,4096]{2,1,0:T(2,128)(2,1)S(1)}, u32[]{:S(2)}, u32[]{:S(2)}) async-start(bf16[16,2,4096]{2,1,0:T(2,128)(2,1)} %broadcast_in_dim.16), calls=%async_computation | async-start | bytes 524288 | tf_op jit(solution)/shard_map/all_to_all | solution.py:17
  10.9 0.9 fusion.19
  11.8 0.9 fusion.21
  12.6 8.1 %all-to-all-done = bf16[16,2,4096]{2,1,0:T(2,128)(2,1)S(1)} async-done(((bf16[16,2,4096]{2,1,0:T(2,128)(2,1)}), bf16[16,2,4096]{2,1,0:T(2,128)(2,1)S(1)}, u32[]{:S(2)}, u32[]{:S(2)}) %all-to-all-start) | async-done | bytes 262176 | tf_op jit(solution)/shard_map/all_to_all | solution.py:17
  20.7 0.4 multiply_reduce_fusion.3
  21.3 0.8 multiply_convert_fusion.1
  22.1 2.3 %all_gather.9 = bf16[64,4096]{1,0:T(8,128)(2,1)} all-gather(bf16[32,4096]{1,0:T(8,128)(2,1)S(1)} %multiply_convert_fusion.1), channel_id=1, replica_groups=mesh['ep'=16,'tp'=2] {'tp'}, dimensions={0}, use_global_device_ids=true | all-gather | bytes 786432 | tf_op jit(solution)/shard_map/all_gather | solution.py:56
  24.4 1.4 %dot_general.34 = bf16[2,16,2,4096]{3,2,1,0:T(2,128)(2,1)S(1)} reshape(bf16[64,4096]{1,0:T(8,128)(2,1)} %all_gather.9) | data formatting | bytes 1048576 | tf_op jit(solution)/shard_map/dot_general | solution.py:12
  25.8 1.8 %convolution_convert_fusion.2 = bf16[2,16,2,128]{3,1,2,0:T(8,128)(2,1)S(1)} fusion(bf16[4096,128,1,1]{0,1,3,2:T(8,128)(2,1)} %bitcast.97, bf16[2,16,2,4096]{3,2,1,0:T(2,128)(2,1)S(1)} %dot_general.34), kind=kOutput, calls=%fused_computation.11 | convolution fusion | flops 67117056 | bytes 1589248 | tf_op jit(solution)/shard_map/dot_general | solution.py:12
  27.6 1.8 %convolution_convert_fusion.3 = bf16[2,16,2,128]{3,1,2,0:T(8,128)(2,1)S(1)} fusion(bf16[4096,128,1,1]{0,1,3,2:T(8,128)(2,1)} %bitcast.98, bf16[2,16,2,4096]{3,2,1,0:T(2,128)(2,1)S(1)} %dot_general.34), kind=kOutput, calls=%fused_computation.12 | convolution fusion | flops 67117056 | bytes 1589248 | tf_op jit(solution)/shard_map/dot_general | solution.py:12
  29.4 1.5 %convolution_convert_fusion.4 = bf16[2,16,2,64]{3,1,2,0:T(8,128)(2,1)S(1)} fusion(bf16[4096,64,1,1]{0,1,3,2:T(8,128)(2,1)} %bitcast.106, bf16[2,16,2,4096]{3,2,1,0:T(2,128)(2,1)S(1)} %dot_general.34), kind=kOutput, calls=%fused_computation.13 | convolution fusion | flops 33558528 | bytes 1056768 | tf_op jit(solution)/shard_map/dot_general | solution.py:12
  30.9 1.5 %convolution_convert_fusion.5 = bf16[2,16,2,64]{3,1,2,0:T(8,128)(2,1)S(1)} fusion(bf16[4096,64,1,1]{0,1,3,2:T(8,128)(2,1)} %bitcast.107, bf16[2,16,2,4096]{3,2,1,0:T(2,128)(2,1)S(1)} %dot_general.34), kind=kOutput, calls=%fused_computation.14 | convolution fusion | flops 33558528 | bytes 1056768 | tf_op jit(solution)/shard_map/dot_general | solution.py:12
  32.5 0.6 copy.124
  33.2 3.5 %all-to-all-start.1 = ((bf16[16,4,384]{2,1,0:T(4,128)(2,1)}), bf16[16,4,384]{2,1,0:T(4,128)(2,1)S(1)}, u32[]{:S(2)}, u32[]{:S(2)}) async-start(bf16[16,4,384]{2,1,0:T(4,128)(2,1)} %copy.124), calls=%async_computation.1 | async-start | bytes 98304 | tf_op jit(solution)/shard_map/all_to_all | solution.py:63
  36.8 0.2 fusion.32
  36.9 7.3 %all-to-all-done.1 = bf16[16,4,384]{2,1,0:T(4,128)(2,1)S(1)} async-done(((bf16[16,4,384]{2,1,0:T(4,128)(2,1)}), bf16[16,4,384]{2,1,0:T(4,128)(2,1)S(1)}, u32[]{:S(2)}, u32[]{:S(2)}) %all-to-all-start.1) | async-done | bytes 49184 | tf_op jit(solution)/shard_map/all_to_all | solution.py:63
  44.6 0.1 mul.221
  44.8 0.1 reshape.233
  45.0 0.1 multiply_reduce_fusion.4
  45.1 0.1 fusion.34
  45.3 0.1 mul.223
  45.6 7.6 %multiply_add_fusion = (f32[4,4,256,512]{3,2,1,0:T(8,128)}, f32[4,4,512]{2,1,0:T(4,128)S(1)}) fusion(f32[4,4,256,512]{3,2,1,0:T(8,128)} %param.20, f32[4,4,512]{2,1,0:T(4,128)S(1)} %reshape.230, f32[4,4,256]{2,1,0:T(4,128)S(1)} %reshape.222, f32[4,4]{1,0:T(4,128)S(1)} %get-tuple-element.7, f32[4,4]{1,0:T(4,128)S(1)} %subtract_exponential_fusion.1, ...), kind=kLoop, calls=%fused_computation | loop fusion | flops 12574720 | bytes 16875648 | tf_op jit(solution)/shard_map/add | solution.py:90
  53.4 0.7 multiply_reduce_fusion.5
  54.4 0.1 reshape.225
  54.6 0.8 broadcast_in_dim.17
  55.4 3.5 %all-to-all-start.2 = ((bf16[16,4,2048]{2,1,0:T(4,128)(2,1)}), bf16[16,4,2048]{2,1,0:T(4,128)(2,1)S(1)}, u32[]{:S(2)}, u32[]{:S(2)}) async-start(bf16[16,4,2048]{2,1,0:T(4,128)(2,1)} %broadcast_in_dim.17), calls=%async_computation.2 | async-start | bytes 524288 | tf_op jit(solution)/shard_map/all_to_all | solution.py:17
  58.9 9.2 %all-to-all-done.2 = bf16[16,4,2048]{2,1,0:T(4,128)(2,1)S(1)} async-done(((bf16[16,4,2048]{2,1,0:T(4,128)(2,1)}), bf16[16,4,2048]{2,1,0:T(4,128)(2,1)S(1)}, u32[]{:S(2)}, u32[]{:S(2)}) %all-to-all-start.2) | async-done | bytes 262176 | tf_op jit(solution)/shard_map/all_to_all | solution.py:17
  68.1 1.5 %convolution_convert_fusion.1 = bf16[64,256]{1,0:T(8,128)(2,1)S(1)} fusion(bf16[64,2048]{1,0:T(8,128)(2,1)S(1)} %reshape.216, bf16[2048,256]{1,0:T(8,128)(2,1)} %param.31), kind=kOutput, calls=%fused_computation.10 | convolution fusion | flops 67125248 | bytes 1343488 | tf_op jit(solution)/shard_map/dot_general | solution.py:12
  69.8 1.2 collective-permute-done
  71.0 13.5 %all_to_all.25 = bf16[16,32,256]{2,1,0:T(8,128)(2,1)S(1)} all-to-all(bf16[16,32,256]{2,1,0:T(8,128)(2,1)S(1)} %broadcast_in_dim.19), channel_id=1, replica_groups=mesh['ep'=16,'tp'=2] {'ep'}, dimensions={0} | all-to-all | bytes 524288 | tf_op jit(solution)/shard_map/all_to_all | solution.py:17
  84.6 1.1 copy.131
  85.7 2.2 %reshape.228 = f32[16,2,4096]{2,1,0:T(2,128)} reshape(f32[32,16,256]{2,1,0:T(8,128)} %copy.131) | data formatting | bytes 1048576 | tf_op jit(solution)/shard_map/convert_element_type | solution.py:105
  87.9 1.5 %multiply_reduce_fusion.2 = f32[16,2]{1,0:T(8,128)S(1)} fusion(f32[16,2,4096]{2,1,0:T(2,128)} %reshape.228, bf16[16,2,4096]{2,1,0:T(2,128)(2,1)S(1)} %all-to-all-done), kind=kLoop, calls=%fused_computation.23 | loop fusion | flops 524256 | bytes 786560 | tf_op jit(solution)/shard_map/reduce_sum | solution.py:8
  89.6 0.9 multiply_convert_fusion
  90.4 2.2 %all_gather.10 = bf16[64,4096]{1,0:T(8,128)(2,1)S(1)} all-gather(bf16[32,4096]{1,0:T(8,128)(2,1)S(1)} %get-tuple-element.4), channel_id=1, replica_groups=mesh['ep'=16,'tp'=2] {'tp'}, dimensions={0}, use_global_device_ids=true | all-gather | bytes 786432 | tf_op jit(solution)/shard_map/all_gather | solution.py:107
  92.6 2.0 %fusion.3 = f32[64,256]{1,0:T(8,128)S(1)} fusion(bf16[64,4096]{1,0:T(8,128)(2,1)S(1)} %all_gather.10, bf16[1,4096,256]{2,1,0:T(8,128)(2,1)} %param.33), kind=kOutput, calls=%fused_computation.6 | convolution fusion | flops 134217728 | bytes 2686976 | tf_op jit(solution)/shard_map/dot_general | solution.py:12
  94.7 3.0 %convolution_convert_fusion = bf16[64,4096]{1,0:T(8,128)(2,1)S(1)} fusion(bf16[1,256,4096]{2,1,0:T(8,128)(2,1)S(1)} %copy-done, bf16[64,4096]{1,0:T(8,128)(2,1)S(1)} %all_gather.10, bf16[1,4096,256]{2,1,0:T(8,128)(2,1)} %param.34, f32[64,256]{1,0:T(8,128)S(1)} %fusion.3), kind=kOutput, calls=%fused_computation.2 | convolution fusion | flops 268795904 | bytes 5308416 | tf_op jit(solution)/shard_map/dot_general | solution.py:12
  97.7 0.2 collective-permute-start.1
  97.9 1.4 %collective-permute-done.1 = bf16[32,4096]{1,0:T(8,128)(2,1)S(1)} collective-permute-done((bf16[32,4096]{1,0:T(8,128)(2,1)S(1)}, bf16[32,4096]{1,0:T(8,128)(2,1)S(1)}, u32[]{:S(2)}, u32[]{:S(2)}) %collective-permute-start.1) | collective-permute-done | bytes 262176 | tf_op jit(solution)/shard_map/ppermute | solution.py:117
  99.4 0.9 reshape.219
  100.2 3.5 %all-to-all-start.4 = ((bf16[16,2,4096]{2,1,0:T(2,128)(2,1)}), bf16[16,2,4096]{2,1,0:T(2,128)(2,1)S(1)}, u32[]{:S(2)}, u32[]{:S(2)}) async-start(bf16[16,2,4096]{2,1,0:T(2,128)(2,1)} %reshape.219), calls=%async_computation.4 | async-start | bytes 524288 | tf_op jit(solution)/shard_map/all_to_all | solution.py:119
  104.3 9.8 %all-to-all-done.4 = bf16[16,2,4096]{2,1,0:T(2,128)(2,1)S(1)} async-done(((bf16[16,2,4096]{2,1,0:T(2,128)(2,1)}), bf16[16,2,4096]{2,1,0:T(2,128)(2,1)S(1)}, u32[]{:S(2)}, u32[]{:S(2)}) %all-to-all-start.4) | async-done | bytes 262176 | tf_op jit(solution)/shard_map/all_to_all | solution.py:119
  114.2 0.3 multiply_reduce_fusion.1
  114.5 0.9 fusion.29
  115.4 1.8 %all-gather = bf16[2,2,4096]{2,1,0:T(2,128)(2,1)S(1)} all-gather(bf16[1,2,4096]{2,1,0:T(2,128)(2,1)S(1)} %fusion.29), channel_id=1, replica_groups=mesh['ep'=16,'tp'=2] {'tp'}, dimensions={0}, use_global_device_ids=true | all-gather | bytes 49152 | tf_op jit(solution)/shard_map/all_gather | solution.py:129
  117.3 0.6 reshape.240
  (67 shorter events, 2.5 us)
Async XLA Ops:
  0.6 94.0 %copy-start = (bf16[1,256,4096]{2,1,0:T(8,128)(2,1)S(1)}, bf16[1,256,4096]{2,1,0:T(8,128)(2,1)}, u32[]{:S(2)}) copy-start(bf16[1,256,4096]{2,1,0:T(8,128)(2,1)} %param.35) | copy-start | bytes 6291460
  0.6 36.1 %copy-start.8 = (f32[4,4]{1,0:T(4,128)S(1)}, f32[4,4]{1,0:T(4,128)}, u32[]{:S(2)}) copy-start(f32[4,4]{1,0:T(4,128)} %param.22) | copy-start | bytes 196
  0.7 36.1 %copy-start.6 = (bf16[4096,4]{0,1:T(4,128)(2,1)S(1)}, bf16[4096,4]{0,1:T(4,128)(2,1)}, u32[]{:S(2)}) copy-start(bf16[4096,4]{0,1:T(4,128)(2,1)} %param.29) | copy-start | bytes 98308
  0.7 36.1 %copy-start.9 = (f32[4]{0:T(128)S(1)}, f32[4]{0:T(128)}, u32[]{:S(2)}) copy-start(f32[4]{0:T(128)} %param.30) | copy-start | bytes 52
  0.7 44.4 %copy-start.7 = (bf16[4096,4]{0,1:T(4,128)(2,1)S(1)}, bf16[4096,4]{0,1:T(4,128)(2,1)}, u32[]{:S(2)}) copy-start(bf16[4096,4]{0,1:T(4,128)(2,1)} %param.28) | copy-start | bytes 98308
  2.5 18.2 %all-to-all-start = ((bf16[16,2,4096]{2,1,0:T(2,128)(2,1)}), bf16[16,2,4096]{2,1,0:T(2,128)(2,1)S(1)}, u32[]{:S(2)}, u32[]{:S(2)}) async-start(bf16[16,2,4096]{2,1,0:T(2,128)(2,1)} %broadcast_in_dim.16), calls=%async_computation | async-start | bytes 524288 | tf_op jit(solution)/shard_map/all_to_all | solution.py:17
  33.2 11.0 %all-to-all-start.1 = ((bf16[16,4,384]{2,1,0:T(4,128)(2,1)}), bf16[16,4,384]{2,1,0:T(4,128)(2,1)S(1)}, u32[]{:S(2)}, u32[]{:S(2)}) async-start(bf16[16,4,384]{2,1,0:T(4,128)(2,1)} %copy.124), calls=%async_computation.1 | async-start | bytes 98304 | tf_op jit(solution)/shard_map/all_to_all | solution.py:63
  45.2 8.8 %copy-start.3 = (f32[4,4]{1,0:T(4,128)}, f32[4,4]{1,0:T(4,128)S(1)}, u32[]{:S(2)}) copy-start(f32[4,4]{1,0:T(4,128)S(1)} %get-tuple-element.8) | copy-start | bytes 196
  45.6 7.7 %copy-start.2 = (f32[4,4,256]{2,1,0:T(4,128)S(1)}, f32[4,4,256]{2,1,0:T(4,128)}, u32[]{:S(2)}) copy-start(f32[4,4,256]{2,1,0:T(4,128)} %param.21) | copy-start | bytes 49156
  53.2 36.3 %copy-start.1 = (f32[4096]{0:T(1024)S(1)}, f32[4096]{0:T(1024)}, u32[]{:S(2)}) copy-start(f32[4096]{0:T(1024)} %param.32) | copy-start | bytes 49156
  55.4 12.7 %all-to-all-start.2 = ((bf16[16,4,2048]{2,1,0:T(4,128)(2,1)}), bf16[16,4,2048]{2,1,0:T(4,128)(2,1)S(1)}, u32[]{:S(2)}, u32[]{:S(2)}) async-start(bf16[16,4,2048]{2,1,0:T(4,128)(2,1)} %broadcast_in_dim.17), calls=%async_computation.2 | async-start | bytes 524288 | tf_op jit(solution)/shard_map/all_to_all | solution.py:17
  69.7 1.2 %collective-permute-start = (bf16[16,2,256]{2,1,0:T(2,128)(2,1)S(1)}, bf16[16,2,256]{2,1,0:T(2,128)(2,1)S(1)}, u32[]{:S(2)}, u32[]{:S(2)}) collective-permute-start(bf16[16,2,256]{2,1,0:T(2,128)(2,1)S(1)} %dynamic-slice_bitcast_fusion.1), channel_id=1, source_target_pairs={{0,1},{1,0},{2,3},{3,2},{4,5},{5,4},{6,7},{7,6},{8,9},{9,8},{10,11... | collective-permute-start | bytes 49160 | tf_op jit(solution)/shard_map/ppermute | solution.py:101
  84.6 19.2 %copy-start.4 = (s32[4,2]{0,1:T(2,128)S(1)}, s32[4,2]{0,1:T(2,128)}, u32[]{:S(2)}) copy-start(s32[4,2]{0,1:T(2,128)} %param.36) | copy-start | bytes 100
  84.6 19.3 %copy-start.5 = (f32[4,2]{0,1:T(2,128)S(1)}, f32[4,2]{0,1:T(2,128)}, u32[]{:S(2)}) copy-start(f32[4,2]{0,1:T(2,128)} %param.37) | copy-start | bytes 100
  97.7 1.6 %collective-permute-start.1 = (bf16[32,4096]{1,0:T(8,128)(2,1)S(1)}, bf16[32,4096]{1,0:T(8,128)(2,1)S(1)}, u32[]{:S(2)}, u32[]{:S(2)}) collective-permute-start(bf16[32,4096]{1,0:T(8,128)(2,1)S(1)} %dynamic-slice_bitcast_fusion), channel_id=1, source_target_pairs={{0,1},{1,0},{2,3},{3,2},{4,5},{5,4},{6,7},{7,6},{8,9},{9,8},{10,11... | collective-permute-start | bytes 786440 | tf_op jit(solution)/shard_map/ppermute | solution.py:117
  100.2 13.9 %all-to-all-start.4 = ((bf16[16,2,4096]{2,1,0:T(2,128)(2,1)}), bf16[16,2,4096]{2,1,0:T(2,128)(2,1)S(1)}, u32[]{:S(2)}, u32[]{:S(2)}) async-start(bf16[16,2,4096]{2,1,0:T(2,128)(2,1)} %reshape.219), calls=%async_computation.4 | async-start | bytes 524288 | tf_op jit(solution)/shard_map/all_to_all | solution.py:119

commit v2 on v1

v2 whole, which is shorter than its diff:
```python
import functools

import jax
import jax.numpy as jnp
from jax import lax
from jax.experimental import pallas as pl
from jax.experimental.pallas import tpu as pltpu
from jax.sharding import PartitionSpec as P

F32 = jnp.float32
BF16 = jnp.bfloat16
ANY = pl.BlockSpec(memory_space=pl.ANY)
HBM = pl.BlockSpec(memory_space=pltpu.HBM)
VMEM = pl.BlockSpec(memory_space=pltpu.VMEM)


def rms_scale(values, gain):
    return values * lax.rsqrt(jnp.mean(values * values, axis=-1, keepdims=True) + 1e-06) * gain


def product(left, right):
    return jnp.dot(left, right, preferred_element_type=F32)


def product_t(left, right):
    return lax.dot_general(left, right, (((1,), (1,)), ((), ())), preferred_element_type=F32)


def to_all(copies):
    return lax.all_to_all(copies, "ep", split_axis=0, concat_axis=0, tiled=True)


def call(kernel, out_shape, in_specs, scratch, args, name, kib=24576, flops=10**6, nbytes=10**6, outs=None):
    many = isinstance(out_shape, tuple)
    args = [pltpu.with_memory_space_constraint(a, pltpu.HBM) if s is HBM else a for a, s in zip(args, in_specs)]
    return pl.pallas_call(
        kernel,
        out_shape=out_shape,
        in_specs=in_specs,
        out_specs=outs or (tuple(VMEM for _ in out_shape) if many else VMEM),
        scratch_shapes=scratch,
        name=name,
        compiler_params=pltpu.CompilerParams(vmem_limit_bytes=kib << 10),
        cost_estimate=pl.CostEstimate(flops=flops, transcendentals=0, bytes_accessed=nbytes),
    )(*args)


def shape(dims, dtype):
    return jax.ShapeDtypeStruct(dims, dtype)


def project_kernel(own, other, gain, wq, wk, wv, wo, out, weights, normed, sems, *, seqs):
    starts, copies = 0, []
    for n, w in enumerate((wq, wk, wv, wo)):
        rows = w.shape[0]
        copies.append(pltpu.make_async_copy(w, weights.at[pl.ds(starts, rows)], sems.at[n]))
        copies[-1].start()
        starts += rows
    half = own.shape[0]
    scale = gain[...]
    normed[0:half] = rms_scale(own[...].astype(F32), scale).astype(BF16)
    normed[half:] = rms_scale(other[...].astype(F32), scale).astype(BF16)
    front = starts - wo.shape[0]
    for c in copies[:3]:
        c.wait()
    left = product_t(normed[...], weights[0:front]).astype(BF16)
    copies[3].wait()
    right = product_t(normed[...], weights[front:starts]).astype(BF16)
    rows = 2 * half
    share = seqs // 2
    me = lax.axis_index("tp")
    r = lax.broadcasted_iota(jnp.int32, (rows, rows), 0)
    c = lax.broadcasted_iota(jnp.int32, (rows, rows), 1)
    token = r % seqs
    which = (token // share + me) % 2
    pick = (c == which * half + (r // seqs) * share + token % share).astype(BF16)
    left = product(pick, left)
    right = product(pick, right)
    for d in range(rows // seqs):
        out[d, :, 0:front] = left[d * seqs : (d + 1) * seqs].astype(BF16)
        out[d, :, front:starts] = right[d * seqs : (d + 1) * seqs].astype(BF16)


def readout_kernel(query, key, value, outgate, decay, inweight, floor, norm, memory, out, norm_out, buf, recalled, sems):
    seqs, heads, dk, dv = memory.shape
    copies = []
    for i in range(seqs):
        for h in range(heads):
            n = i * heads + h
            copies.append(pltpu.make_async_copy(memory.at[i, h], buf.at[n], sems.at[n]))
            copies[-1].start()
    columns = query[...].T
    for n, c in enumerate(copies):
        c.wait()
        i, h = divmod(n, heads)
        part = jnp.sum(buf[n] * columns[:, n : n + 1], axis=0, keepdims=True)
        recalled[i : i + 1, h * dv : (h + 1) * dv] = part
    for h in range(heads):
        rows = [i * heads + h for i in range(seqs)]
        q = jnp.concatenate([query[n : n + 1] for n in rows], axis=0)
        k = jnp.concatenate([key[n : n + 1] for n in rows], axis=0)
        old = jnp.concatenate([norm[n : n + 1] for n in rows], axis=0)
        d = decay[:, h : h + 1]
        w = inweight[:, h : h + 1]
        new = d * old + w * k
        for i, n in enumerate(rows):
            norm_out[n : n + 1] = new[i : i + 1]
        below = jnp.maximum(jnp.abs(jnp.sum(q * new, axis=1, keepdims=True)), floor[:, h : h + 1])
        along = w * jnp.sum(q * k, axis=1, keepdims=True)
        at = slice(h * dv, (h + 1) * dv)
        top = d * recalled[:, at] + along * value[:, at]
        hidden = (top / below * jax.nn.sigmoid(outgate[:, at])).astype(BF16)
        for e in range(out.shape[0]):
            out[e, :, at] = hidden


def update_kernel(key, value, decay, inweight, after, memory, out, token, buf, sems, out_sems):
    token[...] = jnp.zeros(token.shape, F32)
    seqs, heads, dk, dv = memory.shape
    copies, backs = [], []
    for i in range(seqs):
        for h in range(heads):
            n = i * heads + h
            copies.append(pltpu.make_async_copy(memory.at[i, h], buf.at[n], sems.at[n]))
            copies[-1].start()
    columns = key[...].T
    for n, c in enumerate(copies):
        c.wait()
        i, h = divmod(n, heads)
        d = decay[i : i + 1, h : h + 1]
        w = inweight[i : i + 1, h : h + 1]
        row = value[i : i + 1, h * dv : (h + 1) * dv] * w
        buf[n] = d * buf[n] + columns[:, n : n + 1] * row
        backs.append(pltpu.make_async_copy(buf.at[n], out.at[i, h], out_sems.at[n]))
        backs[-1].start()
    for b in backs:
        b.wait()


def output_kernel(hidden, token, w_out, own, other, weights, sems, *, seqs):
    parts = sems.shape[0]
    rows = w_out.shape[0] // parts
    copies = []
    for n in range(parts):
        at = pl.ds(n * rows, rows)
        copies.append(pltpu.make_async_copy(w_out.at[at], weights.at[at], sems.at[n]))
        copies[-1].start()
    total = None
    for n, c in enumerate(copies):
        c.wait()
        part = product(hidden[:, n * rows : (n + 1) * rows], weights[n * rows : (n + 1) * rows])
        total = part if total is None else total + part
    term = total.astype(BF16)
    half, share = own.shape[0], seqs // 2
    me = lax.axis_index("tp")
    r = lax.broadcasted_iota(jnp.int32, (half, 2 * half), 0)
    c = lax.broadcasted_iota(jnp.int32, (half, 2 * half), 1)
    at = (r // share) * seqs + r % share
    own[...] = product((c == at + me * share).astype(BF16), term).astype(BF16)
    other[...] = product((c == at + (1 - me) * share).astype(BF16), term).astype(BF16)


def resid_kernel(raw, mixed, gain, ffn, mine, resid):
    members, rows, cols = mixed.shape
    group = max(1, 128 // cols)
    total = None
    for n in range(0, members, group):
        part = jnp.concatenate([mixed[n + g] for g in range(group)], axis=1) if group > 1 else mixed[n]
        at = slice(n * cols, (n + group) * cols)
        block = raw[:, at].astype(F32) + part.astype(F32)
        resid[:, at] = block
        squares = jnp.sum(block * block, axis=1, keepdims=True)
        total = squares if total is None else total + squares
    scale = lax.rsqrt(total / (members * cols) + 1e-06)
    ffn[...] = (resid[...] * scale * gain[...]).astype(BF16)
    share = mine.shape[0]
    me = lax.axis_index("ep")
    for j in range(share):
        mine[j : j + 1] = resid[pl.ds(me * share + j, 1)]


def expert_kernel(own, other, w_gate, w_up, w_down, out_own, out_other, gate, up, down, sems):
    parts = sems.shape[1]
    copies = [[], [], []]
    for n in range(parts):
        for k, (w, buf) in enumerate(((w_gate, gate), (w_up, up))):
            rows = w.shape[1] // parts
            at = pl.ds(n * rows, rows)
            copies[k].append(pltpu.make_async_copy(w.at[0, at], buf.at[at], sems.at[k, n]))
            copies[k][-1].start()
    width = w_down.shape[2] // parts
    for n in range(parts):
        at = pl.ds(n * width, width)
        copies[2].append(pltpu.make_async_copy(w_down.at[0, :, at], down.at[:, at], sems.at[2, n]))
        copies[2][-1].start()
    rows = w_gate.shape[1] // parts
    gate_sum = up_sum = None
    for n in range(parts):
        at = slice(n * rows, (n + 1) * rows)
        left = jnp.concatenate([own[:, at], other[:, at]], axis=0)
        copies[0][n].wait()
        part = product(left, gate[at])
        gate_sum = part if gate_sum is None else gate_sum + part
        copies[1][n].wait()
        part = product(left, up[at])
        up_sum = part if up_sum is None else up_sum + part
    act = (jax.nn.silu(gate_sum) * up_sum).astype(BF16)
    half = own.shape[0]
    for n in range(parts):
        at = slice(n * width, (n + 1) * width)
        copies[2][n].wait()
        term = product(act, down[:, at]).astype(BF16)
        out_own[:, at] = term[0:half]
        out_other[:, at] = term[half:]


def join_kernel(own, other, out):
    share = out.shape[1]
    both = own[...].astype(F32) + other[...].astype(F32)
    for e in range(out.shape[0]):
        out[e] = both[e * share : (e + 1) * share].astype(BF16)


def share_kernel(tokens, out):
    share = out.shape[1]
    me = lax.axis_index("tp")
    values = tokens[...].astype(F32)
    mine = jnp.where(me == 0, values[0:share], values[share:]).astype(BF16)
    for e in range(out.shape[0]):
        out[e] = mine


def gates_kernel(tokens, gain, w_in, w_forget, bias, stab, stab_out, decay, inweight, floor):
    normed = rms_scale(tokens[...].astype(F32), gain[...]).astype(BF16)
    in_pre = product_t(normed, w_in[...])
    old = jax.nn.log_sigmoid(product_t(normed, w_forget[...]) + bias[...]) + stab[...]
    new = jnp.maximum(old, in_pre)
    stab_out[...] = new
    decay[...] = jnp.exp(old - new)
    inweight[...] = jnp.exp(in_pre - new)
    floor[...] = jnp.exp(-new)


def body(
    tokens,
    memory,
    normalizer,
    stabilizer,
    norm_gain,
    w_query,
    w_key,
    w_value,
    w_outgate,
    w_input,
    w_forget,
    forget_bias,
    w_out,
    ffn_gain,
    w_gate,
    w_up,
    w_down,
    expert_ids,
    route_weights,
):
    n_ep = lax.axis_size("ep")
    n_tp = lax.axis_size("tp")
    assert n_tp == 2
    me_tp = lax.axis_index("tp")
    swap = [(0, 1), (1, 0)]
    seqs, width = tokens.shape
    share = seqs // n_tp
    half = n_ep * share
    heads, key_size, value_size = (memory.shape[1], memory.shape[2], memory.shape[3])
    value_width = heads * value_size
    key_piece = w_query.shape[2]
    value_piece = w_value.shape[2]
    narrow = heads * key_piece
    broad = heads * value_piece
    total = 2 * narrow + 2 * broad

    copies = call(share_kernel, shape((n_ep, share, width), BF16), [VMEM], [], [tokens], "share")
    raw_own = to_all(copies).reshape(half, width)
    raw_other = lax.ppermute(raw_own, "tp", swap)

    columns = [jnp.transpose(w, (1, 2, 0)).reshape(-1, width) for w in (w_query, w_key, w_value, w_outgate)]
    projected = call(
        functools.partial(project_kernel, seqs=seqs),
        shape((n_ep, seqs, total), BF16),
        [VMEM, VMEM, VMEM, HBM, HBM, HBM, HBM],
        [pltpu.VMEM((total, width), BF16), pltpu.VMEM((2 * half, width), BF16), pltpu.SemaphoreType.DMA((4,))],
        [raw_own, raw_other, norm_gain.reshape(1, width), *columns],
        "project",
        flops=2 * 2 * half * total * width,
    )
    pieces = to_all(projected)

    def rows_of(start, piece):
        part = pieces[:, :, start : start + heads * piece].reshape(n_ep, seqs, heads, piece)
        return jnp.transpose(part, (1, 2, 0, 3)).astype(F32)

    query = (rows_of(0, key_piece) * key_size ** (-0.5)).reshape(seqs * heads, key_size)
    key = rows_of(narrow, key_piece).reshape(seqs * heads, key_size)
    value = rows_of(2 * narrow, value_piece).reshape(seqs, value_width)
    outgate = rows_of(2 * narrow + broad, value_piece).reshape(seqs, value_width)

    stab_next, decay, inweight, floor = call(
        gates_kernel,
        (shape((seqs, heads), F32),) * 4,
        [VMEM] * 6,
        [],
        [tokens, norm_gain.reshape(1, width), w_input.T, w_forget.T, forget_bias.reshape(1, heads), stabilizer],
        "gates",
    )

    n_cells = seqs * heads
    hidden, norm_next = call(
        readout_kernel,
        (shape((n_ep, seqs, value_width), BF16), shape((n_cells, key_size), F32)),
        [VMEM] * 8 + [HBM],
        [
            pltpu.VMEM((n_cells, key_size, value_size), F32),
            pltpu.VMEM((seqs, value_width), F32),
            pltpu.SemaphoreType.DMA((n_cells,)),
        ],
        [query, key, value, outgate, decay, inweight, floor, normalizer.reshape(n_cells, key_size), memory],
        "readout",
        flops=2 * memory.size,
    )
    hidden_all = to_all(hidden).reshape(n_ep * seqs, value_width)
    memory_next, token = call(
        update_kernel,
        (shape(memory.shape, F32), shape((8, 128), F32)),
        [VMEM] * 4 + [ANY, HBM],
        [
            pltpu.VMEM((n_cells, key_size, value_size), F32),
            pltpu.SemaphoreType.DMA((n_cells,)),
            pltpu.SemaphoreType.DMA((n_cells,)),
        ],
        [key, value, decay, inweight, norm_next, memory],
        "update",
        flops=10**8,
        outs=(HBM, VMEM),
    )

    own_term, other_term = call(
        functools.partial(output_kernel, seqs=seqs),
        (shape((half, w_out.shape[1]), BF16),) * 2,
        [VMEM, ANY, HBM],
        [pltpu.VMEM(w_out.shape, BF16), pltpu.SemaphoreType.DMA((4,))],
        [hidden_all, token, w_out],
        "output",
        flops=2 * n_ep * seqs * w_out.size,
    )
    mixed = (own_term.astype(F32) + lax.ppermute(other_term, "tp", swap).astype(F32)).astype(BF16)
    mixed_all = to_all(jnp.broadcast_to(mixed[None], (n_ep,) + mixed.shape))

    ffn_own, resid_mine = call(
        resid_kernel,
        (shape((half, width), BF16), shape((share, width), F32)),
        [VMEM] * 3,
        [pltpu.VMEM((half, width), F32)],
        [raw_own, mixed_all, ffn_gain.reshape(1, width)],
        "resid",
    )
    ffn_other = lax.ppermute(ffn_own, "tp", swap)
    units = w_gate.shape[2]
    down_own, down_other = call(
        expert_kernel,
        (shape((half, width), BF16),) * 2,
        [VMEM, VMEM, HBM, HBM, HBM],
        [
            pltpu.VMEM((width, units), BF16),
            pltpu.VMEM((width, units), BF16),
            pltpu.VMEM((units, width), BF16),
            pltpu.SemaphoreType.DMA((3, 4)),
        ],
        [ffn_own, ffn_other, w_gate, w_up, w_down],
        "experts",
        flops=2 * 3 * 2 * half * width * units,
    )
    summed = call(
        join_kernel,
        shape((n_ep, share, width), BF16),
        [VMEM] * 2,
        [],
        [down_own, lax.ppermute(down_other, "tp", swap)],
        "join",
    )
    by_expert = to_all(summed)

    n_experts = n_ep * w_gate.shape[0]
    labels = jnp.arange(n_experts, dtype=jnp.int32)
    ids = lax.dynamic_slice_in_dim(expert_ids, me_tp * share, share, 0)
    gains = lax.dynamic_slice_in_dim(route_weights, me_tp * share, share, 0)
    route = jnp.sum(jnp.where(ids[:, :, None] == labels[None, None, :], gains[:, :, None], 0.0), axis=1)
    ffn_out = jnp.sum(by_expert.astype(F32) * jnp.swapaxes(route, 0, 1)[:, :, None], axis=0)
    out_mine = (resid_mine + ffn_out).astype(BF16)
    out_other = lax.ppermute(out_mine, "tp", swap)
    first = jnp.where(me_tp == 0, out_mine, out_other)
    last = jnp.where(me_tp == 0, out_other, out_mine)
    out = jnp.concatenate([first, last], axis=0)
    return (out, memory_next, norm_next.reshape(normalizer.shape), stab_next)


def solution(mesh):
    return jax.shard_map(
        body,
        mesh=mesh,
        in_specs=(
            P("ep", None),
            P("ep", "tp", None, None),
            P("ep", "tp", None),
            P("ep", "tp"),
            P(),
            P(None, "tp", "ep"),
            P(None, "tp", "ep"),
            P(None, "tp", "ep"),
            P(None, "tp", "ep"),
            P(None, "tp"),
            P(None, "tp"),
            P("tp"),
            P("tp", "ep"),
            P(),
            P("ep", None, "tp"),
            P("ep", None, "tp"),
            P("ep", "tp", None),
            P("ep", None),
            P("ep", None),
        ),
        out_specs=(P("ep", None), P("ep", "tp", None, None), P("ep", "tp", None), P("ep", "tp")),
        check_vma=False,
    )
```

time: 119 us -> 98 us (0.82)
  Pallas kernels: 0 us -> 22.8 us
  other arithmetic: 15.6 us -> 1.25 us
  matrix products: 13.4 us -> 0 us
  blocking collectives: 19.8 us -> 32.4 us
  waiting for transfers between devices: 37 us -> 24.9 us
  starting transfers between devices: 19.2 us -> 11.1 us
  local copies, waits for them, and re-layouts: 11.7 us -> 3.88 us
    pallas_call x0 -> x9, Pallas kernels: none -> 22.8 us  [call(): pl.pallas_call(kernel, out_shape=out_shape, in_specs=in_specs, out_specs=...]
    all_to_all x1 -> x2, blocking collectives: 13.5 us -> 32.4 us  [to_all(): return lax.all_to_all(copies, 'ep', split_axis=0, concat_axis=0, tiled=True)]
    all_to_all x2 -> x0, waiting for transfers between devices: 17.1 us -> none  [the longest x1 9.85 us: body(): lax.all_to_all(summed, 'ep', split_axis=0, concat_axis=0, tiled=True)]
    dot_general x9 -> x0, matrix products: 13.4 us -> none  [product(): return jnp.dot(left, right, preferred_element_type=jnp.float32)]
    add x1 -> x0, other arithmetic: 7.63 us -> none  [body(): decay[:, :, None, None] * memory]
    all_to_all x2 -> x0, starting transfers between devices: 7.09 us -> none  [the longest x1 3.55 us: body(): lax.all_to_all(summed, 'ep', split_axis=0, concat_axis=0, tiled=True)]
    all_gather x3 -> x0, blocking collectives: 6.31 us -> none  [the longest x1 2.31 us: body(): normed_all = lax.all_gather(normed_share, 'tp', axis=0, tiled=True)]
    convert_element_type x11 -> x0, local copies, waits for them, and re-layouts: 4.04 us -> none  [the longest x3 3.32 us: body(): resid_share = raw_share_f32 + mixed_share.astype(jnp.float32)]
  transfers between devices with their start and end apart: 6 -> 8, of which waited for: 6 -> 8; matrix products, arithmetic and copies ran while one was open for 2% -> 1% of each run, Pallas kernels for 0% -> 8%
where the time goes in v2:
time: 98 us; the launch traced here: 97.4 us
  blocking collectives  32.4 us (33%)
  waiting for transfers between devices  24.9 us (25%)
  Pallas kernels  22.8 us (23%)
  starting transfers between devices  11.1 us (11%)
  local copies, waits for them, and re-layouts  3.88 us (4%)
  other arithmetic  1.25 us (1%)
  between operations  1 us (1%)
    all_to_all x2, blocking collectives, to_all(): return lax.all_to_all(copies, 'ep', split_axis=0, concat_axis=0, tiled=True)  32.4 us
    pallas_call x9, Pallas kernels, call(): pl.pallas_call(kernel, out_shape=out_shape, in_specs=in_specs, out_specs=...  22.8 us
    all_to_all x3, waiting for transfers between devices, to_all(): return lax.all_to_all(copies, 'ep', split_axis=0, concat_axis=0, tiled=True)  18.8 us
    all_to_all x3, starting transfers between devices, to_all(): return lax.all_to_all(copies, 'ep', split_axis=0, concat_axis=0, tiled=True)  10.6 us
  transfers between devices with their start and end apart: 8, of which 8 were waited for; matrix products, arithmetic and copies ran while one was open for 1% of the time, Pallas kernels for 8%

profile of v2, /device:TPU:0, one launch (start us, length us, event | category | flops | bytes accessed | tf_op | source)
XLA Modules:
  0.0 97.4 jit_solution(16016032374105159432)
XLA Ops:
  0.7 0.8 copy-done.1
  1.4 18.0 %all_to_all.25 = bf16[16,2,4096]{2,1,0:T(2,128)(2,1)S(1)} all-to-all(bf16[16,2,4096]{2,1,0:T(2,128)(2,1)S(1)} %share.1), channel_id=1, replica_groups=mesh['ep'=16,'tp'=2] {'ep'}, dimensions={0} | all-to-all | bytes 524288 | tf_op jit(solution)/shard_map/all_to_all | solution.py:30
  19.5 0.1 reshape.77.own.raw
  19.6 0.1 collective-permute-start
  19.7 1.5 %collective-permute-done.other = bf16[32,4096]{1,0:T(8,128)(2,1)S(1)} collective-permute-done((bf16[32,4096]{1,0:T(8,128)(2,1)S(1)}, bf16[32,4096]{1,0:T(8,128)(2,1)S(1)}, u32[]{:S(2)}, u32[]{:S(2)}) %collective-permute-start) | collective-permute-done | bytes 262176 | tf_op jit(solution)/shard_map/ppermute | solution.py:283
  21.2 0.7 copy-done.3
  21.9 4.1 %project.1 = bf16[16,4,384]{2,1,0:T(4,128)(2,1)} custom-call(bf16[32,4096]{1,0:T(8,128)(2,1)S(1)} %reshape.77.own.raw, bf16[32,4096]{1,0:T(8,128)(2,1)S(1)} %collective-permute-done.other, f32[1,4096]{1,0:T(1,128)S(1)} %bitcast.38, bf16[64,4096]{1,0:T(8,128)(2,1)} %bitcast.46, bf16[64,4096]{1,0:T(8,128)(2,1)} %bitcast.47, bf16[128,4096]{1,0:T(8,128)(2,1)} %bitcast.44, ...), custom_call_target="tpu_custom_call" | custom-call | flops 201326592 | bytes 1000000 | tf_op jit(solution)/shard_map/project/pallas_call | solution.py:36
  26.0 3.6 %all-to-all-start.1 = ((bf16[16,4,384]{2,1,0:T(4,128)(2,1)}), bf16[16,4,384]{2,1,0:T(4,128)(2,1)S(1)}, u32[]{:S(2)}, u32[]{:S(2)}) async-start(bf16[16,4,384]{2,1,0:T(4,128)(2,1)} %project.1), calls=%async_computation.1 | async-start | bytes 98304 | tf_op jit(solution)/shard_map/all_to_all | solution.py:30
  29.7 1.0 gates.1
  30.6 6.4 %all-to-all-done.1 = bf16[16,4,384]{2,1,0:T(4,128)(2,1)S(1)} async-done(((bf16[16,4,384]{2,1,0:T(4,128)(2,1)}), bf16[16,4,384]{2,1,0:T(4,128)(2,1)S(1)}, u32[]{:S(2)}, u32[]{:S(2)}) %all-to-all-start.1) | async-done | bytes 49184 | tf_op jit(solution)/shard_map/all_to_all | solution.py:30
  37.1 0.1 mul.26
  37.2 0.1 reshape.83.query
  37.3 0.1 slice_convert_fusion.2
  37.4 0.1 reshape.105
  37.6 0.1 reshape.96.key
  37.7 0.1 reshape.107
  37.9 0.1 reshape.98.value
  38.0 0.1 reshape.109
  38.2 0.1 reshape.100.outgate
  38.3 4.5 %readout.1 = (bf16[16,4,2048]{2,1,0:T(4,128)(2,1)}, f32[16,256]{1,0:T(8,128)S(1)}) custom-call(f32[16,256]{1,0:T(8,128)S(1)} %reshape.83.query, f32[16,256]{1,0:T(8,128)S(1)} %reshape.96.key, f32[4,2048]{1,0:T(4,128)S(1)} %reshape.98.value, f32[4,2048]{1,0:T(4,128)S(1)} %reshape.100.outgate, f32[4,4]{1,0:T(4,128)S(1)} %get-tuple-element.18.decay, ...), custom_call_target="tpu_custom_call" | custom-call | flops 4194304 | bytes 1000000 | tf_op jit(solution)/shard_map/readout/pallas_call | solution.py:36
  42.9 3.5 %all-to-all-start.2 = ((bf16[16,4,2048]{2,1,0:T(4,128)(2,1)}), bf16[16,4,2048]{2,1,0:T(4,128)(2,1)S(1)}, u32[]{:S(2)}, u32[]{:S(2)}) async-start(bf16[16,4,2048]{2,1,0:T(4,128)(2,1)} %get-tuple-element.21), calls=%async_computation.2 | async-start | bytes 524288 | tf_op jit(solution)/shard_map/all_to_all | solution.py:30
  46.4 6.7 %update.1 = (f32[4,4,256,512]{3,2,1,0:T(8,128)}, f32[8,128]{1,0:T(8,128)S(1)}) custom-call(f32[16,256]{1,0:T(8,128)S(1)} %reshape.96.key, f32[4,2048]{1,0:T(4,128)S(1)} %reshape.98.value, f32[4,4]{1,0:T(4,128)S(1)} %get-tuple-element.18.decay, f32[4,4]{1,0:T(4,128)S(1)} %get-tuple-element.19.inweight, f32[16,256]{1,0:T(8,128)S(1)} %get-tuple-element.22.after, ...), custom_call_target="tpu_custom_call" | custom-call | flops 100000000 | bytes 1000000 | tf_op jit(solution)/shard_map/update/pallas_call | solution.py:36
  53.1 2.5 %all-to-all-done.2 = bf16[16,4,2048]{2,1,0:T(4,128)(2,1)S(1)} async-done(((bf16[16,4,2048]{2,1,0:T(4,128)(2,1)}), bf16[16,4,2048]{2,1,0:T(4,128)(2,1)S(1)}, u32[]{:S(2)}, u32[]{:S(2)}) %all-to-all-start.2) | async-done | bytes 262176 | tf_op jit(solution)/shard_map/all_to_all | solution.py:30
  55.6 0.1 reshape.92.hidden
  55.6 1.8 %output.1 = (bf16[32,256]{1,0:T(8,128)(2,1)S(1)}, bf16[32,256]{1,0:T(8,128)(2,1)S(1)}) custom-call(bf16[64,2048]{1,0:T(8,128)(2,1)S(1)} %reshape.92.hidden, f32[8,128]{1,0:T(8,128)S(1)} %get-tuple-element.23.token, bf16[2048,256]{1,0:T(8,128)(2,1)} %w_out.1), custom_call_target="tpu_custom_call" | custom-call | flops 67108864 | bytes 1000000 | tf_op jit(solution)/shard_map/output/pallas_call | solution.py:36
  57.4 0.1 collective-permute-start.1
  57.5 1.2 %collective-permute-done.1 = bf16[32,256]{1,0:T(8,128)(2,1)S(1)} collective-permute-done((bf16[32,256]{1,0:T(8,128)(2,1)S(1)}, bf16[32,256]{1,0:T(8,128)(2,1)S(1)}, u32[]{:S(2)}, u32[]{:S(2)}) %collective-permute-start.1) | collective-permute-done | bytes 16416 | tf_op jit(solution)/shard_map/ppermute | solution.py:354
  58.7 14.4 %all_to_all.26.mixed = bf16[16,32,256]{2,1,0:T(8,128)(2,1)S(1)} all-to-all(bf16[16,32,256]{2,1,0:T(8,128)(2,1)S(1)} %broadcast_in_dim.10), channel_id=1, replica_groups=mesh['ep'=16,'tp'=2] {'ep'}, dimensions={0} | all-to-all | bytes 524288 | tf_op jit(solution)/shard_map/all_to_all | solution.py:30
  73.1 0.2 resid.1
  73.3 0.1 collective-permute-start.2
  73.4 1.5 %collective-permute-done.2.other = bf16[32,4096]{1,0:T(8,128)(2,1)S(1)} collective-permute-done((bf16[32,4096]{1,0:T(8,128)(2,1)S(1)}, bf16[32,4096]{1,0:T(8,128)(2,1)S(1)}, u32[]{:S(2)}, u32[]{:S(2)}) %collective-permute-start.2) | collective-permute-done | bytes 262176 | tf_op jit(solution)/shard_map/ppermute | solution.py:365
  74.9 3.8 %experts.1 = (bf16[32,4096]{1,0:T(8,128)(2,1)S(1)}, bf16[32,4096]{1,0:T(8,128)(2,1)S(1)}) custom-call(bf16[32,4096]{1,0:T(8,128)(2,1)S(1)} %get-tuple-element.27.own, bf16[32,4096]{1,0:T(8,128)(2,1)S(1)} %collective-permute-done.2.other, bf16[1,4096,256]{2,1,0:T(8,128)(2,1)} %w_gate.1, bf16[1,4096,256]{2,1,0:T(8,128)(2,1)} %w_up.1, bf16[1,256,4096]{2,1,0:T(8,128)(2,1)} %w_down.1), custom_call_target="tpu_custom_call" | custom-call | flops 402653184 | bytes 1000000 | tf_op jit(solution)/shard_map/experts/pallas_call | solution.py:36
  78.8 0.2 collective-permute-start.3
  79.0 1.4 %collective-permute-done.3.other = bf16[32,4096]{1,0:T(8,128)(2,1)S(1)} collective-permute-done((bf16[32,4096]{1,0:T(8,128)(2,1)S(1)}, bf16[32,4096]{1,0:T(8,128)(2,1)S(1)}, u32[]{:S(2)}, u32[]{:S(2)}) %collective-permute-start.3) | collective-permute-done | bytes 262176 | tf_op jit(solution)/shard_map/ppermute | solution.py:386
  80.4 0.8 join.1
  81.2 3.5 %all-to-all-start.4 = ((bf16[16,2,4096]{2,1,0:T(2,128)(2,1)}), bf16[16,2,4096]{2,1,0:T(2,128)(2,1)S(1)}, u32[]{:S(2)}, u32[]{:S(2)}) async-start(bf16[16,2,4096]{2,1,0:T(2,128)(2,1)} %join.1), calls=%async_computation.4 | async-start | bytes 524288 | tf_op jit(solution)/shard_map/all_to_all | solution.py:30
  84.7 0.1 constant_dynamic-slice_fusion
  84.8 0.1 copy.34
  84.9 0.1 constant_dynamic-slice_fusion.1
  85.0 0.1 copy.33
  85.1 0.1 fusion
  85.2 0.1 copy.35
  85.2 9.8 %all-to-all-done.4 = bf16[16,2,4096]{2,1,0:T(2,128)(2,1)S(1)} async-done(((bf16[16,2,4096]{2,1,0:T(2,128)(2,1)}), bf16[16,2,4096]{2,1,0:T(2,128)(2,1)S(1)}, u32[]{:S(2)}, u32[]{:S(2)}) %all-to-all-start.4) | async-done | bytes 262176 | tf_op jit(solution)/shard_map/all_to_all | solution.py:30
  95.1 0.3 multiply_reduce_fusion
  95.5 0.1 collective-permute-start.4
  95.5 0.6 reshape.94
  96.2 0.6 collective-permute-done.4
  96.7 0.7 pad_maximum_fusion
  (34 shorter events, 0.4 us)
Async XLA Ops:
  0.6 84.1 %copy-start = (f32[4,2]{0,1:T(2,128)S(1)}, f32[4,2]{0,1:T(2,128)}, u32[]{:S(2)}) copy-start(f32[4,2]{0,1:T(2,128)} %param.37) | copy-start | bytes 100
  0.6 0.8 copy-start.1
  19.5 10.1 %copy-start.10 = (f32[4,4,256]{2,1,0:T(4,128)S(1)}, f32[4,4,256]{2,1,0:T(4,128)}, u32[]{:S(2)}) copy-start(f32[4,4,256]{2,1,0:T(4,128)} %param.21) | copy-start | bytes 49156
  19.5 10.1 %copy-start.2 = (bf16[4,4096]{1,0:T(4,128)(2,1)S(1)}, bf16[4,4096]{1,0:T(4,128)(2,1)}, u32[]{:S(2)}) copy-start(bf16[4,4096]{1,0:T(4,128)(2,1)} %tokens.3) | copy-start | bytes 98308
  19.5 10.1 %copy-start.4 = (f32[4096]{0:T(1024)S(1)}, f32[4096]{0:T(1024)}, u32[]{:S(2)}) copy-start(f32[4096]{0:T(1024)} %param.23) | copy-start | bytes 49156
  19.5 10.2 %copy-start.5 = (bf16[4096,4]{0,1:T(4,128)(2,1)S(1)}, bf16[4096,4]{0,1:T(4,128)(2,1)}, u32[]{:S(2)}) copy-start(bf16[4096,4]{0,1:T(4,128)(2,1)} %param.28) | copy-start | bytes 98308
  19.5 10.2 %copy-start.6 = (bf16[4096,4]{0,1:T(4,128)(2,1)S(1)}, bf16[4096,4]{0,1:T(4,128)(2,1)}, u32[]{:S(2)}) copy-start(bf16[4096,4]{0,1:T(4,128)(2,1)} %param.29) | copy-start | bytes 98308
  19.5 10.2 %copy-start.8 = (f32[4,4]{1,0:T(4,128)S(1)}, f32[4,4]{1,0:T(4,128)}, u32[]{:S(2)}) copy-start(f32[4,4]{1,0:T(4,128)} %stab.1) | copy-start | bytes 196
  19.5 10.2 %copy-start.9 = (f32[4]{0:T(128)S(1)}, f32[4]{0:T(128)}, u32[]{:S(2)}) copy-start(f32[4]{0:T(128)} %param.30) | copy-start | bytes 52
  19.6 1.6 %collective-permute-start = (bf16[32,4096]{1,0:T(8,128)(2,1)S(1)}, bf16[32,4096]{1,0:T(8,128)(2,1)S(1)}, u32[]{:S(2)}, u32[]{:S(2)}) collective-permute-start(bf16[32,4096]{1,0:T(8,128)(2,1)S(1)} %reshape.77.own.raw), channel_id=1, source_target_pairs={{0,1},{1,0},{2,3},{3,2},{4,5},{5,4},{6,7},{7,6},{8,9},{9,8},{10,11... | collective-permute-start | bytes 786440 | tf_op jit(solution)/shard_map/ppermute | solution.py:283
  21.2 0.7 copy-start.3
  26.0 11.0 %all-to-all-start.1 = ((bf16[16,4,384]{2,1,0:T(4,128)(2,1)}), bf16[16,4,384]{2,1,0:T(4,128)(2,1)S(1)}, u32[]{:S(2)}, u32[]{:S(2)}) async-start(bf16[16,4,384]{2,1,0:T(4,128)(2,1)} %project.1), calls=%async_computation.1 | async-start | bytes 98304 | tf_op jit(solution)/shard_map/all_to_all | solution.py:30
  42.9 12.7 %all-to-all-start.2 = ((bf16[16,4,2048]{2,1,0:T(4,128)(2,1)}), bf16[16,4,2048]{2,1,0:T(4,128)(2,1)S(1)}, u32[]{:S(2)}, u32[]{:S(2)}) async-start(bf16[16,4,2048]{2,1,0:T(4,128)(2,1)} %get-tuple-element.21), calls=%async_computation.2 | async-start | bytes 524288 | tf_op jit(solution)/shard_map/all_to_all | solution.py:30
  53.1 20.0 %copy-start.7 = (f32[4096]{0:T(1024)S(1)}, f32[4096]{0:T(1024)}, u32[]{:S(2)}) copy-start(f32[4096]{0:T(1024)} %param.32) | copy-start | bytes 49156
  57.4 1.2 %collective-permute-start.1 = (bf16[32,256]{1,0:T(8,128)(2,1)S(1)}, bf16[32,256]{1,0:T(8,128)(2,1)S(1)}, u32[]{:S(2)}, u32[]{:S(2)}) collective-permute-start(bf16[32,256]{1,0:T(8,128)(2,1)S(1)} %get-tuple-element.25), channel_id=1, source_target_pairs={{0,1},{1,0},{2,3},{3,2},{4,5},{5,4},{6,7},{7,6},{8,9},{9,8},{10,11... | collective-permute-start | bytes 49160 | tf_op jit(solution)/shard_map/ppermute | solution.py:354
  73.3 11.6 %copy-start.11 = (s32[4,2]{0,1:T(2,128)S(1)}, s32[4,2]{0,1:T(2,128)}, u32[]{:S(2)}) copy-start(s32[4,2]{0,1:T(2,128)} %param.36) | copy-start | bytes 100
  73.3 1.6 %collective-permute-start.2 = (bf16[32,4096]{1,0:T(8,128)(2,1)S(1)}, bf16[32,4096]{1,0:T(8,128)(2,1)S(1)}, u32[]{:S(2)}, u32[]{:S(2)}) collective-permute-start(bf16[32,4096]{1,0:T(8,128)(2,1)S(1)} %get-tuple-element.27.own), channel_id=1, source_target_pairs={{0,1},{1,0},{2,3},{3,2},{4,5},{5,4},{6,7},{7,6},{8,9},{9,8},{10,11... | collective-permute-start | bytes 786440 | tf_op jit(solution)/shard_map/ppermute | solution.py:365
  78.8 1.6 %collective-permute-start.3 = (bf16[32,4096]{1,0:T(8,128)(2,1)S(1)}, bf16[32,4096]{1,0:T(8,128)(2,1)S(1)}, u32[]{:S(2)}, u32[]{:S(2)}) collective-permute-start(bf16[32,4096]{1,0:T(8,128)(2,1)S(1)} %get-tuple-element.29), channel_id=1, source_target_pairs={{0,1},{1,0},{2,3},{3,2},{4,5},{5,4},{6,7},{7,6},{8,9},{9,8},{10,11... | collective-permute-start | bytes 786440 | tf_op jit(solution)/shard_map/ppermute | solution.py:386
  81.2 13.9 %all-to-all-start.4 = ((bf16[16,2,4096]{2,1,0:T(2,128)(2,1)}), bf16[16,2,4096]{2,1,0:T(2,128)(2,1)S(1)}, u32[]{:S(2)}, u32[]{:S(2)}) async-start(bf16[16,2,4096]{2,1,0:T(2,128)(2,1)} %join.1), calls=%async_computation.4 | async-start | bytes 524288 | tf_op jit(solution)/shard_map/all_to_all | solution.py:30
  95.5 1.2 %collective-permute-start.4 = (bf16[2,4096]{1,0:T(2,128)(2,1)S(1)}, bf16[2,4096]{1,0:T(2,128)(2,1)S(1)}, u32[]{:S(2)}, u32[]{:S(2)}) collective-permute-start(bf16[2,4096]{1,0:T(2,128)(2,1)S(1)} %add_convert_fusion), channel_id=1, source_target_pairs={{0,1},{1,0},{2,3},{3,2},{4,5},{5,4},{6,7},{7,6},{8,9},{9,8},{10,11... | collective-permute-start | bytes 49160 | tf_op jit(solution)/shard_map/ppermute | solution.py:398

commit v3 on v2

v3 whole, which is shorter than its diff:
```python
import functools

import jax
import jax.numpy as jnp
from jax import lax
from jax.experimental import pallas as pl
from jax.experimental.pallas import tpu as pltpu
from jax.sharding import PartitionSpec as P

F32 = jnp.float32
BF16 = jnp.bfloat16
ANY = pl.BlockSpec(memory_space=pl.ANY)
HBM = pl.BlockSpec(memory_space=pltpu.HBM)
VMEM = pl.BlockSpec(memory_space=pltpu.VMEM)
FAST = pl.BlockSpec(memory_space=pltpu.VMEM)


def rms_scale(values, gain):
    return values * lax.rsqrt(jnp.mean(values * values, axis=-1, keepdims=True) + 1e-06) * gain


def product(left, right):
    return jnp.dot(left, right, preferred_element_type=F32)


def product_t(left, right):
    return lax.dot_general(left, right, (((1,), (1,)), ((), ())), preferred_element_type=F32)


def to_all(copies):
    return lax.all_to_all(copies, "ep", split_axis=0, concat_axis=0, tiled=True)


def call(kernel, out_shape, in_specs, scratch, args, name, flops=10**6, outs=None):
    many = isinstance(out_shape, tuple)
    outs = outs or (tuple(VMEM for _ in out_shape) if many else VMEM)
    pins = {id(HBM): pltpu.HBM, id(FAST): pltpu.VMEM}
    args = [pltpu.with_memory_space_constraint(a, pins[id(s)]) if id(s) in pins else a for a, s in zip(args, in_specs)]
    return pl.pallas_call(
        kernel,
        out_shape=out_shape,
        in_specs=in_specs,
        out_specs=outs,
        scratch_shapes=scratch,
        name=name,
        compiler_params=pltpu.CompilerParams(vmem_limit_bytes=24 << 20),
        cost_estimate=pl.CostEstimate(flops=flops, transcendentals=0, bytes_accessed=10**6),
    )(*args)


def shape(dims, dtype):
    return jax.ShapeDtypeStruct(dims, dtype)


def fetch(pairs, sems):
    copies = [pltpu.make_async_copy(src, dst, sems.at[n]) for n, (src, dst) in enumerate(pairs)]
    for c in copies:
        c.start()
    return copies


def front_kernel(own, gain, wq, wk, wv, gain_out, weights, normed, sems):
    pairs, at = [(gain, gain_out)], 0
    for w in (wq, wk, wv):
        pairs.append((w, weights.at[pl.ds(at, w.shape[0])]))
        at += w.shape[0]
    copies = fetch(pairs, sems)
    copies[0].wait()
    normed[...] = rms_scale(own[...].astype(F32), gain_out[...]).astype(BF16)
    for c in copies[1:]:
        c.wait()


def recall_kernel(after, memory, out, sems):
    heads = memory.shape[1]
    for c in fetch([(memory.at[n // heads, n % heads], out.at[n]) for n in range(out.shape[0])], sems):
        c.wait()


def units_kernel(after, w_gate, w_up, out, sems):
    rows, units = out.shape[0] // 2, out.shape[1] // 2
    pairs = []
    for n in range(2):
        at = pl.ds(n * rows, rows)
        pairs.append((w_gate.at[0, at], out.at[at, pl.ds(0, units)]))
        pairs.append((w_up.at[0, at], out.at[at, pl.ds(units, units)]))
    for c in fetch(pairs, sems):
        c.wait()


def expert_kernel(own, other, near, w_gate, w_up, w_down, act_own, down, out, far, sems, down_sems):
    done, units = near.shape[0], w_gate.shape[2]
    parts = sems.shape[0] // 2
    rows = far.shape[0] // parts
    pairs = []
    for n in range(parts):
        src, dst = pl.ds(done + n * rows, rows), pl.ds(n * rows, rows)
        pairs.append((w_gate.at[0, src], far.at[dst, pl.ds(0, units)]))
        pairs.append((w_up.at[0, src], far.at[dst, pl.ds(units, units)]))
    copies = fetch(pairs, sems)
    slabs = down_sems.shape[0]
    width = w_down.shape[2] // slabs
    at = [pl.ds(n * width, width) for n in range(slabs)]
    downs = fetch([(w_down.at[0, :, a], down.at[:, a]) for a in at], down_sems)

    def left(start, stop):
        return jnp.concatenate([own[:, start:stop], other[:, start:stop]], axis=0)

    total = product(left(0, done), near[...])
    for n in range(parts):
        copies[2 * n].wait()
        copies[2 * n + 1].wait()
        start = done + n * rows
        total = total + product(left(start, start + rows), far[n * rows : (n + 1) * rows])
    act = (jax.nn.silu(total[:, 0:units]) * total[:, units:]).astype(BF16)
    half = own.shape[0]
    act_own[...] = act[0:half]
    for n in range(slabs):
        downs[n].wait()
        at = slice(n * width, (n + 1) * width)
        out[:, at] = product(act[half:], down[:, at]).astype(BF16)


def down_kernel(act, down, out):
    out[...] = product(act[...], down[...]).astype(BF16)


def project_kernel(own, other, gain, front, wo, out, back, normed, sems, *, seqs):
    (copy,) = fetch([(wo, back)], sems)
    half = other.shape[0]
    normed[0:half] = own[...]
    normed[half:] = rms_scale(other[...].astype(F32), gain[...]).astype(BF16)
    left = product_t(front[...], normed[...]).astype(BF16)
    copy.wait()
    right = product_t(back[...], normed[...]).astype(BF16)
    rows = 2 * half
    share = seqs // 2
    me = lax.axis_index("tp")
    r = lax.broadcasted_iota(jnp.int32, (rows, rows), 0)
    c = lax.broadcasted_iota(jnp.int32, (rows, rows), 1)
    token = r % seqs
    which = (token // share + me) % 2
    pick = (c == which * half + (r // seqs) * share + token % share).astype(BF16)
    left = product_t(pick, left)
    right = product_t(pick, right)
    cut = front.shape[0]
    for d in range(rows // seqs):
        out[d, :, 0:cut] = left[d * seqs : (d + 1) * seqs].astype(BF16)
        out[d, :, cut:] = right[d * seqs : (d + 1) * seqs].astype(BF16)


def spread(pieces, start, piece, blocks, seqs):
    rows, total = pieces.shape
    members = rows // seqs
    low = start // 128 * 128
    high = min(total, -(-(start + blocks * piece) // 128) * 128)
    entries = members * piece
    wide = blocks * entries
    d = lax.broadcasted_iota(jnp.int32, (1, wide), 1)
    target = start - low + (d // entries) * piece + d % piece
    column = lax.broadcasted_iota(jnp.int32, (high - low, wide), 0)
    placed = product(pieces[:, low:high], jnp.where(column == target, 1.0, 0.0).astype(BF16))
    member = (d % entries) // piece
    r = lax.broadcasted_iota(jnp.int32, (rows, wide), 0) // seqs
    placed = jnp.where(r == member, placed, 0.0).astype(BF16)
    t = lax.broadcasted_iota(jnp.int32, (8, rows), 0)
    gather = jnp.where(lax.broadcasted_iota(jnp.int32, (8, rows), 1) % seqs == t, 1.0, 0.0)
    return product(gather.astype(BF16), placed)


def readout_kernel(
    pieces,
    decay,
    inweight,
    floor,
    norm,
    first,
    memory,
    out,
    norm_out,
    key_out,
    value_out,
    buf,
    recalled,
    hidden,
    sems,
    out_sems,
    *,
    piece,
):
    seqs, heads, dk, dv = memory.shape
    near = first.shape[0]
    cells = [(n // heads, n % heads) for n in range(seqs * heads)]
    copies = fetch([(memory.at[i, h], buf.at[n]) for n, (i, h) in enumerate(cells[near:])], sems)
    rows = jnp.concatenate([pieces[m].astype(F32) for m in range(pieces.shape[0])], axis=0).astype(BF16)
    small, large = piece
    narrow = spread(rows, 0, small, 2 * heads, seqs)
    key_at = heads * dk
    query = [narrow[:, h * dk : (h + 1) * dk] * dk ** (-0.5) for h in range(heads)]
    key = [narrow[:, key_at + h * dk : key_at + (h + 1) * dk] for h in range(heads)]
    columns = jnp.concatenate(query, axis=0).T

    def recall(cell, i, h):
        n = h * 8 + i
        part = jnp.sum(cell * columns[:, n : n + 1], axis=0, keepdims=True)
        recalled[i : i + 1, h * dv : (h + 1) * dv] = part

    for n, (i, h) in enumerate(cells[:near]):
        recall(first[n], i, h)
    value = spread(rows, 2 * heads * small, large, heads, seqs)[0:seqs]
    outgate = spread(rows, 2 * heads * small + heads * large, large, heads, seqs)[0:seqs]
    value_out[...] = value
    below, along = [], []
    for h in range(heads):
        key_out[h * 8 : (h + 1) * 8] = key[h]
        q, k = query[h][0:seqs], key[h][0:seqs]
        old = jnp.concatenate([norm[i, h : h + 1] for i in range(seqs)], axis=0)
        w = inweight[:, h : h + 1]
        new = decay[:, h : h + 1] * old + w * k
        for i in range(seqs):
            norm_out[i, h : h + 1] = new[i : i + 1]
        below.append(jnp.maximum(jnp.abs(jnp.sum(q * new, axis=1, keepdims=True)), floor[:, h : h + 1]))
        along.append(w * jnp.sum(q * k, axis=1, keepdims=True))
    gate = jax.nn.sigmoid(outgate)
    for n, (i, h) in enumerate(cells[near:]):
        copies[n].wait()
        recall(buf[n], i, h)
    for h in range(heads):
        at = slice(h * dv, (h + 1) * dv)
        top = decay[:, h : h + 1] * recalled[:, at] + along[h] * value[:, at]
        hidden[:, at] = (top / below[h] * gate[:, at]).astype(BF16)
    for c in fetch([(hidden, out.at[e]) for e in range(out.shape[0])], out_sems):
        c.wait()


def update_kernel(key, value, decay, inweight, w_out, memory, out, w_copy, buf, sems, out_sems, w_sems):
    seqs, heads, dk, dv = memory.shape
    cells = [(i, h) for i in range(seqs) for h in range(heads)]
    copies = fetch([(memory.at[i, h], buf.at[n]) for n, (i, h) in enumerate(cells)], sems)
    extra = fetch([(w_out, w_copy)], w_sems)
    backs = []
    columns = key[...].T
    for n, (i, h) in enumerate(cells):
        copies[n].wait()
        d = decay[i : i + 1, h : h + 1]
        row = value[i : i + 1, h * dv : (h + 1) * dv] * inweight[i : i + 1, h : h + 1]
        at = h * 8 + i
        buf[n] = d * buf[n] + columns[:, at : at + 1] * row
        backs.append(pltpu.make_async_copy(buf.at[n], out.at[i, h], out_sems.at[n]))
        backs[-1].start()
    for c in extra + backs:
        c.wait()


def output_kernel(hidden, w_out, own, other, *, seqs):
    total = product(hidden[...], w_out[...])
    term = total.astype(BF16)
    half, share = own.shape[0], seqs // 2
    me = lax.axis_index("tp")
    r = lax.broadcasted_iota(jnp.int32, (half, 2 * half), 0)
    c = lax.broadcasted_iota(jnp.int32, (half, 2 * half), 1)
    at = (r // share) * seqs + r % share
    own[...] = product((c == at + me * share).astype(BF16), term).astype(BF16)
    other[...] = product((c == at + (1 - me) * share).astype(BF16), term).astype(BF16)


def resid_kernel(raw, mixed, gain, ffn, mine, resid):
    members, rows, cols = mixed.shape
    group = max(1, 128 // cols)
    total = None
    for n in range(0, members, group):
        part = jnp.concatenate([mixed[n + g] for g in range(group)], axis=1) if group > 1 else mixed[n]
        at = slice(n * cols, (n + group) * cols)
        block = raw[:, at].astype(F32) + part.astype(F32)
        resid[:, at] = block
        squares = jnp.sum(block * block, axis=1, keepdims=True)
        total = squares if total is None else total + squares
    scale = lax.rsqrt(total / (members * cols) + 1e-06)
    ffn[...] = (resid[...] * scale * gain[...]).astype(BF16)
    share = mine.shape[0]
    me = lax.axis_index("ep")
    for j in range(share):
        mine[j : j + 1] = resid[pl.ds(me * share + j, 1)]


def join_kernel(own, other, out):
    share = out.shape[1]
    both = own[...].astype(F32) + other[...].astype(F32)
    for e in range(out.shape[0]):
        out[e] = both[e * share : (e + 1) * share].astype(BF16)


def share_kernel(tokens, out):
    share = out.shape[1]
    me = lax.axis_index("tp")
    values = tokens[...].astype(F32)
    mine = jnp.where(me == 0, values[0:share], values[share:]).astype(BF16)
    for e in range(out.shape[0]):
        out[e] = mine


def gates_kernel(tokens, gain, w_in, w_forget, bias, stab, stab_out, decay, inweight, floor):
    normed = rms_scale(tokens[...].astype(F32), gain[...]).astype(BF16)
    in_pre = product_t(normed, w_in[...])
    old = jax.nn.log_sigmoid(product_t(normed, w_forget[...]) + bias[...]) + stab[...]
    new = jnp.maximum(old, in_pre)
    stab_out[...] = new
    decay[...] = jnp.exp(old - new)
    inweight[...] = jnp.exp(in_pre - new)
    floor[...] = jnp.exp(-new)


def body(
    tokens,
    memory,
    normalizer,
    stabilizer,
    norm_gain,
    w_query,
    w_key,
    w_value,
    w_outgate,
    w_input,
    w_forget,
    forget_bias,
    w_out,
    ffn_gain,
    w_gate,
    w_up,
    w_down,
    expert_ids,
    route_weights,
):
    n_ep = lax.axis_size("ep")
    n_tp = lax.axis_size("tp")
    assert n_tp == 2
    me_tp = lax.axis_index("tp")
    swap = [(0, 1), (1, 0)]
    seqs, width = tokens.shape
    share = seqs // n_tp
    half = n_ep * share
    heads, key_size, value_size = (memory.shape[1], memory.shape[2], memory.shape[3])
    value_width = heads * value_size
    key_piece = w_query.shape[2]
    value_piece = w_value.shape[2]
    narrow = heads * key_piece
    broad = heads * value_piece
    total = 2 * narrow + 2 * broad

    copies = call(share_kernel, shape((n_ep, share, width), BF16), [VMEM], [], [tokens], "share")
    raw_own = to_all(copies).reshape(half, width)
    raw_other = lax.ppermute(raw_own, "tp", swap)

    columns = [jnp.transpose(w, (1, 2, 0)).reshape(-1, width) for w in (w_query, w_key, w_value, w_outgate)]
    cut = 2 * narrow + broad
    gain, front, normed_own = call(
        front_kernel,
        (pltpu.VMEM((1, width), F32), pltpu.VMEM((cut, width), BF16), shape((half, width), BF16)),
        [VMEM] + [HBM] * 4,
        [pltpu.SemaphoreType.DMA((4,))],
        [raw_own, norm_gain.reshape(1, width), *columns[:3]],
        "front",
        flops=10**7,
    )
    projected = call(
        functools.partial(project_kernel, seqs=seqs),
        shape((n_ep, seqs, total), BF16),
        [VMEM, VMEM, FAST, FAST, HBM],
        [pltpu.VMEM((broad, width), BF16), pltpu.VMEM((2 * half, width), BF16), pltpu.SemaphoreType.DMA((1,))],
        [normed_own, raw_other, gain, front, columns[3]],
        "project",
        flops=2 * 2 * half * total * width,
    )
    n_cells = seqs * heads
    near = n_cells * 3 // 8
    first = call(
        recall_kernel,
        pltpu.VMEM((near, key_size, value_size), F32),
        [ANY, HBM],
        [pltpu.SemaphoreType.DMA((near,))],
        [projected, memory],
        "recall",
        flops=10**7,
    )
    pieces = to_all(projected)

    stab_next, decay, inweight, floor = call(
        gates_kernel,
        (shape((seqs, heads), F32),) * 4,
        [VMEM] * 6,
        [],
        [tokens, norm_gain.reshape(1, width), w_input.T, w_forget.T, forget_bias.reshape(1, heads), stabilizer],
        "gates",
    )

    hidden, norm_next, key, value = call(
        functools.partial(readout_kernel, piece=(key_piece, value_piece)),
        (
            pltpu.HBM((n_ep, seqs, value_width), BF16),
            shape(normalizer.shape, F32),
            shape((heads * 8, key_size), F32),
            shape((seqs, value_width), F32),
        ),
        [VMEM] * 5 + [FAST, HBM],
        [
            pltpu.VMEM((n_cells - near, key_size, value_size), F32),
            pltpu.VMEM((seqs, value_width), F32),
            pltpu.VMEM((seqs, value_width), BF16),
            pltpu.SemaphoreType.DMA((n_cells - near,)),
            pltpu.SemaphoreType.DMA((n_ep,)),
        ],
        [pieces, decay, inweight, floor, normalizer, first, memory],
        "readout",
        flops=2 * memory.size,
        outs=(HBM, VMEM, VMEM, VMEM),
    )
    hidden_all = to_all(hidden).reshape(n_ep * seqs, value_width)
    memory_next, w_out_near = call(
        update_kernel,
        (shape(memory.shape, F32), pltpu.VMEM(w_out.shape, BF16)),
        [VMEM] * 4 + [HBM] * 2,
        [
            pltpu.VMEM((n_cells, key_size, value_size), F32),
            pltpu.SemaphoreType.DMA((n_cells,)),
            pltpu.SemaphoreType.DMA((n_cells,)),
            pltpu.SemaphoreType.DMA((1,)),
        ],
        [key, value, decay, inweight, w_out, memory],
        "update",
        flops=10**8,
        outs=(HBM, VMEM),
    )

    own_term, other_term = call(
        functools.partial(output_kernel, seqs=seqs),
        (shape((half, w_out.shape[1]), BF16),) * 2,
        [VMEM, FAST],
        [],
        [hidden_all, w_out_near],
        "output",
        flops=2 * n_ep * seqs * w_out.size,
    )
    mixed = (own_term.astype(F32) + lax.ppermute(other_term, "tp", swap).astype(F32)).astype(BF16)
    mixed_all = to_all(jnp.broadcast_to(mixed[None], (n_ep,) + mixed.shape))

    ffn_own, resid_mine = call(
        resid_kernel,
        (shape((half, width), BF16), shape((share, width), F32)),
        [VMEM] * 3,
        [pltpu.VMEM((half, width), F32)],
        [raw_own, mixed_all, ffn_gain.reshape(1, width)],
        "resid",
    )
    ffn_other = lax.ppermute(ffn_own, "tp", swap)
    units = w_gate.shape[2]
    units_near = call(
        units_kernel,
        pltpu.VMEM((width // 2, 2 * units), BF16),
        [ANY, HBM, HBM],
        [pltpu.SemaphoreType.DMA((4,))],
        [ffn_own, w_gate, w_up],
        "units",
        flops=10**7,
    )
    act_own, down, down_other = call(
        expert_kernel,
        (shape((half, units), BF16), pltpu.VMEM((units, width), BF16), shape((half, width), BF16)),
        [VMEM, VMEM, FAST, HBM, HBM, HBM],
        [
            pltpu.VMEM((width // 2, 2 * units), BF16),
            pltpu.SemaphoreType.DMA((4,)),
            pltpu.SemaphoreType.DMA((4,)),
        ],
        [ffn_own, ffn_other, units_near, w_gate, w_up, w_down],
        "experts",
        flops=2 * 3 * half * width * units,
    )
    down_own = call(
        down_kernel, shape((half, width), BF16), [VMEM, FAST], [], [act_own, down], "down", flops=10**7
    )
    summed = call(
        join_kernel,
        shape((n_ep, share, width), BF16),
        [VMEM] * 2,
        [],
        [down_own, lax.ppermute(down_other, "tp", swap)],
        "join",
    )
    by_expert = to_all(summed)

    n_experts = n_ep * w_gate.shape[0]
    labels = jnp.arange(n_experts, dtype=jnp.int32)
    ids = lax.dynamic_slice_in_dim(expert_ids, me_tp * share, share, 0)
    gains = lax.dynamic_slice_in_dim(route_weights, me_tp * share, share, 0)
    route = jnp.sum(jnp.where(ids[:, :, None] == labels[None, None, :], gains[:, :, None], 0.0), axis=1)
    ffn_out = jnp.sum(by_expert.astype(F32) * jnp.swapaxes(route, 0, 1)[:, :, None], axis=0)
    out_mine = (resid_mine + ffn_out).astype(BF16)
    out_other = lax.ppermute(out_mine, "tp", swap)
    first = jnp.where(me_tp == 0, out_mine, out_other)
    last = jnp.where(me_tp == 0, out_other, out_mine)
    out = jnp.concatenate([first, last], axis=0)
    return (out, memory_next, norm_next, stab_next)


def solution(mesh):
    return jax.shard_map(
        body,
        mesh=mesh,
        in_specs=(
            P("ep", None),
            P("ep", "tp", None, None),
            P("ep", "tp", None),
            P("ep", "tp"),
            P(),
            P(None, "tp", "ep"),
            P(None, "tp", "ep"),
            P(None, "tp", "ep"),
            P(None, "tp", "ep"),
            P(None, "tp"),
            P(None, "tp"),
            P("tp"),
            P("tp", "ep"),
            P(),
            P("ep", None, "tp"),
            P("ep", None, "tp"),
            P("ep", "tp", None),
            P("ep", None),
            P("ep", None),
        ),
        out_specs=(P("ep", None), P("ep", "tp", None, None), P("ep", "tp", None), P("ep", "tp")),
        check_vma=False,
    )
```

time: 98 us -> 93.2 us (0.951)
  waiting for transfers between devices: 24.9 us -> 20.5 us
  local copies, waits for them, and re-layouts: 3.88 us -> 1.43 us
  Pallas kernels: 22.8 us -> 25 us
    pallas_call x9 -> x13, Pallas kernels: 22.8 us -> 25 us  [call(): pl.pallas_call(kernel, out_shape=out_shape, in_specs=in_specs, out_specs=...]
    reshape x12 -> x0, local copies, waits for them, and re-layouts: 1.57 us -> none  [the longest x1 0.61 us: body(): return (out, memory_next, norm_next.reshape(normalizer.shape), stab_next)]
    ppermute x1, waiting for transfers between devices: 1.52 us -> 0.01 us  [body(): ffn_other = lax.ppermute(ffn_own, 'tp', swap)]
    ppermute x1, waiting for transfers between devices: 1.52 us -> 0.01 us  [body(): raw_other = lax.ppermute(raw_own, 'tp', swap)]
    all_to_all x3, waiting for transfers between devices: 18.8 us -> 17.5 us  [to_all(): return lax.all_to_all(copies, 'ep', split_axis=0, concat_axis=0, tiled=True)]
  transfers between devices with their start and end apart: 8 -> 8, of which waited for: 8 -> 6; matrix products, arithmetic and copies ran while one was open for 1% -> 1% of each run, Pallas kernels for 8% -> 14%
where the time goes in v3:
time: 93.2 us; the launch traced here: 92.6 us
  blocking collectives  32.1 us (34%)
  Pallas kernels  25 us (27%)
  waiting for transfers between devices  20.5 us (22%)
  starting transfers between devices  11.4 us (12%)
  local copies, waits for them, and re-layouts  1.43 us (2%)
  other arithmetic  1.15 us (1%)
  between operations  0.95 us (1%)
    all_to_all x2, blocking collectives, to_all(): return lax.all_to_all(copies, 'ep', split_axis=0, concat_axis=0, tiled=True)  32.1 us
    pallas_call x13, Pallas kernels, call(): pl.pallas_call(kernel, out_shape=out_shape, in_specs=in_specs, out_specs=...  25 us
    all_to_all x3, waiting for transfers between devices, to_all(): return lax.all_to_all(copies, 'ep', split_axis=0, concat_axis=0, tiled=True)  17.5 us
    all_to_all x3, starting transfers between devices, to_all(): return lax.all_to_all(copies, 'ep', split_axis=0, concat_axis=0, tiled=True)  10.6 us
  transfers between devices with their start and end apart: 8, of which 6 were waited for; matrix products, arithmetic and copies ran while one was open for 1% of the time, Pallas kernels for 14%

profile of v3, /device:TPU:0, one launch (start us, length us, event | category | flops | bytes accessed | tf_op | source)
XLA Modules:
  0.0 92.6 jit_solution(5412559944963508542)
XLA Ops:
  0.6 0.0 copy-start
  0.6 0.0 copy-start.1
  0.7 0.8 copy-done.1
  1.4 18.0 %all_to_all.25 = bf16[16,2,4096]{2,1,0:T(2,128)(2,1)S(1)} all-to-all(bf16[16,2,4096]{2,1,0:T(2,128)(2,1)S(1)} %share.1), channel_id=1, replica_groups=mesh['ep'=16,'tp'=2] {'ep'}, dimensions={0} | all-to-all | bytes 524288 | tf_op jit(solution)/shard_map/all_to_all | solution.py:31
  19.5 0.1 reshape.40.own.raw
  19.6 0.1 collective-permute-start
  19.6 1.6 %front.1 = (f32[1,4096]{1,0:T(1,128)S(1)}, bf16[256,4096]{1,0:T(8,128)(2,1)S(1)}, bf16[32,4096]{1,0:T(8,128)(2,1)S(1)}) custom-call(bf16[32,4096]{1,0:T(8,128)(2,1)S(1)} %reshape.40.own.raw, f32[1,4096]{1,0:T(1,128)} %bitcast.18, bf16[64,4096]{1,0:T(8,128)(2,1)} %bitcast.26, bf16[64,4096]{1,0:T(8,128)(2,1)} %bitcast.27, bf16[128,4096]{1,0:T(8,128)(2,1)} %bitcast.25), custom_call_target="tpu_custom_call" | custom-call | flops 10000000 | bytes 1000000 | tf_op jit(solution)/shard_map/front/pallas_call | solution.py:39
  21.2 0.0 copy-start.2
  21.3 0.0 copy-start.3
  21.3 0.0 copy-start.4
  21.3 0.0 copy-start.5
  21.3 0.0 copy-start.8
  21.3 0.0 copy-start.9
  21.3 2.7 %project.1.after = bf16[16,4,384]{2,1,0:T(4,128)(2,1)} custom-call(bf16[32,4096]{1,0:T(8,128)(2,1)S(1)} %get-tuple-element.24.own, bf16[32,4096]{1,0:T(8,128)(2,1)S(1)} %collective-permute-done.other, f32[1,4096]{1,0:T(1,128)S(1)} %get-tuple-element.25.gain, bf16[256,4096]{1,0:T(8,128)(2,1)S(1)} %get-tuple-element.26.front, bf16[128,4096]{1,0:T(8,128)(2,1)} %bitcast.24), custom_call_target="tpu_custom_call" | custom-call | flops 201326592 | bytes 1000000 | tf_op jit(solution)/shard_map/project/pallas_call | solution.py:39
  24.0 3.6 %all-to-all-start.1 = ((bf16[16,4,384]{2,1,0:T(4,128)(2,1)}), bf16[16,4,384]{2,1,0:T(4,128)(2,1)S(1)}, u32[]{:S(2)}, u32[]{:S(2)}) async-start(bf16[16,4,384]{2,1,0:T(4,128)(2,1)} %project.1.after), calls=%async_computation.1 | async-start | bytes 98304 | tf_op jit(solution)/shard_map/all_to_all | solution.py:31
  27.6 1.0 %gates.1 = (f32[4,4]{1,0:T(4,128)}, f32[4,4]{1,0:T(4,128)S(1)}, f32[4,4]{1,0:T(4,128)S(1)}, f32[4,4]{1,0:T(4,128)S(1)}) custom-call(bf16[4,4096]{1,0:T(4,128)(2,1)S(1)} %copy-done.2, f32[1,4096]{1,0:T(1,128)S(1)} %bitcast.19, bf16[4,4096]{1,0:T(4,128)(2,1)S(1)} %bitcast.20, bf16[4,4096]{1,0:T(4,128)(2,1)S(1)} %bitcast.21, f32[1,4]{1,0:T(1,128)S(1)} %bitcast.23, ...), custom_call_target="tpu_custom_call" | custom-call | flops 1000000 | bytes 1000000 | tf_op jit(solution)/shard_map/gates/pallas_call | solution.py:39
  28.6 1.9 %recall.1.first = f32[6,256,512]{2,1,0:T(8,128)S(1)} custom-call(bf16[16,4,384]{2,1,0:T(4,128)(2,1)} %project.1.after, f32[4,4,256,512]{3,2,1,0:T(8,128)} %memory.5), custom_call_target="tpu_custom_call" | custom-call | flops 10000000 | bytes 1000000 | tf_op jit(solution)/shard_map/recall/pallas_call | solution.py:39
  30.5 4.6 %all-to-all-done.1.pieces = bf16[16,4,384]{2,1,0:T(4,128)(2,1)S(1)} async-done(((bf16[16,4,384]{2,1,0:T(4,128)(2,1)}), bf16[16,4,384]{2,1,0:T(4,128)(2,1)S(1)}, u32[]{:S(2)}, u32[]{:S(2)}) %all-to-all-start.1) | async-done | bytes 49184 | tf_op jit(solution)/shard_map/all_to_all | solution.py:31
  35.0 4.6 %readout.1 = (bf16[16,4,2048]{2,1,0:T(4,128)(2,1)}, f32[4,4,256]{2,1,0:T(4,128)}, f32[32,256]{1,0:T(8,128)S(1)}, f32[4,2048]{1,0:T(4,128)S(1)}) custom-call(bf16[16,4,384]{2,1,0:T(4,128)(2,1)S(1)} %all-to-all-done.1.pieces, f32[4,4]{1,0:T(4,128)S(1)} %get-tuple-element.27.decay, f32[4,4]{1,0:T(4,128)S(1)} %get-tuple-element.28.inweight, ...), custom_call_target="tpu_custom_call" | custom-call | flops 4194304 | bytes 1000000 | tf_op jit(solution)/shard_map/readout/pallas_call | solution.py:39
  39.6 3.5 %all-to-all-start.2 = ((bf16[16,4,2048]{2,1,0:T(4,128)(2,1)}), bf16[16,4,2048]{2,1,0:T(4,128)(2,1)S(1)}, u32[]{:S(2)}, u32[]{:S(2)}) async-start(bf16[16,4,2048]{2,1,0:T(4,128)(2,1)} %get-tuple-element.30), calls=%async_computation.2 | async-start | bytes 524288 | tf_op jit(solution)/shard_map/all_to_all | solution.py:31
  43.2 6.7 %update.1 = (f32[4,4,256,512]{3,2,1,0:T(8,128)}, bf16[2048,256]{1,0:T(8,128)(2,1)S(1)}) custom-call(f32[32,256]{1,0:T(8,128)S(1)} %get-tuple-element.31.key, f32[4,2048]{1,0:T(4,128)S(1)} %get-tuple-element.32.value, f32[4,4]{1,0:T(4,128)S(1)} %get-tuple-element.27.decay, f32[4,4]{1,0:T(4,128)S(1)} %get-tuple-element.28.inweight, bf16[2048,256]{1,0:T(8,128)(2,1)} %w_out.1, ...), custom_call_target="tpu_custom_call" | custom-call | flops 100000000 | bytes 1000000 | tf_op jit(solution)/shard_map/update/pallas_call | solution.py:39
  49.9 0.0 copy-start.7
  49.9 2.8 %all-to-all-done.2 = bf16[16,4,2048]{2,1,0:T(4,128)(2,1)S(1)} async-done(((bf16[16,4,2048]{2,1,0:T(4,128)(2,1)}), bf16[16,4,2048]{2,1,0:T(4,128)(2,1)S(1)}, u32[]{:S(2)}, u32[]{:S(2)}) %all-to-all-start.2) | async-done | bytes 262176 | tf_op jit(solution)/shard_map/all_to_all | solution.py:31
  52.7 0.1 reshape.47.hidden
  52.8 0.4 output.1
  53.2 1.2 %collective-permute-done.1 = bf16[32,256]{1,0:T(8,128)(2,1)S(1)} collective-permute-done((bf16[32,256]{1,0:T(8,128)(2,1)S(1)}, bf16[32,256]{1,0:T(8,128)(2,1)S(1)}, u32[]{:S(2)}, u32[]{:S(2)}) %collective-permute-start.1) | collective-permute-done | bytes 16416 | tf_op jit(solution)/shard_map/ppermute | solution.py:443
  54.4 14.1 %all_to_all.26.mixed = bf16[16,32,256]{2,1,0:T(8,128)(2,1)S(1)} all-to-all(bf16[16,32,256]{2,1,0:T(8,128)(2,1)S(1)} %broadcast_in_dim.10), channel_id=1, replica_groups=mesh['ep'=16,'tp'=2] {'ep'}, dimensions={0} | all-to-all | bytes 524288 | tf_op jit(solution)/shard_map/all_to_all | solution.py:31
  68.5 0.2 resid.1
  68.7 0.1 collective-permute-start.2
  68.8 1.6 %units.1.near = bf16[2048,512]{1,0:T(8,128)(2,1)S(1)} custom-call(bf16[32,4096]{1,0:T(8,128)(2,1)S(1)} %get-tuple-element.37.after.own, bf16[1,4096,256]{2,1,0:T(8,128)(2,1)} %w_gate.3, bf16[1,4096,256]{2,1,0:T(8,128)(2,1)} %w_up.3), custom_call_target="tpu_custom_call" | custom-call | flops 10000000 | bytes 1000000 | tf_op jit(solution)/shard_map/units/pallas_call | solution.py:39
  70.3 3.2 %experts.1 = (bf16[32,256]{1,0:T(8,128)(2,1)S(1)}, bf16[256,4096]{1,0:T(8,128)(2,1)S(1)}, bf16[32,4096]{1,0:T(8,128)(2,1)S(1)}) custom-call(bf16[32,4096]{1,0:T(8,128)(2,1)S(1)} %get-tuple-element.37.after.own, bf16[32,4096]{1,0:T(8,128)(2,1)S(1)} %collective-permute-done.2.other, bf16[2048,512]{1,0:T(8,128)(2,1)S(1)} %units.1.near, ...), custom_call_target="tpu_custom_call" | custom-call | flops 201326592 | bytes 1000000 | tf_op jit(solution)/shard_map/experts/pallas_call | solution.py:39
  73.5 0.0 copy-start.10
  73.6 0.6 collective-permute-start.3
  74.1 0.5 down.1.own
  74.6 0.7 collective-permute-done.3.other
  75.3 0.8 join.1
  76.1 3.5 %all-to-all-start.4 = ((bf16[16,2,4096]{2,1,0:T(2,128)(2,1)}), bf16[16,2,4096]{2,1,0:T(2,128)(2,1)S(1)}, u32[]{:S(2)}, u32[]{:S(2)}) async-start(bf16[16,2,4096]{2,1,0:T(2,128)(2,1)} %join.1), calls=%async_computation.4 | async-start | bytes 524288 | tf_op jit(solution)/shard_map/all_to_all | solution.py:31
  79.7 0.1 constant_dynamic-slice_fusion
  79.7 0.1 copy.26
  79.8 0.1 constant_dynamic-slice_fusion.1
  79.9 0.1 copy.25
  80.0 0.1 fusion
  80.1 0.1 copy.27
  80.2 10.1 %all-to-all-done.4 = bf16[16,2,4096]{2,1,0:T(2,128)(2,1)S(1)} async-done(((bf16[16,2,4096]{2,1,0:T(2,128)(2,1)}), bf16[16,2,4096]{2,1,0:T(2,128)(2,1)S(1)}, u32[]{:S(2)}, u32[]{:S(2)}) %all-to-all-start.4) | async-done | bytes 262176 | tf_op jit(solution)/shard_map/all_to_all | solution.py:31
  90.3 0.3 multiply_reduce_fusion
  90.6 0.1 collective-permute-start.4
  90.7 1.2 %collective-permute-done.4 = bf16[2,4096]{1,0:T(2,128)(2,1)S(1)} collective-permute-done((bf16[2,4096]{1,0:T(2,128)(2,1)S(1)}, bf16[2,4096]{1,0:T(2,128)(2,1)S(1)}, u32[]{:S(2)}, u32[]{:S(2)}) %collective-permute-start.4) | collective-permute-done | bytes 16416 | tf_op jit(solution)/shard_map/ppermute | solution.py:498
  91.9 0.7 pad_maximum_fusion
  (19 shorter events, 0.1 us)
Async XLA Ops:
  0.6 79.0 %copy-start = (f32[4,2]{0,1:T(2,128)S(1)}, f32[4,2]{0,1:T(2,128)}, u32[]{:S(2)}) copy-start(f32[4,2]{0,1:T(2,128)} %param.37) | copy-start | bytes 100
  0.6 0.8 copy-start.1
  19.6 1.8 %collective-permute-start = (bf16[32,4096]{1,0:T(8,128)(2,1)S(1)}, bf16[32,4096]{1,0:T(8,128)(2,1)S(1)}, u32[]{:S(2)}, u32[]{:S(2)}) collective-permute-start(bf16[32,4096]{1,0:T(8,128)(2,1)S(1)} %reshape.40.own.raw), channel_id=1, source_target_pairs={{0,1},{1,0},{2,3},{3,2},{4,5},{5,4},{6,7},{7,6},{8,9},{9,8},{10,11... | collective-permute-start | bytes 786440 | tf_op jit(solution)/shard_map/ppermute | solution.py:352
  21.2 6.3 %copy-start.2 = (bf16[4,4096]{1,0:T(4,128)(2,1)S(1)}, bf16[4,4096]{1,0:T(4,128)(2,1)}, u32[]{:S(2)}) copy-start(bf16[4,4096]{1,0:T(4,128)(2,1)} %tokens.3) | copy-start | bytes 98308
  21.3 6.3 %copy-start.3 = (f32[4096]{0:T(1024)S(1)}, f32[4096]{0:T(1024)}, u32[]{:S(2)}) copy-start(f32[4096]{0:T(1024)} %param.23) | copy-start | bytes 49156
  21.3 6.3 %copy-start.4 = (bf16[4096,4]{0,1:T(4,128)(2,1)S(1)}, bf16[4096,4]{0,1:T(4,128)(2,1)}, u32[]{:S(2)}) copy-start(bf16[4096,4]{0,1:T(4,128)(2,1)} %param.28) | copy-start | bytes 98308
  21.3 6.3 %copy-start.5 = (bf16[4096,4]{0,1:T(4,128)(2,1)S(1)}, bf16[4096,4]{0,1:T(4,128)(2,1)}, u32[]{:S(2)}) copy-start(bf16[4096,4]{0,1:T(4,128)(2,1)} %param.29) | copy-start | bytes 98308
  21.3 6.3 %copy-start.8 = (f32[4,4]{1,0:T(4,128)S(1)}, f32[4,4]{1,0:T(4,128)}, u32[]{:S(2)}) copy-start(f32[4,4]{1,0:T(4,128)} %stab.1) | copy-start | bytes 196
  21.3 6.3 %copy-start.9 = (f32[4]{0:T(128)S(1)}, f32[4]{0:T(128)}, u32[]{:S(2)}) copy-start(f32[4]{0:T(128)} %param.30) | copy-start | bytes 52
  24.0 11.0 %all-to-all-start.1 = ((bf16[16,4,384]{2,1,0:T(4,128)(2,1)}), bf16[16,4,384]{2,1,0:T(4,128)(2,1)S(1)}, u32[]{:S(2)}, u32[]{:S(2)}) async-start(bf16[16,4,384]{2,1,0:T(4,128)(2,1)} %project.1.after), calls=%async_computation.1 | async-start | bytes 98304 | tf_op jit(solution)/shard_map/all_to_all | solution.py:31
  28.6 6.5 %copy-start.6 = (f32[4,4,256]{2,1,0:T(4,128)S(1)}, f32[4,4,256]{2,1,0:T(4,128)}, u32[]{:S(2)}) copy-start(f32[4,4,256]{2,1,0:T(4,128)} %norm.1) | copy-start | bytes 49156
  39.6 13.1 %all-to-all-start.2 = ((bf16[16,4,2048]{2,1,0:T(4,128)(2,1)}), bf16[16,4,2048]{2,1,0:T(4,128)(2,1)S(1)}, u32[]{:S(2)}, u32[]{:S(2)}) async-start(bf16[16,4,2048]{2,1,0:T(4,128)(2,1)} %get-tuple-element.30), calls=%async_computation.2 | async-start | bytes 524288 | tf_op jit(solution)/shard_map/all_to_all | solution.py:31
  49.9 18.6 %copy-start.7 = (f32[4096]{0:T(1024)S(1)}, f32[4096]{0:T(1024)}, u32[]{:S(2)}) copy-start(f32[4096]{0:T(1024)} %param.32) | copy-start | bytes 49156
  53.2 1.2 %collective-permute-start.1 = (bf16[32,256]{1,0:T(8,128)(2,1)S(1)}, bf16[32,256]{1,0:T(8,128)(2,1)S(1)}, u32[]{:S(2)}, u32[]{:S(2)}) collective-permute-start(bf16[32,256]{1,0:T(8,128)(2,1)S(1)} %get-tuple-element.35), channel_id=1, source_target_pairs={{0,1},{1,0},{2,3},{3,2},{4,5},{5,4},{6,7},{7,6},{8,9},{9,8},{10,11... | collective-permute-start | bytes 49160 | tf_op jit(solution)/shard_map/ppermute | solution.py:443
  68.7 1.6 %collective-permute-start.2 = (bf16[32,4096]{1,0:T(8,128)(2,1)S(1)}, bf16[32,4096]{1,0:T(8,128)(2,1)S(1)}, u32[]{:S(2)}, u32[]{:S(2)}) collective-permute-start(bf16[32,4096]{1,0:T(8,128)(2,1)S(1)} %get-tuple-element.37.after.own), channel_id=1, source_target_pairs={{0,1},{1,0},{2,3},{3,2},{4,5},{5,4},{6,7},{7,6},{8,9},{9,8},{10,11... | collective-permute-start | bytes 786440 | tf_op jit(solution)/shard_map/ppermute | solution.py:454
  73.5 6.3 %copy-start.10 = (s32[4,2]{0,1:T(2,128)S(1)}, s32[4,2]{0,1:T(2,128)}, u32[]{:S(2)}) copy-start(s32[4,2]{0,1:T(2,128)} %param.36) | copy-start | bytes 100
  73.6 1.7 %collective-permute-start.3 = (bf16[32,4096]{1,0:T(8,128)(2,1)S(1)}, bf16[32,4096]{1,0:T(8,128)(2,1)S(1)}, u32[]{:S(2)}, u32[]{:S(2)}) collective-permute-start(bf16[32,4096]{1,0:T(8,128)(2,1)S(1)} %get-tuple-element.40), channel_id=1, source_target_pairs={{0,1},{1,0},{2,3},{3,2},{4,5},{5,4},{6,7},{7,6},{8,9},{9,8},{10,11... | collective-permute-start | bytes 786440 | tf_op jit(solution)/shard_map/ppermute | solution.py:486
  76.1 14.2 %all-to-all-start.4 = ((bf16[16,2,4096]{2,1,0:T(2,128)(2,1)}), bf16[16,2,4096]{2,1,0:T(2,128)(2,1)S(1)}, u32[]{:S(2)}, u32[]{:S(2)}) async-start(bf16[16,2,4096]{2,1,0:T(2,128)(2,1)} %join.1), calls=%async_computation.4 | async-start | bytes 524288 | tf_op jit(solution)/shard_map/all_to_all | solution.py:31
  90.6 1.2 %collective-permute-start.4 = (bf16[2,4096]{1,0:T(2,128)(2,1)S(1)}, bf16[2,4096]{1,0:T(2,128)(2,1)S(1)}, u32[]{:S(2)}, u32[]{:S(2)}) collective-permute-start(bf16[2,4096]{1,0:T(2,128)(2,1)S(1)} %add_convert_fusion), channel_id=1, source_target_pairs={{0,1},{1,0},{2,3},{3,2},{4,5},{5,4},{6,7},{7,6},{8,9},{9,8},{10,11... | collective-permute-start | bytes 49160 | tf_op jit(solution)/shard_map/ppermute | solution.py:498

commit v4 on v3

--- a/solution.py
+++ b/solution.py
@@ -8,6 +8,7 @@
 from jax.sharding import PartitionSpec as P
 
 F32 = jnp.float32
+LONG = 10**11
 BF16 = jnp.bfloat16
 ANY = pl.BlockSpec(memory_space=pl.ANY)
 HBM = pl.BlockSpec(memory_space=pltpu.HBM)
@@ -31,7 +32,7 @@
     return lax.all_to_all(copies, "ep", split_axis=0, concat_axis=0, tiled=True)
 
 
-def call(kernel, out_shape, in_specs, scratch, args, name, flops=10**6, outs=None):
+def call(kernel, out_shape, in_specs, scratch, args, name, flops=10**6, outs=None, nbytes=10**6):
     many = isinstance(out_shape, tuple)
     outs = outs or (tuple(VMEM for _ in out_shape) if many else VMEM)
     pins = {id(HBM): pltpu.HBM, id(FAST): pltpu.VMEM}
@@ -44,7 +45,7 @@
         scratch_shapes=scratch,
         name=name,
         compiler_params=pltpu.CompilerParams(vmem_limit_bytes=24 << 20),
-        cost_estimate=pl.CostEstimate(flops=flops, transcendentals=0, bytes_accessed=10**6),
+        cost_estimate=pl.CostEstimate(flops=flops, transcendentals=0, bytes_accessed=nbytes),
     )(*args)
 
 
@@ -59,80 +60,20 @@
     return copies
 
 
-def front_kernel(own, gain, wq, wk, wv, gain_out, weights, normed, sems):
-    pairs, at = [(gain, gain_out)], 0
-    for w in (wq, wk, wv):
-        pairs.append((w, weights.at[pl.ds(at, w.shape[0])]))
-        at += w.shape[0]
-    copies = fetch(pairs, sems)
-    copies[0].wait()
-    normed[...] = rms_scale(own[...].astype(F32), gain_out[...]).astype(BF16)
-    for c in copies[1:]:
-        c.wait()
-
-
-def recall_kernel(after, memory, out, sems):
-    heads = memory.shape[1]
-    for c in fetch([(memory.at[n // heads, n % heads], out.at[n]) for n in range(out.shape[0])], sems):
-        c.wait()
-
-
-def units_kernel(after, w_gate, w_up, out, sems):
-    rows, units = out.shape[0] // 2, out.shape[1] // 2
-    pairs = []
-    for n in range(2):
-        at = pl.ds(n * rows, rows)
-        pairs.append((w_gate.at[0, at], out.at[at, pl.ds(0, units)]))
-        pairs.append((w_up.at[0, at], out.at[at, pl.ds(units, units)]))
-    for c in fetch(pairs, sems):
-        c.wait()
-
-
-def expert_kernel(own, other, near, w_gate, w_up, w_down, act_own, down, out, far, sems, down_sems):
-    done, units = near.shape[0], w_gate.shape[2]
-    parts = sems.shape[0] // 2
-    rows = far.shape[0] // parts
-    pairs = []
-    for n in range(parts):
-        src, dst = pl.ds(done + n * rows, rows), pl.ds(n * rows, rows)
-        pairs.append((w_gate.at[0, src], far.at[dst, pl.ds(0, units)]))
-        pairs.append((w_up.at[0, src], far.at[dst, pl.ds(units, units)]))
-    copies = fetch(pairs, sems)
-    slabs = down_sems.shape[0]
-    width = w_down.shape[2] // slabs
-    at = [pl.ds(n * width, width) for n in range(slabs)]
-    downs = fetch([(w_down.at[0, :, a], down.at[:, a]) for a in at], down_sems)
-
-    def left(start, stop):
-        return jnp.concatenate([own[:, start:stop], other[:, start:stop]], axis=0)
-
-    total = product(left(0, done), near[...])
-    for n in range(parts):
-        copies[2 * n].wait()
-        copies[2 * n + 1].wait()
-        start = done + n * rows
-        total = total + product(left(start, start + rows), far[n * rows : (n + 1) * rows])
-    act = (jax.nn.silu(total[:, 0:units]) * total[:, units:]).astype(BF16)
+def stack(blocks):
+    return jnp.concatenate([blocks[e].astype(F32) for e in range(blocks.shape[0])], axis=0)
+
+
+def front_kernel(own, gain, raw, normed):
+    rows = stack(own)
+    raw[...] = rows.astype(BF16)
+    normed[...] = rms_scale(rows, gain[...]).astype(BF16)
+
+
+def project_kernel(own, other, gain, wq, wk, wv, wo, after, out, normed, *, seqs):
     half = own.shape[0]
-    act_own[...] = act[0:half]
-    for n in range(slabs):
-        downs[n].wait()
-        at = slice(n * width, (n + 1) * width)
-        out[:, at] = product(act[half:], down[:, at]).astype(BF16)
-
-
-def down_kernel(act, down, out):
-    out[...] = product(act[...], down[...]).astype(BF16)
-
-
-def project_kernel(own, other, gain, front, wo, out, back, normed, sems, *, seqs):
-    (copy,) = fetch([(wo, back)], sems)
-    half = other.shape[0]
     normed[0:half] = own[...]
-    normed[half:] = rms_scale(other[...].astype(F32), gain[...]).astype(BF16)
-    left = product_t(front[...], normed[...]).astype(BF16)
-    copy.wait()
-    right = product_t(back[...], normed[...]).astype(BF16)
+    normed[half:] = rms_scale(stack(other), gain[...]).astype(BF16)
     rows = 2 * half
     share = seqs // 2
     me = lax.axis_index("tp")
@@ -141,12 +82,23 @@
     token = r % seqs
     which = (token // share + me) % 2
     pick = (c == which * half + (r // seqs) * share + token % share).astype(BF16)
-    left = product_t(pick, left)
-    right = product_t(pick, right)
-    cut = front.shape[0]
+    found = [product_t(w[...], normed[...]).astype(BF16) for w in (wq, wk, wv, wo)]
+    found = product_t(pick, jnp.concatenate(found, axis=0))
     for d in range(rows // seqs):
-        out[d, :, 0:cut] = left[d * seqs : (d + 1) * seqs].astype(BF16)
-        out[d, :, cut:] = right[d * seqs : (d + 1) * seqs].astype(BF16)
+        out[d] = found[d * seqs : (d + 1) * seqs].astype(BF16)
+
+
+def expert_kernel(own, other, w_gate, w_up, w_down, act_own, out):
+    left = jnp.concatenate([own[...], other[...]], axis=0)
+    gate = product(left, w_gate[0])
+    act = (jax.nn.silu(gate) * product(left, w_up[0])).astype(BF16)
+    half = own.shape[0]
+    act_own[...] = act[0:half]
+    out[...] = product(act[half:], w_down[0]).astype(BF16)
+
+
+def down_kernel(act, w_down, out):
+    out[...] = product(act[...], w_down[0]).astype(BF16)
 
 
 def spread(pieces, start, piece, blocks, seqs):
@@ -174,24 +126,18 @@
     inweight,
     floor,
     norm,
-    first,
     memory,
     out,
     norm_out,
     key_out,
     value_out,
-    buf,
     recalled,
     hidden,
-    sems,
     out_sems,
     *,
     piece,
 ):
     seqs, heads, dk, dv = memory.shape
-    near = first.shape[0]
-    cells = [(n // heads, n % heads) for n in range(seqs * heads)]
-    copies = fetch([(memory.at[i, h], buf.at[n]) for n, (i, h) in enumerate(cells[near:])], sems)
     rows = jnp.concatenate([pieces[m].astype(F32) for m in range(pieces.shape[0])], axis=0).astype(BF16)
     small, large = piece
     narrow = spread(rows, 0, small, 2 * heads, seqs)
@@ -205,8 +151,9 @@
         part = jnp.sum(cell * columns[:, n : n + 1], axis=0, keepdims=True)
         recalled[i : i + 1, h * dv : (h + 1) * dv] = part
 
-    for n, (i, h) in enumerate(cells[:near]):
-        recall(first[n], i, h)
+    for i in range(seqs):
+        for h in range(heads):
+            recall(memory[i, h], i, h)
     value = spread(rows, 2 * heads * small, large, heads, seqs)[0:seqs]
     outgate = spread(rows, 2 * heads * small + heads * large, large, heads, seqs)[0:seqs]
     value_out[...] = value
@@ -222,9 +169,6 @@
         below.append(jnp.maximum(jnp.abs(jnp.sum(q * new, axis=1, keepdims=True)), floor[:, h : h + 1]))
         along.append(w * jnp.sum(q * k, axis=1, keepdims=True))
     gate = jax.nn.sigmoid(outgate)
-    for n, (i, h) in enumerate(cells[near:]):
-        copies[n].wait()
-        recall(buf[n], i, h)
     for h in range(heads):
         at = slice(h * dv, (h + 1) * dv)
         top = decay[:, h : h + 1] * recalled[:, at] + along[h] * value[:, at]
@@ -299,7 +243,9 @@
         out[e] = mine
 
 
-def gates_kernel(tokens, gain, w_in, w_forget, bias, stab, stab_out, decay, inweight, floor):
+def gates_kernel(
+    tokens, gain, w_in, w_forget, bias, stab, ids, weights, after, stab_out, decay, inweight, floor, route
+):
     normed = rms_scale(tokens[...].astype(F32), gain[...]).astype(BF16)
     in_pre = product_t(normed, w_in[...])
     old = jax.nn.log_sigmoid(product_t(normed, w_forget[...]) + bias[...]) + stab[...]
@@ -308,6 +254,34 @@
     decay[...] = jnp.exp(old - new)
     inweight[...] = jnp.exp(in_pre - new)
     floor[...] = jnp.exp(-new)
+    share, experts = route.shape
+    seqs = ids.shape[1]
+    label = lax.broadcasted_iota(jnp.int32, (seqs, experts), 1)
+    same = lax.broadcasted_iota(jnp.int32, (seqs, seqs), 0) == lax.broadcasted_iota(jnp.int32, (seqs, seqs), 1)
+
+    def column(row):
+        return jnp.sum(jnp.where(same, row, 0.0), axis=1, keepdims=True)
+
+    dense = jnp.zeros(label.shape, F32)
+    for k in range(ids.shape[0]):
+        chosen = column(ids[k : k + 1].astype(F32)).astype(jnp.int32)
+        dense = dense + jnp.where(chosen == label, column(weights[k : k + 1]), 0.0)
+    route[...] = jnp.where(lax.axis_index("tp") == 0, dense[0:share], dense[share:])
+
+
+def finish_kernel(terms, route, resid, out):
+    total = resid[...]
+    for e in range(terms.shape[0]):
+        total = total + route[:, e : e + 1] * terms[e].astype(F32)
+    out[...] = total.astype(BF16)
+
+
+def merge_kernel(mine, other, out):
+    share = mine.shape[0]
+    first = lax.axis_index("tp") == 0
+    a, b = mine[...].astype(F32), other[...].astype(F32)
+    out[0:share] = jnp.where(first, a, b).astype(BF16)
+    out[share:] = jnp.where(first, b, a).astype(BF16)
 
 
 def body(
@@ -334,7 +308,6 @@
     n_ep = lax.axis_size("ep")
     n_tp = lax.axis_size("tp")
     assert n_tp == 2
-    me_tp = lax.axis_index("tp")
     swap = [(0, 1), (1, 0)]
     seqs, width = tokens.shape
     share = seqs // n_tp
@@ -347,51 +320,48 @@
     broad = heads * value_piece
     total = 2 * narrow + 2 * broad
 
-    copies = call(share_kernel, shape((n_ep, share, width), BF16), [VMEM], [], [tokens], "share")
-    raw_own = to_all(copies).reshape(half, width)
-    raw_other = lax.ppermute(raw_own, "tp", swap)
-
+    copies = call(share_kernel, shape((n_ep, share, width), BF16), [VMEM], [], [tokens], "share", flops=LONG)
+    gathered = to_all(copies)
+    gathered_other = lax.ppermute(gathered, "tp", swap)
+    raw_own, normed_own = call(
+        front_kernel,
+        (shape((half, width), BF16),) * 2,
+        [VMEM] * 2,
+        [],
+        [gathered, norm_gain.reshape(1, width)],
+        "front",
+    )
+    n_experts = n_ep * w_gate.shape[0]
+    stab_next, decay, inweight, floor, route = call(
+        gates_kernel,
+        (shape((seqs, heads), F32),) * 4 + (shape((share, n_experts), F32),),
+        [VMEM] * 8 + [ANY],
+        [],
+        [
+            tokens,
+            norm_gain.reshape(1, width),
+            w_input.T,
+            w_forget.T,
+            forget_bias.reshape(1, heads),
+            stabilizer,
+            expert_ids.T,
+            route_weights.T,
+            normed_own,
+        ],
+        "gates",
+    )
     columns = [jnp.transpose(w, (1, 2, 0)).reshape(-1, width) for w in (w_query, w_key, w_value, w_outgate)]
-    cut = 2 * narrow + broad
-    gain, front, normed_own = call(
-        front_kernel,
-        (pltpu.VMEM((1, width), F32), pltpu.VMEM((cut, width), BF16), shape((half, width), BF16)),
-        [VMEM] + [HBM] * 4,
-        [pltpu.SemaphoreType.DMA((4,))],
-        [raw_own, norm_gain.reshape(1, width), *columns[:3]],
-        "front",
-        flops=10**7,
-    )
     projected = call(
         functools.partial(project_kernel, seqs=seqs),
         shape((n_ep, seqs, total), BF16),
-        [VMEM, VMEM, FAST, FAST, HBM],
-        [pltpu.VMEM((broad, width), BF16), pltpu.VMEM((2 * half, width), BF16), pltpu.SemaphoreType.DMA((1,))],
-        [normed_own, raw_other, gain, front, columns[3]],
+        [VMEM] * 7 + [ANY],
+        [pltpu.VMEM((2 * half, width), BF16)],
+        [normed_own, gathered_other, norm_gain.reshape(1, width), *columns, route],
         "project",
-        flops=2 * 2 * half * total * width,
+        flops=LONG,
     )
     n_cells = seqs * heads
-    near = n_cells * 3 // 8
-    first = call(
-        recall_kernel,
-        pltpu.VMEM((near, key_size, value_size), F32),
-        [ANY, HBM],
-        [pltpu.SemaphoreType.DMA((near,))],
-        [projected, memory],
-        "recall",
-        flops=10**7,
-    )
     pieces = to_all(projected)
-
-    stab_next, decay, inweight, floor = call(
-        gates_kernel,
-        (shape((seqs, heads), F32),) * 4,
-        [VMEM] * 6,
-        [],
-        [tokens, norm_gain.reshape(1, width), w_input.T, w_forget.T, forget_bias.reshape(1, heads), stabilizer],
-        "gates",
-    )
 
     hidden, norm_next, key, value = call(
         functools.partial(readout_kernel, piece=(key_piece, value_piece)),
@@ -401,15 +371,13 @@
             shape((heads * 8, key_size), F32),
             shape((seqs, value_width), F32),
         ),
-        [VMEM] * 5 + [FAST, HBM],
+        [VMEM] * 6,
         [
-            pltpu.VMEM((n_cells - near, key_size, value_size), F32),
             pltpu.VMEM((seqs, value_width), F32),
             pltpu.VMEM((seqs, value_width), BF16),
-            pltpu.SemaphoreType.DMA((n_cells - near,)),
             pltpu.SemaphoreType.DMA((n_ep,)),
         ],
-        [pieces, decay, inweight, floor, normalizer, first, memory],
+        [pieces, decay, inweight, floor, normalizer, memory],
         "readout",
         flops=2 * memory.size,
         outs=(HBM, VMEM, VMEM, VMEM),
@@ -438,7 +406,7 @@
         [],
         [hidden_all, w_out_near],
         "output",
-        flops=2 * n_ep * seqs * w_out.size,
+        flops=LONG,
     )
     mixed = (own_term.astype(F32) + lax.ppermute(other_term, "tp", swap).astype(F32)).astype(BF16)
     mixed_all = to_all(jnp.broadcast_to(mixed[None], (n_ep,) + mixed.shape))
@@ -453,30 +421,17 @@
     )
     ffn_other = lax.ppermute(ffn_own, "tp", swap)
     units = w_gate.shape[2]
-    units_near = call(
-        units_kernel,
-        pltpu.VMEM((width // 2, 2 * units), BF16),
-        [ANY, HBM, HBM],
-        [pltpu.SemaphoreType.DMA((4,))],
-        [ffn_own, w_gate, w_up],
-        "units",
-        flops=10**7,
-    )
-    act_own, down, down_other = call(
+    act_own, down_other = call(
         expert_kernel,
-        (shape((half, units), BF16), pltpu.VMEM((units, width), BF16), shape((half, width), BF16)),
-        [VMEM, VMEM, FAST, HBM, HBM, HBM],
-        [
-            pltpu.VMEM((width // 2, 2 * units), BF16),
-            pltpu.SemaphoreType.DMA((4,)),
-            pltpu.SemaphoreType.DMA((4,)),
-        ],
-        [ffn_own, ffn_other, units_near, w_gate, w_up, w_down],
+        (shape((half, units), BF16), shape((half, width), BF16)),
+        [VMEM] * 5,
+        [],
+        [ffn_own, ffn_other, w_gate, w_up, w_down],
         "experts",
         flops=2 * 3 * half * width * units,
     )
     down_own = call(
-        down_kernel, shape((half, width), BF16), [VMEM, FAST], [], [act_own, down], "down", flops=10**7
+        down_kernel, shape((half, width), BF16), [VMEM] * 2, [], [act_own, w_down], "down", flops=10**7
     )
     summed = call(
         join_kernel,
@@ -488,17 +443,17 @@
     )
     by_expert = to_all(summed)
 
-    n_experts = n_ep * w_gate.shape[0]
-    labels = jnp.arange(n_experts, dtype=jnp.int32)
-    ids = lax.dynamic_slice_in_dim(expert_ids, me_tp * share, share, 0)
-    gains = lax.dynamic_slice_in_dim(route_weights, me_tp * share, share, 0)
-    route = jnp.sum(jnp.where(ids[:, :, None] == labels[None, None, :], gains[:, :, None], 0.0), axis=1)
-    ffn_out = jnp.sum(by_expert.astype(F32) * jnp.swapaxes(route, 0, 1)[:, :, None], axis=0)
-    out_mine = (resid_mine + ffn_out).astype(BF16)
-    out_other = lax.ppermute(out_mine, "tp", swap)
-    first = jnp.where(me_tp == 0, out_mine, out_other)
-    last = jnp.where(me_tp == 0, out_other, out_mine)
-    out = jnp.concatenate([first, last], axis=0)
+    out_mine = call(
+        finish_kernel, shape((share, width), BF16), [VMEM] * 3, [], [by_expert, route, resid_mine], "finish"
+    )
+    out = call(
+        merge_kernel,
+        shape((seqs, width), BF16),
+        [VMEM] * 2,
+        [],
+        [out_mine, lax.ppermute(out_mine, "tp", swap)],
+        "merge",
+    )
     return (out, memory_next, norm_next, stab_next)
 
 

time: 93.2 us -> 87 us (0.933)
  blocking collectives: 32.1 us -> 57.3 us
  waiting for transfers between devices: 20.5 us -> 7.49 us
  Pallas kernels: 25 us -> 16.1 us
  starting transfers between devices: 11.4 us -> 3.87 us
  other arithmetic: 1.15 us -> 0.01 us
    all_to_all x2 -> x4, blocking collectives: 32.1 us -> 57.3 us  [to_all(): return lax.all_to_all(copies, 'ep', split_axis=0, concat_axis=0, tiled=True)]
    all_to_all x3 -> x1, waiting for transfers between devices: 17.5 us -> 2.44 us  [to_all(): return lax.all_to_all(copies, 'ep', split_axis=0, concat_axis=0, tiled=True)]
    pallas_call x13, Pallas kernels: 25 us -> 16.1 us  [call(): pl.pallas_call(kernel, out_shape=out_shape, in_specs=in_specs, out_specs=...]
    all_to_all x3 -> x1, starting transfers between devices: 10.6 us -> 3.54 us  [to_all(): return lax.all_to_all(copies, 'ep', split_axis=0, concat_axis=0, tiled=True)]
    ppermute x1, waiting for transfers between devices: 0.01 us -> 1.52 us  [body(): ffn_other = lax.ppermute(ffn_own, 'tp', swap)]
  transfers between devices with their start and end apart: 8 -> 6, of which waited for: 6 -> 6; matrix products, arithmetic and copies ran while one was open for 1% -> 0% of each run, Pallas kernels for 14% -> 10%
where the time goes in v4:
time: 87 us; the launch traced here: 86.6 us
  blocking collectives  57.3 us (66%)
  Pallas kernels  16.1 us (19%)
  waiting for transfers between devices  7.49 us (9%)
  starting transfers between devices  3.87 us (4%)
  between operations  0.94 us (1%)
  local copies, waits for them, and re-layouts  0.92 us (1%)
    all_to_all x4, blocking collectives, to_all(): return lax.all_to_all(copies, 'ep', split_axis=0, concat_axis=0, tiled=True)  57.3 us
    pallas_call x13, Pallas kernels, call(): pl.pallas_call(kernel, out_shape=out_shape, in_specs=in_specs, out_specs=...  16.1 us
    all_to_all x1, starting transfers between devices, to_all(): return lax.all_to_all(copies, 'ep', split_axis=0, concat_axis=0, tiled=True)  3.54 us
    all_to_all x1, waiting for transfers between devices, to_all(): return lax.all_to_all(copies, 'ep', split_axis=0, concat_axis=0, tiled=True)  2.44 us
  transfers between devices with their start and end apart: 6, of which 6 were waited for; matrix products, arithmetic and copies ran while one was open for 0% of the time, Pallas kernels for 10%

profile of v4, /device:TPU:0, one launch (start us, length us, event | category | flops | bytes accessed | tf_op | source)
XLA Modules:
  0.0 86.6 jit_solution(11459875112853743563)
XLA Ops:
  0.6 0.0 copy-start.3
  0.6 0.0 copy-start.4
  0.7 0.8 copy-done.4
  1.4 0.0 copy-start.11
  1.4 0.0 copy-start.12
  1.4 0.0 copy-start.13
  1.5 0.0 copy-start.14
  1.5 0.0 copy-start.15
  1.5 0.0 copy-start.16
  1.5 18.3 %all_to_all.25.own = bf16[16,2,4096]{2,1,0:T(2,128)(2,1)S(1)} all-to-all(bf16[16,2,4096]{2,1,0:T(2,128)(2,1)S(1)} %share.1), channel_id=1, replica_groups=mesh['ep'=16,'tp'=2] {'ep'}, dimensions={0} | all-to-all | bytes 524288 | tf_op jit(solution)/shard_map/all_to_all | solution.py:32
  19.8 0.0 collective-permute-start
  19.8 0.0 copy-done.3
  19.8 0.3 front.1
  20.2 1.0 %gates.1 = (f32[4,4]{1,0:T(4,128)}, f32[4,4]{1,0:T(4,128)S(1)}, f32[4,4]{1,0:T(4,128)S(1)}, f32[4,4]{1,0:T(4,128)S(1)}, f32[2,16]{1,0:T(2,128)S(1)}) custom-call(bf16[4,4096]{1,0:T(4,128)(2,1)S(1)} %copy-done.4, f32[1,4096]{1,0:T(1,128)S(1)} %bitcast.22, bf16[4,4096]{1,0:T(4,128)(2,1)S(1)} %bitcast.24, bf16[4,4096]{1,0:T(4,128)(2,1)S(1)} %bitcast.25, ...), custom_call_target="tpu_custom_call" | custom-call | flops 1000000 | bytes 1000000 | tf_op jit(solution)/shard_map/gates/pallas_call | solution.py:40
  21.1 0.2 collective-permute-done.other
  21.3 0.0 copy-done.14
  21.3 0.0 copy-done.16
  21.4 0.0 slice-start.1
  21.4 0.0 copy-start.7
  21.4 1.4 %project.1 = bf16[16,4,384]{2,1,0:T(4,128)(2,1)S(1)} custom-call(bf16[32,4096]{1,0:T(8,128)(2,1)S(1)} %get-tuple-element.24.after.own, bf16[16,2,4096]{2,1,0:T(2,128)(2,1)S(1)} %collective-permute-done.other, f32[1,4096]{1,0:T(1,128)S(1)} %bitcast.23, bf16[64,4096]{1,0:T(8,128)(2,1)S(1)} %bitcast.32, bf16[64,4096]{1,0:T(8,128)(2,1)S(1)} %bitcast.33, ...), custom_call_target="tpu_custom_call" | custom-call | flops 99999997952 | bytes 1000000 | tf_op jit(solution)/shard_map/project/pallas_call | solution.py:40
  22.8 11.1 %all_to_all.26.pieces = bf16[16,4,384]{2,1,0:T(4,128)(2,1)S(1)} all-to-all(bf16[16,4,384]{2,1,0:T(4,128)(2,1)S(1)} %project.1), channel_id=1, replica_groups=mesh['ep'=16,'tp'=2] {'ep'}, dimensions={0} | all-to-all | bytes 98304 | tf_op jit(solution)/shard_map/all_to_all | solution.py:32
  33.8 0.0 slice-done.1
  33.8 3.4 %readout.1 = (bf16[16,4,2048]{2,1,0:T(4,128)(2,1)}, f32[4,4,256]{2,1,0:T(4,128)}, f32[32,256]{1,0:T(8,128)S(1)}, f32[4,2048]{1,0:T(4,128)S(1)}) custom-call(bf16[16,4,384]{2,1,0:T(4,128)(2,1)S(1)} %all_to_all.26.pieces, f32[4,4]{1,0:T(4,128)S(1)} %get-tuple-element.26.decay, f32[4,4]{1,0:T(4,128)S(1)} %get-tuple-element.27.inweight, ...), custom_call_target="tpu_custom_call" | custom-call | flops 4194304 | bytes 1000000 | tf_op jit(solution)/shard_map/readout/pallas_call | solution.py:40
  37.2 3.5 %all-to-all-start.2 = ((bf16[16,4,2048]{2,1,0:T(4,128)(2,1)}), bf16[16,4,2048]{2,1,0:T(4,128)(2,1)S(1)}, u32[]{:S(2)}, u32[]{:S(2)}) async-start(bf16[16,4,2048]{2,1,0:T(4,128)(2,1)} %get-tuple-element.29), calls=%async_computation.2 | async-start | bytes 524288 | tf_op jit(solution)/shard_map/all_to_all | solution.py:32
  40.8 6.7 %update.1 = (f32[4,4,256,512]{3,2,1,0:T(8,128)}, bf16[2048,256]{1,0:T(8,128)(2,1)S(1)}) custom-call(f32[32,256]{1,0:T(8,128)S(1)} %get-tuple-element.30.key, f32[4,2048]{1,0:T(4,128)S(1)} %get-tuple-element.31.value, f32[4,4]{1,0:T(4,128)S(1)} %get-tuple-element.26.decay, f32[4,4]{1,0:T(4,128)S(1)} %get-tuple-element.27.inweight, bf16[2048,256]{1,0:T(8,128)(2,1)} %w_out.1, ...), custom_call_target="tpu_custom_call" | custom-call | flops 100000000 | bytes 1000000 | tf_op jit(solution)/shard_map/update/pallas_call | solution.py:40
  47.5 2.4 %all-to-all-done.2 = bf16[16,4,2048]{2,1,0:T(4,128)(2,1)S(1)} async-done(((bf16[16,4,2048]{2,1,0:T(4,128)(2,1)}), bf16[16,4,2048]{2,1,0:T(4,128)(2,1)S(1)}, u32[]{:S(2)}, u32[]{:S(2)}) %all-to-all-start.2) | async-done | bytes 262176 | tf_op jit(solution)/shard_map/all_to_all | solution.py:32
  49.9 0.1 reshape.41.hidden
  50.0 0.0 copy-start.8
  50.0 0.0 copy-start
  50.0 0.0 copy-start.1
  50.0 0.0 copy-start.2
  50.0 0.4 output.1
  50.4 0.0 collective-permute-start.1
  50.4 1.2 %collective-permute-done.1 = bf16[32,256]{1,0:T(8,128)(2,1)S(1)} collective-permute-done((bf16[32,256]{1,0:T(8,128)(2,1)S(1)}, bf16[32,256]{1,0:T(8,128)(2,1)S(1)}, u32[]{:S(2)}, u32[]{:S(2)}) %collective-permute-start.1) | collective-permute-done | bytes 16416 | tf_op jit(solution)/shard_map/ppermute | solution.py:411
  51.7 14.4 %all_to_all.27.mixed = bf16[16,32,256]{2,1,0:T(8,128)(2,1)S(1)} all-to-all(bf16[16,32,256]{2,1,0:T(8,128)(2,1)S(1)} %broadcast_in_dim.2), channel_id=1, replica_groups=mesh['ep'=16,'tp'=2] {'ep'}, dimensions={0} | all-to-all | bytes 524288 | tf_op jit(solution)/shard_map/all_to_all | solution.py:32
  66.1 0.2 resid.1
  66.3 0.1 collective-permute-start.2
  66.4 1.5 %collective-permute-done.2.other = bf16[32,4096]{1,0:T(8,128)(2,1)S(1)} collective-permute-done((bf16[32,4096]{1,0:T(8,128)(2,1)S(1)}, bf16[32,4096]{1,0:T(8,128)(2,1)S(1)}, u32[]{:S(2)}, u32[]{:S(2)}) %collective-permute-start.2) | collective-permute-done | bytes 262176 | tf_op jit(solution)/shard_map/ppermute | solution.py:422
  67.9 1.3 %experts.1 = (bf16[32,256]{1,0:T(8,128)(2,1)S(1)}, bf16[32,4096]{1,0:T(8,128)(2,1)S(1)}) custom-call(bf16[32,4096]{1,0:T(8,128)(2,1)S(1)} %get-tuple-element.35.own, bf16[32,4096]{1,0:T(8,128)(2,1)S(1)} %collective-permute-done.2.other, bf16[1,4096,256]{2,1,0:T(8,128)(2,1)S(1)} %copy-done.1, bf16[1,4096,256]{2,1,0:T(8,128)(2,1)S(1)} %copy-done.2, ...), custom_call_target="tpu_custom_call" | custom-call | flops 201326592 | bytes 1000000 | tf_op jit(solution)/shard_map/experts/pallas_call | solution.py:40
  69.2 0.2 collective-permute-start.3
  69.4 0.5 down.1.own
  69.8 0.9 %collective-permute-done.3.other = bf16[32,4096]{1,0:T(8,128)(2,1)S(1)} collective-permute-done((bf16[32,4096]{1,0:T(8,128)(2,1)S(1)}, bf16[32,4096]{1,0:T(8,128)(2,1)S(1)}, u32[]{:S(2)}, u32[]{:S(2)}) %collective-permute-start.3) | collective-permute-done | bytes 262176 | tf_op jit(solution)/shard_map/ppermute | solution.py:441
  70.8 0.1 join.1
  70.9 13.5 %all_to_all.28.terms = bf16[16,2,4096]{2,1,0:T(2,128)(2,1)S(1)} all-to-all(bf16[16,2,4096]{2,1,0:T(2,128)(2,1)S(1)} %join.1), channel_id=1, replica_groups=mesh['ep'=16,'tp'=2] {'ep'}, dimensions={0} | all-to-all | bytes 524288 | tf_op jit(solution)/shard_map/all_to_all | solution.py:32
  84.4 0.3 finish.1.mine
  84.7 0.1 collective-permute-start.4
  84.8 1.2 %collective-permute-done.4.other = bf16[2,4096]{1,0:T(2,128)(2,1)S(1)} collective-permute-done((bf16[2,4096]{1,0:T(2,128)(2,1)S(1)}, bf16[2,4096]{1,0:T(2,128)(2,1)S(1)}, u32[]{:S(2)}, u32[]{:S(2)}) %collective-permute-start.4) | collective-permute-done | bytes 16416 | tf_op jit(solution)/shard_map/ppermute | solution.py:454
  86.0 0.6 merge.1
  (23 shorter events, 0.1 us)
Async XLA Ops:
  0.6 19.2 %copy-start.3 = (f32[4096]{0:T(1024)S(1)}, f32[4096]{0:T(1024)}, u32[]{:S(2)}) copy-start(f32[4096]{0:T(1024)} %param.23) | copy-start | bytes 49156
  0.6 0.8 copy-start.4
  1.4 18.7 %copy-start.5 = (bf16[4096,4]{0,1:T(4,128)(2,1)S(1)}, bf16[4096,4]{0,1:T(4,128)(2,1)}, u32[]{:S(2)}) copy-start(bf16[4096,4]{0,1:T(4,128)(2,1)} %param.28) | copy-start | bytes 98308
  1.4 18.7 %copy-start.6 = (bf16[4096,4]{0,1:T(4,128)(2,1)S(1)}, bf16[4096,4]{0,1:T(4,128)(2,1)}, u32[]{:S(2)}) copy-start(bf16[4096,4]{0,1:T(4,128)(2,1)} %param.29) | copy-start | bytes 98308
  1.4 18.7 %copy-start.9 = (f32[4,4]{1,0:T(4,128)S(1)}, f32[4,4]{1,0:T(4,128)}, u32[]{:S(2)}) copy-start(f32[4,4]{1,0:T(4,128)} %stab.1) | copy-start | bytes 196
  1.4 18.7 %copy-start.10 = (s32[4,2]{0,1:T(2,128)S(1)}, s32[4,2]{0,1:T(2,128)}, u32[]{:S(2)}) copy-start(s32[4,2]{0,1:T(2,128)} %param.36) | copy-start | bytes 100
  1.4 18.7 %copy-start.11 = (f32[4,2]{0,1:T(2,128)S(1)}, f32[4,2]{0,1:T(2,128)}, u32[]{:S(2)}) copy-start(f32[4,2]{0,1:T(2,128)} %param.37) | copy-start | bytes 100
  1.4 18.7 %copy-start.12 = (f32[4]{0:T(128)S(1)}, f32[4]{0:T(128)}, u32[]{:S(2)}) copy-start(f32[4]{0:T(128)} %param.30) | copy-start | bytes 52
  1.4 19.9 %copy-start.13 = (bf16[4096,4,32]{0,2,1:T(8,128)(2,1)S(1)}, bf16[4096,4,32]{0,2,1:T(8,128)(2,1)}, u32[]{:S(2)}) copy-start(bf16[4096,4,32]{0,2,1:T(8,128)(2,1)} %param.26) | copy-start | bytes 3145732
  1.5 19.9 %copy-start.14 = (bf16[4096,4,32]{0,2,1:T(8,128)(2,1)S(1)}, bf16[4096,4,32]{0,2,1:T(8,128)(2,1)}, u32[]{:S(2)}) copy-start(bf16[4096,4,32]{0,2,1:T(8,128)(2,1)} %param.27) | copy-start | bytes 3145732
  1.5 19.9 %copy-start.15 = (bf16[4096,4,16]{0,2,1:T(8,128)(2,1)S(1)}, bf16[4096,4,16]{0,2,1:T(8,128)(2,1)}, u32[]{:S(2)}) copy-start(bf16[4096,4,16]{0,2,1:T(8,128)(2,1)} %param.24) | copy-start | bytes 1572868
  1.5 19.9 %copy-start.16 = (bf16[4096,4,16]{0,2,1:T(8,128)(2,1)S(1)}, bf16[4096,4,16]{0,2,1:T(8,128)(2,1)}, u32[]{:S(2)}) copy-start(bf16[4096,4,16]{0,2,1:T(8,128)(2,1)} %param.25) | copy-start | bytes 1572868
  19.8 1.5 %collective-permute-start = (bf16[16,2,4096]{2,1,0:T(2,128)(2,1)S(1)}, bf16[16,2,4096]{2,1,0:T(2,128)(2,1)S(1)}, u32[]{:S(2)}, u32[]{:S(2)}) collective-permute-start(bf16[16,2,4096]{2,1,0:T(2,128)(2,1)S(1)} %all_to_all.25.own), channel_id=1, source_target_pairs={{0,1},{1,0},{2,3},{3,2},{4,5},{5,4},{6,7},{7,6},{8,9},{9,8},{10,11... | collective-permute-start | bytes 786440 | tf_op jit(solution)/shard_map/ppermute | solution.py:325
  21.3 12.5 %slice-start = ((s8[8388608]{0:T(1024)(128)(4,1)}), s8[4194304]{0:T(1024)(128)(4,1)S(1)}, s32[]{:S(2)}) async-start(s8[8388608]{0:T(1024)(128)(4,1)} %bitcast.19), calls=%async_computation.5 | async-start | bytes 8388608
  21.4 12.5 %slice-start.1 = ((s8[8388608]{0:T(1024)(128)(4,1)}), s8[4194304]{0:T(1024)(128)(4,1)S(1)}, s32[]{:S(2)}) async-start(s8[8388608]{0:T(1024)(128)(4,1)} %bitcast.19), calls=%async_computation.6 | async-start | bytes 8388608
  21.4 12.5 %copy-start.7 = (f32[4,4,256]{2,1,0:T(4,128)S(1)}, f32[4,4,256]{2,1,0:T(4,128)}, u32[]{:S(2)}) copy-start(f32[4,4,256]{2,1,0:T(4,128)} %norm.1) | copy-start | bytes 49156
  37.2 12.7 %all-to-all-start.2 = ((bf16[16,4,2048]{2,1,0:T(4,128)(2,1)}), bf16[16,4,2048]{2,1,0:T(4,128)(2,1)S(1)}, u32[]{:S(2)}, u32[]{:S(2)}) async-start(bf16[16,4,2048]{2,1,0:T(4,128)(2,1)} %get-tuple-element.29), calls=%async_computation.2 | async-start | bytes 524288 | tf_op jit(solution)/shard_map/all_to_all | solution.py:32
  50.0 16.1 %copy-start.8 = (f32[4096]{0:T(1024)S(1)}, f32[4096]{0:T(1024)}, u32[]{:S(2)}) copy-start(f32[4096]{0:T(1024)} %param.32) | copy-start | bytes 49156
  50.0 17.9 %copy-start = (bf16[1,256,4096]{2,1,0:T(8,128)(2,1)S(1)}, bf16[1,256,4096]{2,1,0:T(8,128)(2,1)}, u32[]{:S(2)}) copy-start(bf16[1,256,4096]{2,1,0:T(8,128)(2,1)} %w_down.3) | copy-start | bytes 6291460
  50.0 17.9 %copy-start.1 = (bf16[1,4096,256]{2,1,0:T(8,128)(2,1)S(1)}, bf16[1,4096,256]{2,1,0:T(8,128)(2,1)}, u32[]{:S(2)}) copy-start(bf16[1,4096,256]{2,1,0:T(8,128)(2,1)} %w_gate.1) | copy-start | bytes 6291460
  50.0 17.9 %copy-start.2 = (bf16[1,4096,256]{2,1,0:T(8,128)(2,1)S(1)}, bf16[1,4096,256]{2,1,0:T(8,128)(2,1)}, u32[]{:S(2)}) copy-start(bf16[1,4096,256]{2,1,0:T(8,128)(2,1)} %w_up.1) | copy-start | bytes 6291460
  50.4 1.2 %collective-permute-start.1 = (bf16[32,256]{1,0:T(8,128)(2,1)S(1)}, bf16[32,256]{1,0:T(8,128)(2,1)S(1)}, u32[]{:S(2)}, u32[]{:S(2)}) collective-permute-start(bf16[32,256]{1,0:T(8,128)(2,1)S(1)} %get-tuple-element.34), channel_id=1, source_target_pairs={{0,1},{1,0},{2,3},{3,2},{4,5},{5,4},{6,7},{7,6},{8,9},{9,8},{10,11... | collective-permute-start | bytes 49160 | tf_op jit(solution)/shard_map/ppermute | solution.py:411
  66.3 1.6 %collective-permute-start.2 = (bf16[32,4096]{1,0:T(8,128)(2,1)S(1)}, bf16[32,4096]{1,0:T(8,128)(2,1)S(1)}, u32[]{:S(2)}, u32[]{:S(2)}) collective-permute-start(bf16[32,4096]{1,0:T(8,128)(2,1)S(1)} %get-tuple-element.35.own), channel_id=1, source_target_pairs={{0,1},{1,0},{2,3},{3,2},{4,5},{5,4},{6,7},{7,6},{8,9},{9,8},{10,11... | collective-permute-start | bytes 786440 | tf_op jit(solution)/shard_map/ppermute | solution.py:422
  69.2 1.6 %collective-permute-start.3 = (bf16[32,4096]{1,0:T(8,128)(2,1)S(1)}, bf16[32,4096]{1,0:T(8,128)(2,1)S(1)}, u32[]{:S(2)}, u32[]{:S(2)}) collective-permute-start(bf16[32,4096]{1,0:T(8,128)(2,1)S(1)} %get-tuple-element.37), channel_id=1, source_target_pairs={{0,1},{1,0},{2,3},{3,2},{4,5},{5,4},{6,7},{7,6},{8,9},{9,8},{10,11... | collective-permute-start | bytes 786440 | tf_op jit(solution)/shard_map/ppermute | solution.py:441
  84.7 1.2 %collective-permute-start.4 = (bf16[2,4096]{1,0:T(2,128)(2,1)S(1)}, bf16[2,4096]{1,0:T(2,128)(2,1)S(1)}, u32[]{:S(2)}, u32[]{:S(2)}) collective-permute-start(bf16[2,4096]{1,0:T(2,128)(2,1)S(1)} %finish.1.mine), channel_id=1, source_target_pairs={{0,1},{1,0},{2,3},{3,2},{4,5},{5,4},{6,7},{7,6},{8,9},{9,8},{10,11... | collective-permute-start | bytes 49160 | tf_op jit(solution)/shard_map/ppermute | solution.py:454

commit v5 on v4

--- a/solution.py
+++ b/solution.py
@@ -133,7 +133,9 @@
     value_out,
     recalled,
     hidden,
+    norm_new,
     out_sems,
+    norm_sems,
     *,
     piece,
 ):
@@ -165,15 +167,16 @@
         w = inweight[:, h : h + 1]
         new = decay[:, h : h + 1] * old + w * k
         for i in range(seqs):
-            norm_out[i, h : h + 1] = new[i : i + 1]
+            norm_new[i, h : h + 1] = new[i : i + 1]
         below.append(jnp.maximum(jnp.abs(jnp.sum(q * new, axis=1, keepdims=True)), floor[:, h : h + 1]))
         along.append(w * jnp.sum(q * k, axis=1, keepdims=True))
+    backs = fetch([(norm_new, norm_out)], norm_sems)
     gate = jax.nn.sigmoid(outgate)
     for h in range(heads):
         at = slice(h * dv, (h + 1) * dv)
         top = decay[:, h : h + 1] * recalled[:, at] + along[h] * value[:, at]
         hidden[:, at] = (top / below[h] * gate[:, at]).astype(BF16)
-    for c in fetch([(hidden, out.at[e]) for e in range(out.shape[0])], out_sems):
+    for c in fetch([(hidden, out.at[e]) for e in range(out.shape[0])], out_sems) + backs:
         c.wait()
 
 
@@ -367,7 +370,7 @@
         functools.partial(readout_kernel, piece=(key_piece, value_piece)),
         (
             pltpu.HBM((n_ep, seqs, value_width), BF16),
-            shape(normalizer.shape, F32),
+            pltpu.HBM(normalizer.shape, F32),
             shape((heads * 8, key_size), F32),
             shape((seqs, value_width), F32),
         ),
@@ -375,12 +378,14 @@
         [
             pltpu.VMEM((seqs, value_width), F32),
             pltpu.VMEM((seqs, value_width), BF16),
+            pltpu.VMEM(normalizer.shape, F32),
             pltpu.SemaphoreType.DMA((n_ep,)),
+            pltpu.SemaphoreType.DMA((1,)),
         ],
         [pieces, decay, inweight, floor, normalizer, memory],
         "readout",
         flops=2 * memory.size,
-        outs=(HBM, VMEM, VMEM, VMEM),
+        outs=(HBM, HBM, VMEM, VMEM),
     )
     hidden_all = to_all(hidden).reshape(n_ep * seqs, value_width)
     memory_next, w_out_near = call(

time: 87 us -> 86.4 us (level)
  no operation moved by 1% of the time
where the time goes in v5:
time: 86.4 us; the launch traced here: 86 us
  blocking collectives  57.3 us (66%)
  Pallas kernels  15.5 us (18%)
  waiting for transfers between devices  7.49 us (9%)
  starting transfers between devices  3.87 us (4%)
  between operations  0.94 us (1%)
  local copies, waits for them, and re-layouts  0.92 us (1%)
    all_to_all x4, blocking collectives, to_all(): return lax.all_to_all(copies, 'ep', split_axis=0, concat_axis=0, tiled=True)  57.3 us
    pallas_call x13, Pallas kernels, call(): pl.pallas_call(kernel, out_shape=out_shape, in_specs=in_specs, out_specs=...  15.5 us
    all_to_all x1, starting transfers between devices, to_all(): return lax.all_to_all(copies, 'ep', split_axis=0, concat_axis=0, tiled=True)  3.54 us
    all_to_all x1, waiting for transfers between devices, to_all(): return lax.all_to_all(copies, 'ep', split_axis=0, concat_axis=0, tiled=True)  2.44 us
  transfers between devices with their start and end apart: 6, of which 6 were waited for; matrix products, arithmetic and copies ran while one was open for 0% of the time, Pallas kernels for 10%

profile of v5, /device:TPU:0, one launch (start us, length us, event | category | flops | bytes accessed | tf_op | source)
XLA Modules:
  0.0 86.0 jit_solution(14891393680599697572)
XLA Ops:
  0.6 0.0 copy-start.3
  0.6 0.0 copy-start.4
  0.7 0.8 copy-done.4
  1.4 0.0 copy-start.11
  1.4 0.0 copy-start.12
  1.4 0.0 copy-start.13
  1.5 0.0 copy-start.14
  1.5 0.0 copy-start.15
  1.5 0.0 copy-start.16
  1.5 18.3 %all_to_all.25.own = bf16[16,2,4096]{2,1,0:T(2,128)(2,1)S(1)} all-to-all(bf16[16,2,4096]{2,1,0:T(2,128)(2,1)S(1)} %share.1), channel_id=1, replica_groups=mesh['ep'=16,'tp'=2] {'ep'}, dimensions={0} | all-to-all | bytes 524288 | tf_op jit(solution)/shard_map/all_to_all | solution.py:32
  19.8 0.0 collective-permute-start
  19.8 0.3 front.1
  20.2 1.0 %gates.1 = (f32[4,4]{1,0:T(4,128)}, f32[4,4]{1,0:T(4,128)S(1)}, f32[4,4]{1,0:T(4,128)S(1)}, f32[4,4]{1,0:T(4,128)S(1)}, f32[2,16]{1,0:T(2,128)S(1)}) custom-call(bf16[4,4096]{1,0:T(4,128)(2,1)S(1)} %copy-done.4, f32[1,4096]{1,0:T(1,128)S(1)} %bitcast.22, bf16[4,4096]{1,0:T(4,128)(2,1)S(1)} %bitcast.24, bf16[4,4096]{1,0:T(4,128)(2,1)S(1)} %bitcast.25, ...), custom_call_target="tpu_custom_call" | custom-call | flops 1000000 | bytes 1000000 | tf_op jit(solution)/shard_map/gates/pallas_call | solution.py:40
  21.1 0.2 collective-permute-done.other
  21.3 0.0 copy-done.14
  21.3 0.0 copy-done.16
  21.4 0.0 slice-start.1
  21.4 0.0 copy-start.7
  21.4 1.4 %project.1 = bf16[16,4,384]{2,1,0:T(4,128)(2,1)S(1)} custom-call(bf16[32,4096]{1,0:T(8,128)(2,1)S(1)} %get-tuple-element.24.after.own, bf16[16,2,4096]{2,1,0:T(2,128)(2,1)S(1)} %collective-permute-done.other, f32[1,4096]{1,0:T(1,128)S(1)} %bitcast.23, bf16[64,4096]{1,0:T(8,128)(2,1)S(1)} %bitcast.32, bf16[64,4096]{1,0:T(8,128)(2,1)S(1)} %bitcast.33, ...), custom_call_target="tpu_custom_call" | custom-call | flops 99999997952 | bytes 1000000 | tf_op jit(solution)/shard_map/project/pallas_call | solution.py:40
  22.8 11.1 %all_to_all.26.pieces = bf16[16,4,384]{2,1,0:T(4,128)(2,1)S(1)} all-to-all(bf16[16,4,384]{2,1,0:T(4,128)(2,1)S(1)} %project.1), channel_id=1, replica_groups=mesh['ep'=16,'tp'=2] {'ep'}, dimensions={0} | all-to-all | bytes 98304 | tf_op jit(solution)/shard_map/all_to_all | solution.py:32
  33.8 0.0 slice-done.1
  33.8 2.8 %readout.1 = (bf16[16,4,2048]{2,1,0:T(4,128)(2,1)}, f32[4,4,256]{2,1,0:T(4,128)}, f32[32,256]{1,0:T(8,128)S(1)}, f32[4,2048]{1,0:T(4,128)S(1)}) custom-call(bf16[16,4,384]{2,1,0:T(4,128)(2,1)S(1)} %all_to_all.26.pieces, f32[4,4]{1,0:T(4,128)S(1)} %get-tuple-element.26.decay, f32[4,4]{1,0:T(4,128)S(1)} %get-tuple-element.27.inweight, ...), custom_call_target="tpu_custom_call" | custom-call | flops 4194304 | bytes 1000000 | tf_op jit(solution)/shard_map/readout/pallas_call | solution.py:40
  36.6 3.5 %all-to-all-start.2 = ((bf16[16,4,2048]{2,1,0:T(4,128)(2,1)}), bf16[16,4,2048]{2,1,0:T(4,128)(2,1)S(1)}, u32[]{:S(2)}, u32[]{:S(2)}) async-start(bf16[16,4,2048]{2,1,0:T(4,128)(2,1)} %get-tuple-element.29), calls=%async_computation.2 | async-start | bytes 524288 | tf_op jit(solution)/shard_map/all_to_all | solution.py:32
  40.2 6.7 %update.1 = (f32[4,4,256,512]{3,2,1,0:T(8,128)}, bf16[2048,256]{1,0:T(8,128)(2,1)S(1)}) custom-call(f32[32,256]{1,0:T(8,128)S(1)} %get-tuple-element.30.key, f32[4,2048]{1,0:T(4,128)S(1)} %get-tuple-element.31.value, f32[4,4]{1,0:T(4,128)S(1)} %get-tuple-element.26.decay, f32[4,4]{1,0:T(4,128)S(1)} %get-tuple-element.27.inweight, bf16[2048,256]{1,0:T(8,128)(2,1)} %w_out.1, ...), custom_call_target="tpu_custom_call" | custom-call | flops 100000000 | bytes 1000000 | tf_op jit(solution)/shard_map/update/pallas_call | solution.py:40
  46.9 2.4 %all-to-all-done.2 = bf16[16,4,2048]{2,1,0:T(4,128)(2,1)S(1)} async-done(((bf16[16,4,2048]{2,1,0:T(4,128)(2,1)}), bf16[16,4,2048]{2,1,0:T(4,128)(2,1)S(1)}, u32[]{:S(2)}, u32[]{:S(2)}) %all-to-all-start.2) | async-done | bytes 262176 | tf_op jit(solution)/shard_map/all_to_all | solution.py:32
  49.3 0.1 reshape.41.hidden
  49.4 0.0 copy-start.8
  49.4 0.0 copy-start
  49.4 0.0 copy-start.1
  49.4 0.0 copy-start.2
  49.4 0.4 output.1
  49.8 0.0 collective-permute-start.1
  49.8 1.2 %collective-permute-done.1 = bf16[32,256]{1,0:T(8,128)(2,1)S(1)} collective-permute-done((bf16[32,256]{1,0:T(8,128)(2,1)S(1)}, bf16[32,256]{1,0:T(8,128)(2,1)S(1)}, u32[]{:S(2)}, u32[]{:S(2)}) %collective-permute-start.1) | collective-permute-done | bytes 16416 | tf_op jit(solution)/shard_map/ppermute | solution.py:416
  51.1 14.4 %all_to_all.27.mixed = bf16[16,32,256]{2,1,0:T(8,128)(2,1)S(1)} all-to-all(bf16[16,32,256]{2,1,0:T(8,128)(2,1)S(1)} %broadcast_in_dim.2), channel_id=1, replica_groups=mesh['ep'=16,'tp'=2] {'ep'}, dimensions={0} | all-to-all | bytes 524288 | tf_op jit(solution)/shard_map/all_to_all | solution.py:32
  65.5 0.2 resid.1
  65.7 0.1 collective-permute-start.2
  65.8 1.5 %collective-permute-done.2.other = bf16[32,4096]{1,0:T(8,128)(2,1)S(1)} collective-permute-done((bf16[32,4096]{1,0:T(8,128)(2,1)S(1)}, bf16[32,4096]{1,0:T(8,128)(2,1)S(1)}, u32[]{:S(2)}, u32[]{:S(2)}) %collective-permute-start.2) | collective-permute-done | bytes 262176 | tf_op jit(solution)/shard_map/ppermute | solution.py:427
  67.3 0.0 copy-done
  67.3 1.3 %experts.1 = (bf16[32,256]{1,0:T(8,128)(2,1)S(1)}, bf16[32,4096]{1,0:T(8,128)(2,1)S(1)}) custom-call(bf16[32,4096]{1,0:T(8,128)(2,1)S(1)} %get-tuple-element.35.own, bf16[32,4096]{1,0:T(8,128)(2,1)S(1)} %collective-permute-done.2.other, bf16[1,4096,256]{2,1,0:T(8,128)(2,1)S(1)} %copy-done.1, bf16[1,4096,256]{2,1,0:T(8,128)(2,1)S(1)} %copy-done.2, ...), custom_call_target="tpu_custom_call" | custom-call | flops 201326592 | bytes 1000000 | tf_op jit(solution)/shard_map/experts/pallas_call | solution.py:40
  68.6 0.2 collective-permute-start.3
  68.8 0.5 down.1.own
  69.2 0.9 %collective-permute-done.3.other = bf16[32,4096]{1,0:T(8,128)(2,1)S(1)} collective-permute-done((bf16[32,4096]{1,0:T(8,128)(2,1)S(1)}, bf16[32,4096]{1,0:T(8,128)(2,1)S(1)}, u32[]{:S(2)}, u32[]{:S(2)}) %collective-permute-start.3) | collective-permute-done | bytes 262176 | tf_op jit(solution)/shard_map/ppermute | solution.py:446
  70.2 0.1 join.1
  70.3 13.5 %all_to_all.28.terms = bf16[16,2,4096]{2,1,0:T(2,128)(2,1)S(1)} all-to-all(bf16[16,2,4096]{2,1,0:T(2,128)(2,1)S(1)} %join.1), channel_id=1, replica_groups=mesh['ep'=16,'tp'=2] {'ep'}, dimensions={0} | all-to-all | bytes 524288 | tf_op jit(solution)/shard_map/all_to_all | solution.py:32
  83.8 0.3 finish.1.mine
  84.1 0.1 collective-permute-start.4
  84.2 1.2 %collective-permute-done.4.other = bf16[2,4096]{1,0:T(2,128)(2,1)S(1)} collective-permute-done((bf16[2,4096]{1,0:T(2,128)(2,1)S(1)}, bf16[2,4096]{1,0:T(2,128)(2,1)S(1)}, u32[]{:S(2)}, u32[]{:S(2)}) %collective-permute-start.4) | collective-permute-done | bytes 16416 | tf_op jit(solution)/shard_map/ppermute | solution.py:459
  85.4 0.6 merge.1
  (23 shorter events, 0.1 us)
Async XLA Ops:
  0.6 19.2 %copy-start.3 = (f32[4096]{0:T(1024)S(1)}, f32[4096]{0:T(1024)}, u32[]{:S(2)}) copy-start(f32[4096]{0:T(1024)} %param.23) | copy-start | bytes 49156
  0.6 0.8 copy-start.4
  1.4 18.7 %copy-start.5 = (bf16[4096,4]{0,1:T(4,128)(2,1)S(1)}, bf16[4096,4]{0,1:T(4,128)(2,1)}, u32[]{:S(2)}) copy-start(bf16[4096,4]{0,1:T(4,128)(2,1)} %param.28) | copy-start | bytes 98308
  1.4 18.7 %copy-start.6 = (bf16[4096,4]{0,1:T(4,128)(2,1)S(1)}, bf16[4096,4]{0,1:T(4,128)(2,1)}, u32[]{:S(2)}) copy-start(bf16[4096,4]{0,1:T(4,128)(2,1)} %param.29) | copy-start | bytes 98308
  1.4 18.7 %copy-start.9 = (f32[4,4]{1,0:T(4,128)S(1)}, f32[4,4]{1,0:T(4,128)}, u32[]{:S(2)}) copy-start(f32[4,4]{1,0:T(4,128)} %stab.1) | copy-start | bytes 196
  1.4 18.7 %copy-start.10 = (s32[4,2]{0,1:T(2,128)S(1)}, s32[4,2]{0,1:T(2,128)}, u32[]{:S(2)}) copy-start(s32[4,2]{0,1:T(2,128)} %param.36) | copy-start | bytes 100
  1.4 18.7 %copy-start.11 = (f32[4,2]{0,1:T(2,128)S(1)}, f32[4,2]{0,1:T(2,128)}, u32[]{:S(2)}) copy-start(f32[4,2]{0,1:T(2,128)} %param.37) | copy-start | bytes 100
  1.4 18.7 %copy-start.12 = (f32[4]{0:T(128)S(1)}, f32[4]{0:T(128)}, u32[]{:S(2)}) copy-start(f32[4]{0:T(128)} %param.30) | copy-start | bytes 52
  1.4 19.9 %copy-start.13 = (bf16[4096,4,32]{0,2,1:T(8,128)(2,1)S(1)}, bf16[4096,4,32]{0,2,1:T(8,128)(2,1)}, u32[]{:S(2)}) copy-start(bf16[4096,4,32]{0,2,1:T(8,128)(2,1)} %param.26) | copy-start | bytes 3145732
  1.5 19.9 %copy-start.14 = (bf16[4096,4,32]{0,2,1:T(8,128)(2,1)S(1)}, bf16[4096,4,32]{0,2,1:T(8,128)(2,1)}, u32[]{:S(2)}) copy-start(bf16[4096,4,32]{0,2,1:T(8,128)(2,1)} %param.27) | copy-start | bytes 3145732
  1.5 19.9 %copy-start.15 = (bf16[4096,4,16]{0,2,1:T(8,128)(2,1)S(1)}, bf16[4096,4,16]{0,2,1:T(8,128)(2,1)}, u32[]{:S(2)}) copy-start(bf16[4096,4,16]{0,2,1:T(8,128)(2,1)} %param.24) | copy-start | bytes 1572868
  1.5 19.9 %copy-start.16 = (bf16[4096,4,16]{0,2,1:T(8,128)(2,1)S(1)}, bf16[4096,4,16]{0,2,1:T(8,128)(2,1)}, u32[]{:S(2)}) copy-start(bf16[4096,4,16]{0,2,1:T(8,128)(2,1)} %param.25) | copy-start | bytes 1572868
  19.8 1.5 %collective-permute-start = (bf16[16,2,4096]{2,1,0:T(2,128)(2,1)S(1)}, bf16[16,2,4096]{2,1,0:T(2,128)(2,1)S(1)}, u32[]{:S(2)}, u32[]{:S(2)}) collective-permute-start(bf16[16,2,4096]{2,1,0:T(2,128)(2,1)S(1)} %all_to_all.25.own), channel_id=1, source_target_pairs={{0,1},{1,0},{2,3},{3,2},{4,5},{5,4},{6,7},{7,6},{8,9},{9,8},{10,11... | collective-permute-start | bytes 786440 | tf_op jit(solution)/shard_map/ppermute | solution.py:328
  21.3 12.5 %slice-start = ((s8[8388608]{0:T(1024)(128)(4,1)}), s8[4194304]{0:T(1024)(128)(4,1)S(1)}, s32[]{:S(2)}) async-start(s8[8388608]{0:T(1024)(128)(4,1)} %bitcast.19), calls=%async_computation.5 | async-start | bytes 8388608
  21.4 12.5 %slice-start.1 = ((s8[8388608]{0:T(1024)(128)(4,1)}), s8[4194304]{0:T(1024)(128)(4,1)S(1)}, s32[]{:S(2)}) async-start(s8[8388608]{0:T(1024)(128)(4,1)} %bitcast.19), calls=%async_computation.6 | async-start | bytes 8388608
  21.4 12.5 %copy-start.7 = (f32[4,4,256]{2,1,0:T(4,128)S(1)}, f32[4,4,256]{2,1,0:T(4,128)}, u32[]{:S(2)}) copy-start(f32[4,4,256]{2,1,0:T(4,128)} %norm.1) | copy-start | bytes 49156
  36.6 12.7 %all-to-all-start.2 = ((bf16[16,4,2048]{2,1,0:T(4,128)(2,1)}), bf16[16,4,2048]{2,1,0:T(4,128)(2,1)S(1)}, u32[]{:S(2)}, u32[]{:S(2)}) async-start(bf16[16,4,2048]{2,1,0:T(4,128)(2,1)} %get-tuple-element.29), calls=%async_computation.2 | async-start | bytes 524288 | tf_op jit(solution)/shard_map/all_to_all | solution.py:32
  49.4 16.1 %copy-start.8 = (f32[4096]{0:T(1024)S(1)}, f32[4096]{0:T(1024)}, u32[]{:S(2)}) copy-start(f32[4096]{0:T(1024)} %param.32) | copy-start | bytes 49156
  49.4 17.9 %copy-start = (bf16[1,256,4096]{2,1,0:T(8,128)(2,1)S(1)}, bf16[1,256,4096]{2,1,0:T(8,128)(2,1)}, u32[]{:S(2)}) copy-start(bf16[1,256,4096]{2,1,0:T(8,128)(2,1)} %w_down.3) | copy-start | bytes 6291460
  49.4 17.9 %copy-start.1 = (bf16[1,4096,256]{2,1,0:T(8,128)(2,1)S(1)}, bf16[1,4096,256]{2,1,0:T(8,128)(2,1)}, u32[]{:S(2)}) copy-start(bf16[1,4096,256]{2,1,0:T(8,128)(2,1)} %w_gate.1) | copy-start | bytes 6291460
  49.4 17.9 %copy-start.2 = (bf16[1,4096,256]{2,1,0:T(8,128)(2,1)S(1)}, bf16[1,4096,256]{2,1,0:T(8,128)(2,1)}, u32[]{:S(2)}) copy-start(bf16[1,4096,256]{2,1,0:T(8,128)(2,1)} %w_up.1) | copy-start | bytes 6291460
  49.8 1.2 %collective-permute-start.1 = (bf16[32,256]{1,0:T(8,128)(2,1)S(1)}, bf16[32,256]{1,0:T(8,128)(2,1)S(1)}, u32[]{:S(2)}, u32[]{:S(2)}) collective-permute-start(bf16[32,256]{1,0:T(8,128)(2,1)S(1)} %get-tuple-element.34), channel_id=1, source_target_pairs={{0,1},{1,0},{2,3},{3,2},{4,5},{5,4},{6,7},{7,6},{8,9},{9,8},{10,11... | collective-permute-start | bytes 49160 | tf_op jit(solution)/shard_map/ppermute | solution.py:416
  65.7 1.6 %collective-permute-start.2 = (bf16[32,4096]{1,0:T(8,128)(2,1)S(1)}, bf16[32,4096]{1,0:T(8,128)(2,1)S(1)}, u32[]{:S(2)}, u32[]{:S(2)}) collective-permute-start(bf16[32,4096]{1,0:T(8,128)(2,1)S(1)} %get-tuple-element.35.own), channel_id=1, source_target_pairs={{0,1},{1,0},{2,3},{3,2},{4,5},{5,4},{6,7},{7,6},{8,9},{9,8},{10,11... | collective-permute-start | bytes 786440 | tf_op jit(solution)/shard_map/ppermute | solution.py:427
  68.6 1.6 %collective-permute-start.3 = (bf16[32,4096]{1,0:T(8,128)(2,1)S(1)}, bf16[32,4096]{1,0:T(8,128)(2,1)S(1)}, u32[]{:S(2)}, u32[]{:S(2)}) collective-permute-start(bf16[32,4096]{1,0:T(8,128)(2,1)S(1)} %get-tuple-element.37), channel_id=1, source_target_pairs={{0,1},{1,0},{2,3},{3,2},{4,5},{5,4},{6,7},{7,6},{8,9},{9,8},{10,11... | collective-permute-start | bytes 786440 | tf_op jit(solution)/shard_map/ppermute | solution.py:446
  84.1 1.2 %collective-permute-start.4 = (bf16[2,4096]{1,0:T(2,128)(2,1)S(1)}, bf16[2,4096]{1,0:T(2,128)(2,1)S(1)}, u32[]{:S(2)}, u32[]{:S(2)}) collective-permute-start(bf16[2,4096]{1,0:T(2,128)(2,1)S(1)} %finish.1.mine), channel_id=1, source_target_pairs={{0,1},{1,0},{2,3},{3,2},{4,5},{5,4},{6,7},{7,6},{8,9},{9,8},{10,11... | collective-permute-start | bytes 49160 | tf_op jit(solution)/shard_map/ppermute | solution.py:459

commit v6 on v5

--- a/solution.py
+++ b/solution.py
@@ -153,9 +153,6 @@
         part = jnp.sum(cell * columns[:, n : n + 1], axis=0, keepdims=True)
         recalled[i : i + 1, h * dv : (h + 1) * dv] = part
 
-    for i in range(seqs):
-        for h in range(heads):
-            recall(memory[i, h], i, h)
     value = spread(rows, 2 * heads * small, large, heads, seqs)[0:seqs]
     outgate = spread(rows, 2 * heads * small + heads * large, large, heads, seqs)[0:seqs]
     value_out[...] = value
@@ -172,6 +169,9 @@
         along.append(w * jnp.sum(q * k, axis=1, keepdims=True))
     backs = fetch([(norm_new, norm_out)], norm_sems)
     gate = jax.nn.sigmoid(outgate)
+    for i in range(seqs):
+        for h in range(heads):
+            recall(memory[i, h], i, h)
     for h in range(heads):
         at = slice(h * dv, (h + 1) * dv)
         top = decay[:, h : h + 1] * recalled[:, at] + along[h] * value[:, at]

time: 86.4 us -> 86.2 us (level)
  no operation moved by 1% of the time
where the time goes in v6:
time: 86.2 us; the launch traced here: 85.8 us
  blocking collectives  57.3 us (66%)
  Pallas kernels  15.2 us (18%)
  waiting for transfers between devices  7.49 us (9%)
  starting transfers between devices  3.87 us (4%)
  between operations  0.94 us (1%)
  local copies, waits for them, and re-layouts  0.92 us (1%)
    all_to_all x4, blocking collectives, to_all(): return lax.all_to_all(copies, 'ep', split_axis=0, concat_axis=0, tiled=True)  57.3 us
    pallas_call x13, Pallas kernels, call(): pl.pallas_call(kernel, out_shape=out_shape, in_specs=in_specs, out_specs=...  15.2 us
    all_to_all x1, starting transfers between devices, to_all(): return lax.all_to_all(copies, 'ep', split_axis=0, concat_axis=0, tiled=True)  3.54 us
    all_to_all x1, waiting for transfers between devices, to_all(): return lax.all_to_all(copies, 'ep', split_axis=0, concat_axis=0, tiled=True)  2.44 us
  transfers between devices with their start and end apart: 6, of which 6 were waited for; matrix products, arithmetic and copies ran while one was open for 0% of the time, Pallas kernels for 10%

profile of v6, /device:TPU:0, one launch (start us, length us, event | category | flops | bytes accessed | tf_op | source)
XLA Modules:
  0.0 85.8 jit_solution(189454442915295473)
XLA Ops:
  0.6 0.0 copy-start.3
  0.6 0.0 copy-start.4
  0.7 0.8 copy-done.4
  1.4 0.0 copy-start.11
  1.4 0.0 copy-start.12
  1.4 0.0 copy-start.13
  1.5 0.0 copy-start.14
  1.5 0.0 copy-start.15
  1.5 0.0 copy-start.16
  1.5 18.3 %all_to_all.25.own = bf16[16,2,4096]{2,1,0:T(2,128)(2,1)S(1)} all-to-all(bf16[16,2,4096]{2,1,0:T(2,128)(2,1)S(1)} %share.1), channel_id=1, replica_groups=mesh['ep'=16,'tp'=2] {'ep'}, dimensions={0} | all-to-all | bytes 524288 | tf_op jit(solution)/shard_map/all_to_all | solution.py:32
  19.8 0.0 collective-permute-start
  19.8 0.3 front.1
  20.2 1.0 %gates.1 = (f32[4,4]{1,0:T(4,128)}, f32[4,4]{1,0:T(4,128)S(1)}, f32[4,4]{1,0:T(4,128)S(1)}, f32[4,4]{1,0:T(4,128)S(1)}, f32[2,16]{1,0:T(2,128)S(1)}) custom-call(bf16[4,4096]{1,0:T(4,128)(2,1)S(1)} %copy-done.4, f32[1,4096]{1,0:T(1,128)S(1)} %bitcast.22, bf16[4,4096]{1,0:T(4,128)(2,1)S(1)} %bitcast.24, bf16[4,4096]{1,0:T(4,128)(2,1)S(1)} %bitcast.25, ...), custom_call_target="tpu_custom_call" | custom-call | flops 1000000 | bytes 1000000 | tf_op jit(solution)/shard_map/gates/pallas_call | solution.py:40
  21.1 0.2 collective-permute-done.other
  21.3 0.0 copy-done.14
  21.3 0.0 copy-done.16
  21.4 0.0 slice-start.1
  21.4 0.0 copy-start.7
  21.4 1.4 %project.1 = bf16[16,4,384]{2,1,0:T(4,128)(2,1)S(1)} custom-call(bf16[32,4096]{1,0:T(8,128)(2,1)S(1)} %get-tuple-element.24.after.own, bf16[16,2,4096]{2,1,0:T(2,128)(2,1)S(1)} %collective-permute-done.other, f32[1,4096]{1,0:T(1,128)S(1)} %bitcast.23, bf16[64,4096]{1,0:T(8,128)(2,1)S(1)} %bitcast.32, bf16[64,4096]{1,0:T(8,128)(2,1)S(1)} %bitcast.33, ...), custom_call_target="tpu_custom_call" | custom-call | flops 99999997952 | bytes 1000000 | tf_op jit(solution)/shard_map/project/pallas_call | solution.py:40
  22.8 11.1 %all_to_all.26.pieces = bf16[16,4,384]{2,1,0:T(4,128)(2,1)S(1)} all-to-all(bf16[16,4,384]{2,1,0:T(4,128)(2,1)S(1)} %project.1), channel_id=1, replica_groups=mesh['ep'=16,'tp'=2] {'ep'}, dimensions={0} | all-to-all | bytes 98304 | tf_op jit(solution)/shard_map/all_to_all | solution.py:32
  33.8 0.0 slice-done.1
  33.8 2.5 %readout.1 = (bf16[16,4,2048]{2,1,0:T(4,128)(2,1)}, f32[4,4,256]{2,1,0:T(4,128)}, f32[32,256]{1,0:T(8,128)S(1)}, f32[4,2048]{1,0:T(4,128)S(1)}) custom-call(bf16[16,4,384]{2,1,0:T(4,128)(2,1)S(1)} %all_to_all.26.pieces, f32[4,4]{1,0:T(4,128)S(1)} %get-tuple-element.26.decay, f32[4,4]{1,0:T(4,128)S(1)} %get-tuple-element.27.inweight, ...), custom_call_target="tpu_custom_call" | custom-call | flops 4194304 | bytes 1000000 | tf_op jit(solution)/shard_map/readout/pallas_call | solution.py:40
  36.3 3.5 %all-to-all-start.2 = ((bf16[16,4,2048]{2,1,0:T(4,128)(2,1)}), bf16[16,4,2048]{2,1,0:T(4,128)(2,1)S(1)}, u32[]{:S(2)}, u32[]{:S(2)}) async-start(bf16[16,4,2048]{2,1,0:T(4,128)(2,1)} %get-tuple-element.29), calls=%async_computation.2 | async-start | bytes 524288 | tf_op jit(solution)/shard_map/all_to_all | solution.py:32
  39.9 6.7 %update.1 = (f32[4,4,256,512]{3,2,1,0:T(8,128)}, bf16[2048,256]{1,0:T(8,128)(2,1)S(1)}) custom-call(f32[32,256]{1,0:T(8,128)S(1)} %get-tuple-element.30.key, f32[4,2048]{1,0:T(4,128)S(1)} %get-tuple-element.31.value, f32[4,4]{1,0:T(4,128)S(1)} %get-tuple-element.26.decay, f32[4,4]{1,0:T(4,128)S(1)} %get-tuple-element.27.inweight, bf16[2048,256]{1,0:T(8,128)(2,1)} %w_out.1, ...), custom_call_target="tpu_custom_call" | custom-call | flops 100000000 | bytes 1000000 | tf_op jit(solution)/shard_map/update/pallas_call | solution.py:40
  46.6 2.4 %all-to-all-done.2 = bf16[16,4,2048]{2,1,0:T(4,128)(2,1)S(1)} async-done(((bf16[16,4,2048]{2,1,0:T(4,128)(2,1)}), bf16[16,4,2048]{2,1,0:T(4,128)(2,1)S(1)}, u32[]{:S(2)}, u32[]{:S(2)}) %all-to-all-start.2) | async-done | bytes 262176 | tf_op jit(solution)/shard_map/all_to_all | solution.py:32
  49.0 0.1 reshape.41.hidden
  49.1 0.0 copy-start.8
  49.1 0.0 copy-start
  49.1 0.0 copy-start.1
  49.1 0.0 copy-start.2
  49.1 0.4 output.1
  49.5 0.0 collective-permute-start.1
  49.6 1.2 %collective-permute-done.1 = bf16[32,256]{1,0:T(8,128)(2,1)S(1)} collective-permute-done((bf16[32,256]{1,0:T(8,128)(2,1)S(1)}, bf16[32,256]{1,0:T(8,128)(2,1)S(1)}, u32[]{:S(2)}, u32[]{:S(2)}) %collective-permute-start.1) | collective-permute-done | bytes 16416 | tf_op jit(solution)/shard_map/ppermute | solution.py:416
  50.8 14.4 %all_to_all.27.mixed = bf16[16,32,256]{2,1,0:T(8,128)(2,1)S(1)} all-to-all(bf16[16,32,256]{2,1,0:T(8,128)(2,1)S(1)} %broadcast_in_dim.2), channel_id=1, replica_groups=mesh['ep'=16,'tp'=2] {'ep'}, dimensions={0} | all-to-all | bytes 524288 | tf_op jit(solution)/shard_map/all_to_all | solution.py:32
  65.2 0.2 resid.1
  65.4 0.1 collective-permute-start.2
  65.5 1.5 %collective-permute-done.2.other = bf16[32,4096]{1,0:T(8,128)(2,1)S(1)} collective-permute-done((bf16[32,4096]{1,0:T(8,128)(2,1)S(1)}, bf16[32,4096]{1,0:T(8,128)(2,1)S(1)}, u32[]{:S(2)}, u32[]{:S(2)}) %collective-permute-start.2) | collective-permute-done | bytes 262176 | tf_op jit(solution)/shard_map/ppermute | solution.py:427
  67.0 0.0 copy-done
  67.0 1.3 %experts.1 = (bf16[32,256]{1,0:T(8,128)(2,1)S(1)}, bf16[32,4096]{1,0:T(8,128)(2,1)S(1)}) custom-call(bf16[32,4096]{1,0:T(8,128)(2,1)S(1)} %get-tuple-element.35.own, bf16[32,4096]{1,0:T(8,128)(2,1)S(1)} %collective-permute-done.2.other, bf16[1,4096,256]{2,1,0:T(8,128)(2,1)S(1)} %copy-done.1, bf16[1,4096,256]{2,1,0:T(8,128)(2,1)S(1)} %copy-done.2, ...), custom_call_target="tpu_custom_call" | custom-call | flops 201326592 | bytes 1000000 | tf_op jit(solution)/shard_map/experts/pallas_call | solution.py:40
  68.3 0.2 collective-permute-start.3
  68.5 0.5 down.1.own
  69.0 0.9 %collective-permute-done.3.other = bf16[32,4096]{1,0:T(8,128)(2,1)S(1)} collective-permute-done((bf16[32,4096]{1,0:T(8,128)(2,1)S(1)}, bf16[32,4096]{1,0:T(8,128)(2,1)S(1)}, u32[]{:S(2)}, u32[]{:S(2)}) %collective-permute-start.3) | collective-permute-done | bytes 262176 | tf_op jit(solution)/shard_map/ppermute | solution.py:446
  69.9 0.1 join.1
  70.0 13.5 %all_to_all.28.terms = bf16[16,2,4096]{2,1,0:T(2,128)(2,1)S(1)} all-to-all(bf16[16,2,4096]{2,1,0:T(2,128)(2,1)S(1)} %join.1), channel_id=1, replica_groups=mesh['ep'=16,'tp'=2] {'ep'}, dimensions={0} | all-to-all | bytes 524288 | tf_op jit(solution)/shard_map/all_to_all | solution.py:32
  83.5 0.3 finish.1.mine
  83.9 0.1 collective-permute-start.4
  83.9 1.2 %collective-permute-done.4.other = bf16[2,4096]{1,0:T(2,128)(2,1)S(1)} collective-permute-done((bf16[2,4096]{1,0:T(2,128)(2,1)S(1)}, bf16[2,4096]{1,0:T(2,128)(2,1)S(1)}, u32[]{:S(2)}, u32[]{:S(2)}) %collective-permute-start.4) | collective-permute-done | bytes 16416 | tf_op jit(solution)/shard_map/ppermute | solution.py:459
  85.1 0.6 merge.1
  (23 shorter events, 0.1 us)
Async XLA Ops:
  0.6 19.2 %copy-start.3 = (f32[4096]{0:T(1024)S(1)}, f32[4096]{0:T(1024)}, u32[]{:S(2)}) copy-start(f32[4096]{0:T(1024)} %param.23) | copy-start | bytes 49156
  0.6 0.8 copy-start.4
  1.4 18.7 %copy-start.5 = (bf16[4096,4]{0,1:T(4,128)(2,1)S(1)}, bf16[4096,4]{0,1:T(4,128)(2,1)}, u32[]{:S(2)}) copy-start(bf16[4096,4]{0,1:T(4,128)(2,1)} %param.28) | copy-start | bytes 98308
  1.4 18.7 %copy-start.6 = (bf16[4096,4]{0,1:T(4,128)(2,1)S(1)}, bf16[4096,4]{0,1:T(4,128)(2,1)}, u32[]{:S(2)}) copy-start(bf16[4096,4]{0,1:T(4,128)(2,1)} %param.29) | copy-start | bytes 98308
  1.4 18.7 %copy-start.9 = (f32[4,4]{1,0:T(4,128)S(1)}, f32[4,4]{1,0:T(4,128)}, u32[]{:S(2)}) copy-start(f32[4,4]{1,0:T(4,128)} %stab.1) | copy-start | bytes 196
  1.4 18.7 %copy-start.10 = (s32[4,2]{0,1:T(2,128)S(1)}, s32[4,2]{0,1:T(2,128)}, u32[]{:S(2)}) copy-start(s32[4,2]{0,1:T(2,128)} %param.36) | copy-start | bytes 100
  1.4 18.7 %copy-start.11 = (f32[4,2]{0,1:T(2,128)S(1)}, f32[4,2]{0,1:T(2,128)}, u32[]{:S(2)}) copy-start(f32[4,2]{0,1:T(2,128)} %param.37) | copy-start | bytes 100
  1.4 18.7 %copy-start.12 = (f32[4]{0:T(128)S(1)}, f32[4]{0:T(128)}, u32[]{:S(2)}) copy-start(f32[4]{0:T(128)} %param.30) | copy-start | bytes 52
  1.4 19.9 %copy-start.13 = (bf16[4096,4,32]{0,2,1:T(8,128)(2,1)S(1)}, bf16[4096,4,32]{0,2,1:T(8,128)(2,1)}, u32[]{:S(2)}) copy-start(bf16[4096,4,32]{0,2,1:T(8,128)(2,1)} %param.26) | copy-start | bytes 3145732
  1.5 19.9 %copy-start.14 = (bf16[4096,4,32]{0,2,1:T(8,128)(2,1)S(1)}, bf16[4096,4,32]{0,2,1:T(8,128)(2,1)}, u32[]{:S(2)}) copy-start(bf16[4096,4,32]{0,2,1:T(8,128)(2,1)} %param.27) | copy-start | bytes 3145732
  1.5 19.9 %copy-start.15 = (bf16[4096,4,16]{0,2,1:T(8,128)(2,1)S(1)}, bf16[4096,4,16]{0,2,1:T(8,128)(2,1)}, u32[]{:S(2)}) copy-start(bf16[4096,4,16]{0,2,1:T(8,128)(2,1)} %param.24) | copy-start | bytes 1572868
  1.5 19.9 %copy-start.16 = (bf16[4096,4,16]{0,2,1:T(8,128)(2,1)S(1)}, bf16[4096,4,16]{0,2,1:T(8,128)(2,1)}, u32[]{:S(2)}) copy-start(bf16[4096,4,16]{0,2,1:T(8,128)(2,1)} %param.25) | copy-start | bytes 1572868
  19.8 1.5 %collective-permute-start = (bf16[16,2,4096]{2,1,0:T(2,128)(2,1)S(1)}, bf16[16,2,4096]{2,1,0:T(2,128)(2,1)S(1)}, u32[]{:S(2)}, u32[]{:S(2)}) collective-permute-start(bf16[16,2,4096]{2,1,0:T(2,128)(2,1)S(1)} %all_to_all.25.own), channel_id=1, source_target_pairs={{0,1},{1,0},{2,3},{3,2},{4,5},{5,4},{6,7},{7,6},{8,9},{9,8},{10,11... | collective-permute-start | bytes 786440 | tf_op jit(solution)/shard_map/ppermute | solution.py:328
  21.3 12.5 %slice-start = ((s8[8388608]{0:T(1024)(128)(4,1)}), s8[4194304]{0:T(1024)(128)(4,1)S(1)}, s32[]{:S(2)}) async-start(s8[8388608]{0:T(1024)(128)(4,1)} %bitcast.19), calls=%async_computation.5 | async-start | bytes 8388608
  21.4 12.5 %slice-start.1 = ((s8[8388608]{0:T(1024)(128)(4,1)}), s8[4194304]{0:T(1024)(128)(4,1)S(1)}, s32[]{:S(2)}) async-start(s8[8388608]{0:T(1024)(128)(4,1)} %bitcast.19), calls=%async_computation.6 | async-start | bytes 8388608
  21.4 12.5 %copy-start.7 = (f32[4,4,256]{2,1,0:T(4,128)S(1)}, f32[4,4,256]{2,1,0:T(4,128)}, u32[]{:S(2)}) copy-start(f32[4,4,256]{2,1,0:T(4,128)} %norm.1) | copy-start | bytes 49156
  36.3 12.7 %all-to-all-start.2 = ((bf16[16,4,2048]{2,1,0:T(4,128)(2,1)}), bf16[16,4,2048]{2,1,0:T(4,128)(2,1)S(1)}, u32[]{:S(2)}, u32[]{:S(2)}) async-start(bf16[16,4,2048]{2,1,0:T(4,128)(2,1)} %get-tuple-element.29), calls=%async_computation.2 | async-start | bytes 524288 | tf_op jit(solution)/shard_map/all_to_all | solution.py:32
  49.1 16.1 %copy-start.8 = (f32[4096]{0:T(1024)S(1)}, f32[4096]{0:T(1024)}, u32[]{:S(2)}) copy-start(f32[4096]{0:T(1024)} %param.32) | copy-start | bytes 49156
  49.1 17.9 %copy-start = (bf16[1,256,4096]{2,1,0:T(8,128)(2,1)S(1)}, bf16[1,256,4096]{2,1,0:T(8,128)(2,1)}, u32[]{:S(2)}) copy-start(bf16[1,256,4096]{2,1,0:T(8,128)(2,1)} %w_down.3) | copy-start | bytes 6291460
  49.1 17.9 %copy-start.1 = (bf16[1,4096,256]{2,1,0:T(8,128)(2,1)S(1)}, bf16[1,4096,256]{2,1,0:T(8,128)(2,1)}, u32[]{:S(2)}) copy-start(bf16[1,4096,256]{2,1,0:T(8,128)(2,1)} %w_gate.1) | copy-start | bytes 6291460
  49.1 17.9 %copy-start.2 = (bf16[1,4096,256]{2,1,0:T(8,128)(2,1)S(1)}, bf16[1,4096,256]{2,1,0:T(8,128)(2,1)}, u32[]{:S(2)}) copy-start(bf16[1,4096,256]{2,1,0:T(8,128)(2,1)} %w_up.1) | copy-start | bytes 6291460
  49.5 1.2 %collective-permute-start.1 = (bf16[32,256]{1,0:T(8,128)(2,1)S(1)}, bf16[32,256]{1,0:T(8,128)(2,1)S(1)}, u32[]{:S(2)}, u32[]{:S(2)}) collective-permute-start(bf16[32,256]{1,0:T(8,128)(2,1)S(1)} %get-tuple-element.34), channel_id=1, source_target_pairs={{0,1},{1,0},{2,3},{3,2},{4,5},{5,4},{6,7},{7,6},{8,9},{9,8},{10,11... | collective-permute-start | bytes 49160 | tf_op jit(solution)/shard_map/ppermute | solution.py:416
  65.4 1.6 %collective-permute-start.2 = (bf16[32,4096]{1,0:T(8,128)(2,1)S(1)}, bf16[32,4096]{1,0:T(8,128)(2,1)S(1)}, u32[]{:S(2)}, u32[]{:S(2)}) collective-permute-start(bf16[32,4096]{1,0:T(8,128)(2,1)S(1)} %get-tuple-element.35.own), channel_id=1, source_target_pairs={{0,1},{1,0},{2,3},{3,2},{4,5},{5,4},{6,7},{7,6},{8,9},{9,8},{10,11... | collective-permute-start | bytes 786440 | tf_op jit(solution)/shard_map/ppermute | solution.py:427
  68.3 1.6 %collective-permute-start.3 = (bf16[32,4096]{1,0:T(8,128)(2,1)S(1)}, bf16[32,4096]{1,0:T(8,128)(2,1)S(1)}, u32[]{:S(2)}, u32[]{:S(2)}) collective-permute-start(bf16[32,4096]{1,0:T(8,128)(2,1)S(1)} %get-tuple-element.37), channel_id=1, source_target_pairs={{0,1},{1,0},{2,3},{3,2},{4,5},{5,4},{6,7},{7,6},{8,9},{9,8},{10,11... | collective-permute-start | bytes 786440 | tf_op jit(solution)/shard_map/ppermute | solution.py:446
  83.9 1.2 %collective-permute-start.4 = (bf16[2,4096]{1,0:T(2,128)(2,1)S(1)}, bf16[2,4096]{1,0:T(2,128)(2,1)S(1)}, u32[]{:S(2)}, u32[]{:S(2)}) collective-permute-start(bf16[2,4096]{1,0:T(2,128)(2,1)S(1)} %finish.1.mine), channel_id=1, source_target_pairs={{0,1},{1,0},{2,3},{3,2},{4,5},{5,4},{6,7},{7,6},{8,9},{9,8},{10,11... | collective-permute-start | bytes 49160 | tf_op jit(solution)/shard_map/ppermute | solution.py:459
